TPU v7x, 32 devices: a whole 2x2x4 slice. The times are simulated.
32 devices in a mesh: ep: 8 (over z, x), tp: 4 (over y, core).
Axes of the slice: x: 2, y: 2, z: 4, core: 2. Of those that a mesh axis runs over, the one named last changes fastest.
Arguments:
- queries: bfloat16 [2048, 1024], P('ep', 'tp'), may hold values from -256 to 256
- key_rows: bfloat16 [2048, 1024], P('ep', 'tp'), may hold values from -8 to 8
- value_rows: bfloat16 [2048, 1024], P('ep', 'tp'), may hold values from -6 to 6
- head_lambda: float32 [8], P('tp'), may hold values from 0.3 to 0.8
- sub_gain: float32 [128], replicated, may hold values from 0.1 to 1.9
- out_weight: bfloat16 [1024, 2048], P('tp'), may hold values from -0.1875 to 0.1875
- expert_input: bfloat16 [1536, 2048], P('ep'), may hold values from -6 to 6
- norm_gain: float32 [2048], replicated, may hold values from 0.1 to 1.9
- route_ids: int32 [1536, 2], P('ep'), may hold values from 0 to 7, all different within a row; in each aligned block of 192 rows (0 to 191, 192 to 383, ...) at most 80 rows name the same one
- route_weight: float32 [1536, 2], P('ep'), may hold values from 0.25 to 1
- gate_weight: bfloat16 [8, 2048, 3584], P('ep', None, 'tp'), may hold values from -0.125 to 0.125
- up_weight: bfloat16 [8, 2048, 3584], P('ep', None, 'tp'), may hold values from -0.125 to 0.125
- down_weight: bfloat16 [8, 3584, 2048], P('ep', 'tp'), may hold values from -0.09375 to 0.09375
Outputs:
- mixer_out: bfloat16 [2048, 2048], P(('ep', 'tp'))
- expert_out: bfloat16 [1536, 2048], P('ep', 'tp')
Inputs may be any that keep to these rules, and one draw needn't show every extreme that they name: `route_ids`: each row names 2 different experts. In each aligned block of 192 rows no expert is named by more than 80 rows, a bound that some block reaches.
All inputs are finite; a program needn't handle non-finite values.
Results may differ from a plain program's by a relative error of at most 0.014.
Values may be sent and summed in bfloat16 or wider, within the bound.
No kernel may reach another device: no remote copies, remote signals or barrier semaphores. Data moves between devices by JAX's collectives and lax.ppermute only.
A program may use at most 256 MiB of HBM per device.

v0:
```python
import jax
import jax.numpy as jnp
from jax import lax
from jax.sharding import PartitionSpec as P

EPS = 1e-06


def mixer_half(queries, key_rows, value_rows, head_lambda, sub_gain, out_weight):
    rows_here = queries.shape[0]
    heads_here = head_lambda.shape[0]
    head_width = queries.shape[1] // (2 * heads_here)
    value_width = value_rows.shape[1] // heads_here
    scaling = head_width ** (-0.5)
    query_blocks = queries.reshape(rows_here, heads_here, 2, head_width)
    query_pos = lax.axis_index("ep") * rows_here + jnp.arange(rows_here, dtype=jnp.int32)
    row_max = jnp.full((heads_here, 2, rows_here), -1e30, jnp.float32)
    key_piece = lax.all_gather(key_rows, "ep", axis=0, tiled=True)
    value_piece = lax.all_gather(value_rows, "ep", axis=0, tiled=True)
    length = key_piece.shape[0]
    key_blocks = key_piece.reshape(length, heads_here, 2, head_width)
    value_blocks = value_piece.reshape(length, heads_here, value_width)
    scores = (
        jnp.einsum("qhmd,khmd->hmqk", query_blocks, key_blocks, preferred_element_type=jnp.float32)
        * scaling
    )
    allowed = query_pos[:, None] >= jnp.arange(length, dtype=jnp.int32)[None, :]
    scores = jnp.where(allowed, scores, -1e30)
    new_max = jnp.maximum(row_max, jnp.max(scores, axis=-1))
    weights = jnp.where(allowed, jnp.exp(scores - new_max[..., None]), 0.0)
    row_total = jnp.sum(weights, axis=-1)
    numerator = jnp.einsum(
        "hmqk,khd->hmqd",
        weights.astype(jnp.bfloat16),
        value_blocks,
        preferred_element_type=jnp.float32,
    )
    row_max, row_total, numerator = (new_max, row_total, numerator)
    per_map = numerator / row_total[..., None]
    contrast = per_map[:, 0] - head_lambda[:, None, None] * per_map[:, 1]
    normed = (
        contrast * lax.rsqrt(jnp.mean(contrast * contrast, axis=-1, keepdims=True) + EPS) * sub_gain
    ).astype(jnp.bfloat16)
    attended = jnp.transpose(normed, (1, 0, 2)).reshape(rows_here, heads_here * value_width)
    return lax.psum_scatter(
        jnp.dot(attended, out_weight, preferred_element_type=jnp.float32).astype(jnp.bfloat16),
        "tp",
        scatter_dimension=0,
        tiled=True,
    )


def expert_half(
    expert_input, norm_gain, route_ids, route_weight, gate_weight, up_weight, down_weight
):
    rows_here, model_width = expert_input.shape
    experts = lax.axis_size("ep")
    top_count = route_ids.shape[1]
    capacity = 5 * top_count * rows_here // (3 * experts)
    slots = experts * capacity
    wide_rows = expert_input.astype(jnp.float32)
    normed = (
        wide_rows
        * lax.rsqrt(jnp.mean(wide_rows * wide_rows, axis=-1, keepdims=True) + EPS)
        * norm_gain
    ).astype(jnp.bfloat16)
    flat_ids = route_ids.reshape(-1)
    onehot = (flat_ids[:, None] == jnp.arange(experts, dtype=jnp.int32)[None, :]).astype(jnp.int32)
    rank_before = jnp.cumsum(onehot, axis=0) - onehot
    slot_index = jnp.sum(rank_before * onehot, axis=1)
    buffer_pos = (flat_ids * capacity + slot_index).reshape(rows_here, top_count)
    matches = buffer_pos[None, :, :] == jnp.arange(slots, dtype=jnp.int32)[:, None, None]
    dispatch = jnp.any(matches, axis=-1).astype(jnp.bfloat16)
    combine = jnp.sum(jnp.where(matches, route_weight[None, :, :], 0.0), axis=-1)
    gate_mat = gate_weight[0]
    up_mat = up_weight[0]
    down_mat = down_weight[0]
    outgoing = jnp.dot(dispatch, normed, preferred_element_type=jnp.float32).astype(jnp.bfloat16)
    arrived = lax.all_to_all(
        outgoing.reshape(experts, capacity, model_width),
        "ep",
        split_axis=0,
        concat_axis=0,
        tiled=True,
    ).reshape(slots, model_width)
    gate_act = jnp.dot(arrived, gate_mat, preferred_element_type=jnp.float32)
    up_act = jnp.dot(arrived, up_mat, preferred_element_type=jnp.float32)
    hidden = (jax.nn.silu(gate_act) * up_act).astype(jnp.bfloat16)
    partial_result = jnp.dot(hidden, down_mat, preferred_element_type=jnp.float32)
    summed = lax.psum_scatter(
        partial_result.astype(jnp.bfloat16), "tp", scatter_dimension=1, tiled=True
    )
    col_count = summed.shape[1]
    returned = lax.all_to_all(
        summed.reshape(experts, capacity, col_count), "ep", split_axis=0, concat_axis=0, tiled=True
    ).reshape(slots, col_count)
    mixed = lax.dot_general(
        combine,
        returned.astype(jnp.float32),
        (((0,), (0,)), ((), ())),
        precision=lax.Precision.HIGHEST,
        preferred_element_type=jnp.float32,
    )
    return mixed.astype(jnp.bfloat16)


def shards(
    queries,
    key_rows,
    value_rows,
    head_lambda,
    sub_gain,
    out_weight,
    expert_input,
    norm_gain,
    route_ids,
    route_weight,
    gate_weight,
    up_weight,
    down_weight,
):
    mixer_out = mixer_half(queries, key_rows, value_rows, head_lambda, sub_gain, out_weight)
    expert_out = expert_half(
        expert_input, norm_gain, route_ids, route_weight, gate_weight, up_weight, down_weight
    )
    return (mixer_out, expert_out)


def solution(mesh):
    placed = (
        P("ep", "tp"),
        P("ep", "tp"),
        P("ep", "tp"),
        P("tp"),
        P(),
        P("tp", None),
        P("ep", None),
        P(),
        P("ep", None),
        P("ep", None),
        P("ep", None, "tp"),
        P("ep", None, "tp"),
        P("ep", "tp", None),
    )
    return jax.shard_map(
        shards,
        mesh=mesh,
        in_specs=placed,
        out_specs=(P(("ep", "tp"), None), P("ep", "tp")),
        check_vma=False,
    )
```

profile of v0, /device:TPU:0, one launch (start us, length us, event | category | flops | bytes accessed | tf_op | source)
XLA Modules:
  0.0 183.7 jit_solution(2173405152536160842)
XLA Ops:
  8.0 0.9 copy.43
  9.2 0.9 reduce-window.6
  10.6 0.7 multiply_add_fusion
  11.5 1.4 fusion.17
  12.9 3.6 %convolution_convert_fusion = bf16[640,2048]{1,0:T(8,128)(2,1)} fusion(pred[640,192]{0,1:T(8,128)(4,1)S(1)} %fusion.23, bf16[192,2048]{1,0:T(8,128)(2,1)} %param.19, f32[2048]{0:T(1024)} %param.20, f32[192]{0:T(256)S(1)} %add_rsqrt_fusion.1), kind=kOutput, calls=%fused_computation.14 | convolution fusion | flops 506200064 | bytes 3539712 | tf_op jit(solution)/shard_map/dot_general | solution.py:78
  16.5 7.3 %all-to-all-start = ((bf16[8,80,2048]{2,1,0:T(8,128)(2,1)}), bf16[8,80,2048]{2,1,0:T(8,128)(2,1)}, u32[]{:S(2)}, u32[]{:S(2)}) async-start(bf16[8,80,2048]{2,1,0:T(8,128)(2,1)} %bitcast.68), calls=%async_computation.1 | async-start | bytes 5242880 | tf_op jit(solution)/shard_map/all_to_all | solution.py:79
  23.8 0.7 all-gather.3.cloned.1.call-update
  24.6 0.7 all-gather.5.cloned.1.call-update
  25.3 70.7 %all-to-all-done = bf16[8,80,2048]{2,1,0:T(8,128)(2,1)} async-done(((bf16[8,80,2048]{2,1,0:T(8,128)(2,1)}), bf16[8,80,2048]{2,1,0:T(8,128)(2,1)}, u32[]{:S(2)}, u32[]{:S(2)}) %all-to-all-start) | async-done | bytes 2621472 | tf_op jit(solution)/shard_map/all_to_all | solution.py:79
  96.0 7.2 %fusion.10 = f32[640,896]{1,0:T(8,128)} fusion(bf16[640,2048]{1,0:T(8,128)(2,1)} %bitcast.12, bf16[1,2048,896]{2,1,0:T(8,128)(2,1)} %param.23), kind=kOutput, calls=%fused_computation.11 | convolution fusion | flops 2348810240 | bytes 8585216 | tf_op jit(solution)/shard_map/dot_general | solution.py:86
  103.2 11.8 %fusion.12 = bf16[640,2048]{1,0:T(8,128)(2,1)} fusion(bf16[1,896,2048]{2,1,0:T(8,128)(2,1)} %param.25, f32[640,896]{1,0:T(8,128)} %fusion.10, bf16[640,2048]{1,0:T(8,128)(2,1)} %bitcast.12, bf16[1,2048,896]{2,1,0:T(8,128)(2,1)} %param.24), kind=kOutput, calls=%fused_computation.13 | convolution fusion | flops 4702371840 | bytes 14876672 | tf_op jit(solution)/shard_map/dot_general | solution.py:89
  115.4 0.4 iota_compare_fusion
  115.8 1.5 copy.40
  117.3 11.8 %all-gather.5.cloned.1.call-done = bf16[2048,256]{1,0:T(8,128)(2,1)} async-done(((bf16[256,256]{1,0:T(8,128)(2,1)}), bf16[2048,256]{1,0:T(8,128)(2,1)}) %all-gather.5.cloned.1.call-update) | async-done | bytes 1048592 | tf_op jit(solution)/shard_map/all_gather | solution.py:19
  129.1 2.3 %copy.41 = bf16[2048,256]{0,1:T(8,128)(2,1)} copy(bf16[2048,256]{1,0:T(8,128)(2,1)} %all-gather.5.cloned.1.call-done) | data formatting | bytes 2097152 | tf_op jit(solution)/shard_map/all_gather | solution.py:19
  131.3 1.8 fusion
  133.1 2.5 %fusion.1 = f32[2,2,256]{2,1,0:T(2,128)S(1)} fusion(f32[2,2,256,2048]{3,2,1,0:T(8,128)S(1)} %get-tuple-element.3, f32[2,2,256]{2,1,0:T(2,128)S(1)} %broadcast_maximum_fusion, pred[256,2048]{1,0:T(8,128)(4,1)S(1)} %iota_compare_fusion), kind=kLoop, calls=%fused_computation.3 | loop fusion | flops 10484736 | bytes 8921088 | tf_op jit(solution)/shard_map/reduce_sum | solution.py:31
  135.6 2.2 %fusion.20 = f32[2,2,256,128]{2,3,1,0:T(8,128)S(1)} fusion(bf16[2048,2,128,1]{0,2,3,1:T(8,128)(2,1)S(1)} %bitcast.71, f32[2,2,256,2048]{3,2,1,0:T(8,128)S(1)} %get-tuple-element.3, f32[2,2,256]{2,1,0:T(2,128)S(1)} %broadcast_maximum_fusion, pred[256,2048]{1,0:T(8,128)(4,1)S(1)} %iota_compare_fusion, f32[2,2,256]{2,1,0:T(2,128)S(1)} %fusion.1), kind=kOutput, calls=%fused_computation.24 | convolution fusion | flops 547487744 | bytes 10493952 | tf_op jit(solution)/shard_map/hmqk,khd->hmqd/dot_general | solution.py:32
  138.2 1.5 convolution_convert_fusion.1
  139.7 8.8 %reduce-scatter.5.cloned.1.call-done = bf16[640,512]{1,0:T(8,128)(2,1)} async-done(((bf16[640,2048]{1,0:T(8,128)(2,1)}), bf16[640,512]{1,0:T(8,128)(2,1)}) %reduce-scatter.5.cloned.1.call-update) | async-done | bytes 655376 | tf_op jit(solution)/shard_map/reduce_scatter | solution.py:90
  148.5 5.5 %all-to-all-start.1 = ((bf16[8,80,512]{2,1,0:T(8,128)(2,1)}), bf16[8,80,512]{2,1,0:T(8,128)(2,1)S(1)}, u32[]{:S(2)}, u32[]{:S(2)}) async-start(bf16[8,80,512]{2,1,0:T(8,128)(2,1)} %bitcast.72), calls=%async_computation.3 | async-start | bytes 1310720 | tf_op jit(solution)/shard_map/all_to_all | solution.py:94
  154.2 16.9 %all-to-all-done.1 = bf16[8,80,512]{2,1,0:T(8,128)(2,1)S(1)} async-done(((bf16[8,80,512]{2,1,0:T(8,128)(2,1)}), bf16[8,80,512]{2,1,0:T(8,128)(2,1)S(1)}, u32[]{:S(2)}, u32[]{:S(2)}) %all-to-all-start.1) | async-done | bytes 655392 | tf_op jit(solution)/shard_map/all_to_all | solution.py:94
  171.1 1.3 convolution_convert_fusion.2
  172.4 3.9 %reduce-scatter.3.cloned.1.call-done = bf16[64,2048]{1,0:T(8,128)(2,1)} async-done(((bf16[256,2048]{1,0:T(8,128)(2,1)}), bf16[64,2048]{1,0:T(8,128)(2,1)}) %reduce-scatter.3.cloned.1.call-update) | async-done | bytes 262160 | tf_op jit(solution)/shard_map/reduce_scatter | solution.py:45
  (36 shorter events, 2.0 us)
Async XLA Ops:
  8.0 130.2 %copy-start = (bf16[256,2048]{1,0:T(8,128)(2,1)S(1)}, bf16[256,2048]{1,0:T(8,128)(2,1)}, u32[]{:S(2)}) copy-start(bf16[256,2048]{1,0:T(8,128)(2,1)} %param.18) | copy-start | bytes 3145732
  16.5 79.5 %all-to-all-start = ((bf16[8,80,2048]{2,1,0:T(8,128)(2,1)}), bf16[8,80,2048]{2,1,0:T(8,128)(2,1)}, u32[]{:S(2)}, u32[]{:S(2)}) async-start(bf16[8,80,2048]{2,1,0:T(8,128)(2,1)} %bitcast.68), calls=%async_computation.1 | async-start | bytes 5242880 | tf_op jit(solution)/shard_map/all_to_all | solution.py:79
  23.8 92.0 %all-gather.3.cloned.1.call-start = ((), (), s32[]{:S(2)}) async-start(), calls=%async_computation.4 | async-start | bytes 1179648 | tf_op jit(solution)/shard_map/all_gather | solution.py:18
  24.5 104.6 %all-gather.5.cloned.1.call-start = ((), (), s32[]{:S(2)}) async-start(), calls=%async_computation.5 | async-start | bytes 1179648 | tf_op jit(solution)/shard_map/all_gather | solution.py:19
  25.3 123.2 %reduce-scatter.5.cloned.1.call-start = ((), (), s32[]{:S(2)}) async-start(), calls=%async_computation.7 | async-start | bytes 3276800 | tf_op jit(solution)/shard_map/reduce_scatter | solution.py:90
  103.2 12.1 %copy-start.2 = (bf16[256,256]{1,0:T(8,128)(2,1)S(1)}, bf16[256,256]{1,0:T(8,128)(2,1)}, u32[]{:S(2)}) copy-start(bf16[256,256]{1,0:T(8,128)(2,1)} %param.13) | copy-start | bytes 393220
  115.0 61.2 %reduce-scatter.3.cloned.1.call-start = ((), (), s32[]{:S(2)}) async-start(), calls=%async_computation.6 | async-start | bytes 1310720 | tf_op jit(solution)/shard_map/reduce_scatter | solution.py:45
  133.1 2.5 %copy-start.1 = (bf16[2048,256]{0,1:T(8,128)(2,1)S(1)}, bf16[2048,256]{0,1:T(8,128)(2,1)}, u32[]{:S(2)}) copy-start(bf16[2048,256]{0,1:T(8,128)(2,1)} %copy.41) | copy-start | bytes 3145732
  135.6 2.3 %copy-start.4 = (f32[2]{0:T(128)S(1)}, f32[2]{0:T(128)}, u32[]{:S(2)}) copy-start(f32[2]{0:T(128)} %param.16) | copy-start | bytes 28
  135.6 2.4 %copy-start.5 = (f32[128]{0:T(128)S(1)}, f32[128]{0:T(128)}, u32[]{:S(2)}) copy-start(f32[128]{0:T(128)} %param.17) | copy-start | bytes 1540
  137.9 16.1 %copy-start.3 = (f32[192,2]{0,1:T(2,128)S(1)}, f32[192,2]{0,1:T(2,128)}, u32[]{:S(2)}) copy-start(f32[192,2]{0,1:T(2,128)} %param.22) | copy-start | bytes 4612
  148.5 22.6 %all-to-all-start.1 = ((bf16[8,80,512]{2,1,0:T(8,128)(2,1)}), bf16[8,80,512]{2,1,0:T(8,128)(2,1)S(1)}, u32[]{:S(2)}, u32[]{:S(2)}) async-start(bf16[8,80,512]{2,1,0:T(8,128)(2,1)} %bitcast.72), calls=%async_computation.3 | async-start | bytes 1310720 | tf_op jit(solution)/shard_map/all_to_all | solution.py:94
Sparse Core Ops, SparseCore 0:
  26.7 60.7 all-gather.2
  89.7 39.3 all-gather.4
Sparse Core Ops, SparseCore 1:
  115.1 33.3 reduce-scatter.4
  151.5 24.7 reduce-scatter.2
where the time goes:
time: 184 us
  waiting for transfers between devices  113 us (61%)
  matrix products  29.4 us (16%)
  between operations  15.7 us (9%)
  starting transfers between devices  13.2 us (7%)
  other arithmetic  6.48 us (4%)
  local copies, waits for them, and re-layouts  5.48 us (3%)
    all_to_all x1, waiting for transfers between devices, expert_half(): lax.all_to_all(outgoing.reshape(experts, capacity, model_width), 'ep', sp...  70.7 us
    all_to_all x1, waiting for transfers between devices, expert_half(): lax.all_to_all(summed.reshape(experts, capacity, col_count), 'ep', split_...  16.9 us
    dot_general x1, matrix products, expert_half(): jnp.dot(hidden, down_mat, preferred_element_type=jnp.float32)  11.8 us
    all_gather x1, waiting for transfers between devices, mixer_half(): value_piece = lax.all_gather(value_rows, 'ep', axis=0, tiled=True)  11.8 us
    reduce_scatter x1, waiting for transfers between devices, expert_half(): lax.psum_scatter(partial_result.astype(jnp.bfloat16), 'tp', scatter_dimen...  8.83 us
    all_to_all x1, starting transfers between devices, expert_half(): lax.all_to_all(outgoing.reshape(experts, capacity, model_width), 'ep', sp...  7.28 us
    dot_general x1, matrix products, expert_half(): gate_act = jnp.dot(arrived, gate_mat, preferred_element_type=jnp.float32)  7.18 us
    all_to_all x1, starting transfers between devices, expert_half(): lax.all_to_all(summed.reshape(experts, capacity, col_count), 'ep', split_...  5.54 us
  transfers between devices with their start and end apart: 6, of which 5 were waited for; matrix products, arithmetic and copies ran while one was open for 18% of the time, Pallas kernels for 0%

commit v1 on v0

v1 whole, which is shorter than its diff:
```python
import functools

import jax
import jax.numpy as jnp
from jax import lax
from jax.experimental import pallas as pl
from jax.experimental.pallas import tpu as pltpu
from jax.sharding import PartitionSpec as P

EPS = 1e-06
F32 = jnp.float32
BF16 = jnp.bfloat16


def swap(x, axis, mask):
    count = lax.axis_size(axis)
    return lax.ppermute(x, axis, [(i, i ^ mask) for i in range(count)])


def later(x, axis, step):
    count = lax.axis_size(axis)
    return lax.ppermute(x, axis, [(i, i + step) for i in range(count - step)])


def gathered_keys(key_rows, value_rows):
    rows_here, width = key_rows.shape
    count = lax.axis_size("ep")
    own = jnp.concatenate([key_rows, value_rows], axis=1)
    here = lax.axis_index("ep")
    if count > 8 or count % 2:
        both = lax.all_gather(own, "ep", axis=0, tiled=True)
        return both, jnp.arange(count, dtype=jnp.int32)
    pieces = [own] + [later(own, "ep", 2 * k) for k in range(1, count // 2)]
    line = jnp.concatenate(pieces, axis=0)
    other = swap(line, "ep", 1)
    steps = 2 * jnp.arange(count // 2, dtype=jnp.int32)
    places = jnp.concatenate([here - steps, (here ^ 1) - steps])
    return jnp.concatenate([line, other], axis=0), places


def attention(queries, both, places, head_lambda, sub_gain, out_weight):
    rows_here = queries.shape[0]
    heads_here = head_lambda.shape[0]
    head_width = queries.shape[1] // (2 * heads_here)
    width = queries.shape[1]
    value_width = (both.shape[1] - width) // heads_here
    scaling = head_width ** (-0.5)
    length = both.shape[0]
    query_blocks = queries.reshape(rows_here, heads_here, 2, head_width)
    query_pos = lax.axis_index("ep") * rows_here + jnp.arange(rows_here, dtype=jnp.int32)
    key_pos = (
        places[:, None] * rows_here + jnp.arange(rows_here, dtype=jnp.int32)[None, :]
    ).reshape(length)
    key_blocks = both[:, :width].reshape(length, heads_here, 2, head_width)
    value_blocks = both[:, width:].reshape(length, heads_here, value_width)
    scores = (
        jnp.einsum("qhmd,khmd->hmqk", query_blocks, key_blocks, preferred_element_type=F32)
        * scaling
    )
    allowed = (query_pos[:, None] >= key_pos[None, :]) & (key_pos[None, :] >= 0)
    scores = jnp.where(allowed, scores, -1e30)
    row_max = jnp.max(scores, axis=-1)
    weights = jnp.where(allowed, jnp.exp(scores - row_max[..., None]), 0.0)
    row_total = jnp.sum(weights, axis=-1)
    numerator = jnp.einsum(
        "hmqk,khd->hmqd", weights.astype(BF16), value_blocks, preferred_element_type=F32
    )
    per_map = numerator / row_total[..., None]
    contrast = per_map[:, 0] - head_lambda[:, None, None] * per_map[:, 1]
    normed = (
        contrast * lax.rsqrt(jnp.mean(contrast * contrast, axis=-1, keepdims=True) + EPS) * sub_gain
    ).astype(BF16)
    attended = jnp.transpose(normed, (1, 0, 2)).reshape(rows_here, heads_here * value_width)
    return jnp.dot(attended, out_weight, preferred_element_type=F32).astype(BF16)


def dispatch_kernel(
    experts, capacity, place_ref, ids_ref, rows_ref, gain_ref, out_ref, onehot_ref
):
    rows, width = rows_ref.shape
    cols = out_ref.shape[1]
    first = pl.multiple_of(place_ref[0] * cols, cols)
    wide = rows_ref[...].astype(F32)
    scale = lax.rsqrt(jnp.mean(wide * wide, axis=-1, keepdims=True) + EPS)
    part = rows_ref[:, pl.ds(first, cols)].astype(F32)
    normed = (part * scale * gain_ref[:, pl.ds(first, cols)]).astype(BF16)
    numbers = lax.broadcasted_iota(jnp.int32, (experts, rows), 0)
    named = (ids_ref[0:1, :] == numbers) | (ids_ref[1:2, :] == numbers)
    before = (
        lax.broadcasted_iota(jnp.int32, (rows, rows), 0)
        < lax.broadcasted_iota(jnp.int32, (rows, rows), 1)
    ).astype(F32).astype(BF16)
    rank = jnp.dot(named.astype(F32).astype(BF16), before, preferred_element_type=F32)
    rank = jnp.where(named, rank, -1.0)
    slot = lax.broadcasted_iota(jnp.int32, (capacity, rows), 0).astype(F32)
    for e in range(experts):
        onehot_ref[e * capacity : (e + 1) * capacity, :] = (
            rank[e : e + 1, :] == slot
        ).astype(F32)
    out_ref[...] = jnp.dot(
        onehot_ref[...].astype(BF16), normed, preferred_element_type=F32
    ).astype(BF16)


def dispatched(expert_input, norm_gain, ids_across, capacity):
    rows, width = expert_input.shape
    experts = lax.axis_size("ep")
    cols = width // lax.axis_size("tp")
    slots = experts * capacity
    vmem = pl.BlockSpec(memory_space=pltpu.VMEM)
    return pl.pallas_call(
        functools.partial(dispatch_kernel, experts, capacity),
        out_shape=jax.ShapeDtypeStruct((slots, cols), BF16),
        in_specs=[pl.BlockSpec(memory_space=pltpu.SMEM), vmem, vmem, vmem],
        out_specs=vmem,
        scratch_shapes=[pltpu.VMEM((slots, rows), F32)],
        cost_estimate=pl.CostEstimate(
            flops=2 * slots * rows * cols, bytes_accessed=2 * rows * width, transcendentals=rows
        ),
        name="dispatch",
    )(
        lax.axis_index("tp").astype(jnp.int32).reshape(1),
        ids_across,
        expert_input,
        norm_gain.reshape(1, width),
    )


def ffn_kernel(
    order_ref, x0, x1, x2, x3, gate_ref, up_ref, down_ref, keep_ref, send_ref, acc_g, acc_u, hidden
):
    step = pl.program_id(0)
    for k, x_ref in enumerate((x0, x1, x2, x3)):

        @pl.when(step == k)
        def _(k=k, x_ref=x_ref):
            gate = jnp.dot(x_ref[...], gate_ref[0], preferred_element_type=F32)
            up = jnp.dot(x_ref[...], up_ref[0], preferred_element_type=F32)
            if k:
                gate += acc_g[...]
                up += acc_u[...]
            if k < 3:
                acc_g[...] = gate
                acc_u[...] = up
            else:
                hidden[...] = (gate / (1.0 + jnp.exp(-gate)) * up).astype(BF16)

    @pl.when((step == 4) | (step == 5))
    def _():
        send_ref[...] = jnp.dot(hidden[...], down_ref[0], preferred_element_type=F32).astype(BF16)

    @pl.when(step >= 6)
    def _():
        keep_ref[...] = jnp.dot(hidden[...], down_ref[0], preferred_element_type=F32).astype(BF16)


def ffn(order, pieces, gate_weight, up_weight, down_weight):
    rows, cols = pieces[0].shape
    width, units = gate_weight.shape[1:]

    def clamp(i, low, high):
        return jnp.minimum(jnp.maximum(i, low), high)

    def whole():
        return pl.BlockSpec((rows, cols), lambda i, order: (0, 0))

    def weight_in():
        return pl.BlockSpec((1, cols, units), lambda i, order: (0, order[clamp(i, 0, 3)], 0))

    return pl.pallas_call(
        ffn_kernel,
        grid_spec=pltpu.PrefetchScalarGridSpec(
            num_scalar_prefetch=1,
            grid=(8,),
            in_specs=[whole(), whole(), whole(), whole(), weight_in(), weight_in()]
            + [
                pl.BlockSpec(
                    (1, units, cols), lambda i, order: (0, 0, order[4 + clamp(i - 4, 0, 3)])
                )
            ],
            out_specs=[
                pl.BlockSpec((rows, cols), lambda i, order: (0, clamp(i - 6, 0, 1))),
                pl.BlockSpec((rows, cols), lambda i, order: (0, clamp(i - 4, 0, 1))),
            ],
            scratch_shapes=[
                pltpu.VMEM((rows, units), F32),
                pltpu.VMEM((rows, units), F32),
                pltpu.VMEM((rows, units), BF16),
            ],
        ),
        out_shape=[jax.ShapeDtypeStruct((rows, 2 * cols), BF16)] * 2,
        compiler_params=pltpu.CompilerParams(
            dimension_semantics=("arbitrary",), vmem_limit_bytes=40 * 1024 * 1024
        ),
        cost_estimate=pl.CostEstimate(
            flops=6 * rows * width * units,
            bytes_accessed=6 * width * units + 8 * rows * width,
            transcendentals=rows * units,
        ),
        name="ffn",
    )(order, *pieces, gate_weight, up_weight, down_weight)


def combine_weights(ids_across, weight_across, capacity):
    experts = lax.axis_size("ep")
    rows = ids_across.shape[1]
    numbers = jnp.arange(experts, dtype=jnp.int32)[:, None]
    first = ids_across[0:1] == numbers
    second = ids_across[1:2] == numbers
    named = first | second
    before = jnp.triu(jnp.ones((rows, rows), BF16), 1)
    rank = jnp.dot(named.astype(BF16), before, preferred_element_type=F32)
    weight = jnp.where(first, weight_across[0:1], 0.0) + jnp.where(second, weight_across[1:2], 0.0)
    slot = jnp.arange(capacity, dtype=jnp.int32).astype(F32)[None, :, None]
    held = (rank[:, None, :] == slot) & named[:, None, :]
    return jnp.where(held, weight[:, None, :], 0.0).reshape(experts * capacity, rows)


def shards(
    queries,
    key_rows,
    value_rows,
    head_lambda,
    sub_gain,
    out_weight,
    expert_input,
    norm_gain,
    route_ids,
    route_weight,
    gate_weight,
    up_weight,
    down_weight,
):
    rows_b, width = expert_input.shape
    experts = lax.axis_size("ep")
    capacity = 5 * route_ids.shape[1] * rows_b // (3 * experts)
    slots = experts * capacity
    place = lax.axis_index("tp").astype(jnp.int32)
    cols = width // lax.axis_size("tp")
    ids_across = route_ids.T
    weight_across = route_weight.T

    outgoing = dispatched(expert_input, norm_gain, ids_across, capacity)
    own = lax.all_to_all(
        outgoing.reshape(experts, capacity, cols), "ep", split_axis=0, concat_axis=0, tiled=True
    ).reshape(slots, cols)
    far = swap(own, "tp", 2)
    near = swap(own, "tp", 1)
    near_far = swap(far, "tp", 1)

    key_in, value_in, own_done = lax.optimization_barrier((key_rows, value_rows, own))
    both, places = gathered_keys(key_in, value_in)
    share = attention(queries, both, places, head_lambda, sub_gain, out_weight)
    parts = lax.all_to_all(
        share.reshape(lax.axis_size("tp"), -1, share.shape[1]), "tp", 0, 0, tiled=True
    )
    mixer_out = jnp.sum(parts.astype(F32), axis=0).astype(BF16)

    order = jnp.array([0, 1, 2, 3, 1, 3, 0, 2], jnp.int32) ^ place
    keep, send = ffn(order, (own, near, far, near_far), gate_weight, up_weight, down_weight)
    got = swap(send, "tp", 1)
    across = (keep[:, cols:].astype(F32) + got[:, cols:].astype(F32)).astype(BF16)
    got_across = swap(across, "tp", 2)
    mine = keep[:, :cols].astype(F32) + got[:, :cols].astype(F32)
    summed = (mine + got_across.astype(F32)).astype(BF16)
    returned = lax.all_to_all(
        summed.reshape(experts, capacity, cols), "ep", split_axis=0, concat_axis=0, tiled=True
    ).reshape(slots, cols)
    mixed = lax.dot_general(
        combine_weights(ids_across, weight_across, capacity),
        returned.astype(F32),
        (((0,), (0,)), ((), ())),
        precision=lax.Precision.HIGHEST,
        preferred_element_type=F32,
    )
    return (mixer_out, mixed.astype(BF16))


def solution(mesh):
    placed = (
        P("ep", "tp"),
        P("ep", "tp"),
        P("ep", "tp"),
        P("tp"),
        P(),
        P("tp", None),
        P("ep", None),
        P(),
        P("ep", None),
        P("ep", None),
        P("ep", None, "tp"),
        P("ep", None, "tp"),
        P("ep", "tp", None),
    )
    return jax.shard_map(
        shards,
        mesh=mesh,
        in_specs=placed,
        out_specs=(P(("ep", "tp"), None), P("ep", "tp")),
        check_vma=False,
    )
```

time: 184 us -> 159 us (0.86)
  waiting for transfers between devices: 113 us -> 63.9 us
  starting transfers between devices: 13.2 us -> 32.3 us
  Pallas kernels: 0 us -> 16.5 us
  local copies, waits for them, and re-layouts: 5.48 us -> 21.9 us
  matrix products: 29.4 us -> 13.8 us
  between operations: 15.7 us -> 0.84 us
  other arithmetic: 6.48 us -> 9.31 us
    all_to_all x2 -> x3, waiting for transfers between devices: 87.6 us -> 41.3 us  [the longest x1 17.1 us: shards(): lax.all_to_all(outgoing.reshape(experts, capacity, cols), 'ep', split_axi...]
    dot_general x7 -> x4, matrix products: 29.4 us -> 6.35 us  [the longest x1 3.24 us: attention(): jnp.einsum('hmqk,khd->hmqd', weights.astype(BF16), value_blocks, preferre...]
    ppermute x0 -> x9, waiting for transfers between devices: none -> 22.6 us  [the longest x6 15.3 us: swap(): return lax.ppermute(x, axis, [(i, i ^ mask) for i in range(count)])]
    pallas_call x0 -> x2, Pallas kernels: none -> 16.5 us  [the longest x1 13.8 us: ffn(): pl.pallas_call(ffn_kernel, grid_spec=pltpu.PrefetchScalarGridSpec(num_sca...]
    reduce_scatter x2 -> x0, waiting for transfers between devices: 12.7 us -> none  [the longest x1 8.83 us: expert_half(): lax.psum_scatter(partial_result.astype(jnp.bfloat16), 'tp', scatter_dimen...]
    all_gather x2 -> x0, waiting for transfers between devices: 11.8 us -> none  [the longest x1 11.8 us: mixer_half(): value_piece = lax.all_gather(value_rows, 'ep', axis=0, tiled=True)]
    unnamed x14 -> x38, local copies, waits for them, and re-layouts: 1.02 us -> 12.6 us
    ppermute x0 -> x9, starting transfers between devices: none -> 11.1 us  [the longest x3 6.87 us: later(): return lax.ppermute(x, axis, [(i, i + step) for i in range(count - step)])]
  transfers between devices with their start and end apart: 6 -> 12, of which waited for: 5 -> 7; matrix products, arithmetic and copies ran while one was open for 18% -> 22% of each run, Pallas kernels for 0% -> 9%
where the time goes in v1:
time: 159 us
  waiting for transfers between devices  63.9 us (40%)
  starting transfers between devices  32.3 us (20%)
  local copies, waits for them, and re-layouts  21.9 us (14%)
  Pallas kernels  16.5 us (10%)
  matrix products  13.8 us (9%)
  other arithmetic  9.31 us (6%)
    all_to_all x1, waiting for transfers between devices, shards(): lax.all_to_all(outgoing.reshape(experts, capacity, cols), 'ep', split_axi...  17.1 us
    all_to_all x1, waiting for transfers between devices, shards(): lax.all_to_all(summed.reshape(experts, capacity, cols), 'ep', split_axis=...  16 us
    ppermute x6, waiting for transfers between devices, swap(): return lax.ppermute(x, axis, [(i, i ^ mask) for i in range(count)])  15.3 us
    pallas_call x1, Pallas kernels, ffn(): pl.pallas_call(ffn_kernel, grid_spec=pltpu.PrefetchScalarGridSpec(num_sca...  13.8 us
    unnamed x38, local copies, waits for them, and re-layouts  12.6 us
    all_to_all x1, starting transfers between devices, shards(): lax.all_to_all(summed.reshape(experts, capacity, cols), 'ep', split_axis=...  10.2 us
    all_to_all x1, waiting for transfers between devices, shards(): lax.all_to_all(share.reshape(lax.axis_size('tp'), -1, share.shape[1]), 't...  8.22 us
    sub x1, matrix products, attention(): weights = jnp.where(allowed, jnp.exp(scores - row_max[..., None]), 0.0)  7.5 us
  transfers between devices with their start and end apart: 12, of which 7 were waited for; matrix products, arithmetic and copies ran while one was open for 22% of the time, Pallas kernels for 9%

profile of v1, /device:TPU:0, one launch (start us, length us, event | category | flops | bytes accessed | tf_op | source)
XLA Modules:
  0.0 158.5 jit_solution(4997063954357629849)
XLA Ops:
  0.7 2.7 %dispatch.1 = bf16[640,512]{1,0:T(8,128)(2,1)} custom-call(s32[1]{0:T(128)} %bitcast.place_ref, s32[2,192]{1,0:T(2,128)} %bitcast.88, bf16[192,2048]{1,0:T(8,128)(2,1)} %rows_ref.1, f32[1,2048]{1,0:T(1,128)} %bitcast.87), custom_call_target="tpu_custom_call" | custom-call | flops 125829120 | bytes 786432 | tf_op jit(solution)/shard_map/dispatch/pallas_call | solution.py:111
  3.3 7.4 %all-to-all-start = ((bf16[8,80,512]{2,1,0:T(8,128)(2,1)}), bf16[8,80,512]{2,1,0:T(8,128)(2,1)S(1)}, u32[]{:S(2)}, u32[]{:S(2)}) async-start(bf16[8,80,512]{2,1,0:T(8,128)(2,1)} %bitcast.74), calls=%async_computation | async-start | bytes 1310720 | tf_op jit(solution)/shard_map/all_to_all | solution.py:244
  10.9 17.1 %all-to-all-done = bf16[8,80,512]{2,1,0:T(8,128)(2,1)S(1)} async-done(((bf16[8,80,512]{2,1,0:T(8,128)(2,1)}), bf16[8,80,512]{2,1,0:T(8,128)(2,1)S(1)}, u32[]{:S(2)}, u32[]{:S(2)}) %all-to-all-start) | async-done | bytes 655392 | tf_op jit(solution)/shard_map/all_to_all | solution.py:244
  30.9 3.1 %collective-permute-start.2 = (bf16[256,512]{1,0:T(8,128)(2,1)S(1)}, bf16[256,512]{1,0:T(8,128)(2,1)S(1)}, u32[]{:S(2)}, u32[]{:S(2)}) collective-permute-start(bf16[256,512]{1,0:T(8,128)(2,1)S(1)} %get-tuple-element.12), channel_id=1, source_target_pairs={{0,24},{4,28},{1,25},{5,29},{2,26},{6,30},{3,27},{7,31}} | collective-permute-start | bytes 786440 | tf_op jit(solution)/shard_map/ppermute | solution.py:22
  35.3 2.5 %collective-permute-start = (bf16[256,512]{1,0:T(8,128)(2,1)S(1)}, bf16[256,512]{1,0:T(8,128)(2,1)S(1)}, u32[]{:S(2)}, u32[]{:S(2)}) collective-permute-start(bf16[256,512]{1,0:T(8,128)(2,1)S(1)} %get-tuple-element.12), channel_id=1, source_target_pairs={{0,8},{4,12},{8,16},{12,20},{16,24},{20,28},{1,9},{5,13},{9,17},{1... | collective-permute-start | bytes 786440 | tf_op jit(solution)/shard_map/ppermute | solution.py:22
  37.8 2.3 %compare_and_fusion = pred[256,2048]{0,1:T(8,128)(4,1)} fusion(s32[256]{0:T(256)S(1)} %iota_add_fusion, s32[2048]{0:T(1024)S(1)} %bitcast.80, pred[2048]{0:T(1024)(128)(4,1)S(1)} %broadcast_compare_fusion), kind=kLoop, calls=%fused_computation.11 | loop fusion | flops 1048576 | bytes 535552 | tf_op jit(solution)/shard_map/and | solution.py:60
  40.2 2.9 %collective-permute-done.5.x2 = bf16[640,512]{1,0:T(8,128)(2,1)S(1)} collective-permute-done((bf16[640,512]{1,0:T(8,128)(2,1)S(1)}, bf16[640,512]{1,0:T(8,128)(2,1)S(1)}, u32[]{:S(2)}, u32[]{:S(2)}) %collective-permute-start.5) | collective-permute-done | bytes 655392 | tf_op jit(solution)/shard_map/ppermute | solution.py:17
  43.1 3.3 %collective-permute-done.1 = bf16[256,512]{1,0:T(8,128)(2,1)S(1)} collective-permute-done((bf16[256,512]{1,0:T(8,128)(2,1)S(1)}, bf16[256,512]{1,0:T(8,128)(2,1)S(1)}, u32[]{:S(2)}, u32[]{:S(2)}) %collective-permute-start.1) | collective-permute-done | bytes 262176 | tf_op jit(solution)/shard_map/ppermute | solution.py:22
  46.4 3.9 %collective-permute-done = bf16[256,512]{1,0:T(8,128)(2,1)S(1)} collective-permute-done((bf16[256,512]{1,0:T(8,128)(2,1)S(1)}, bf16[256,512]{1,0:T(8,128)(2,1)S(1)}, u32[]{:S(2)}, u32[]{:S(2)}) %collective-permute-start) | collective-permute-done | bytes 262176 | tf_op jit(solution)/shard_map/ppermute | solution.py:22
  51.4 2.2 %collective-permute-start.3 = (bf16[1024,512]{1,0:T(8,128)(2,1)}, bf16[1024,512]{1,0:T(8,128)(2,1)}, u32[]{:S(2)}, u32[]{:S(2)}) collective-permute-start(bf16[1024,512]{1,0:T(8,128)(2,1)} %pad_maximum_fusion), channel_id=1, source_target_pairs={{0,4},{4,0},{8,12},{12,8},{16,20},{20,16},{24,28},{28,24},{1,5},{5... | collective-permute-start | bytes 3145736 | tf_op jit(solution)/shard_map/ppermute | solution.py:17
  59.2 2.0 %copy-done.1 = bf16[1,2048,896]{2,1,0:T(8,128)(2,1)S(1)} copy-done((bf16[1,2048,896]{2,1,0:T(8,128)(2,1)S(1)}, bf16[1,2048,896]{2,1,0:T(8,128)(2,1)}, u32[]{:S(2)}) %copy-start.1) | copy-done | bytes 3670040
  65.5 13.8 %ffn.1 = (bf16[640,1024]{1,0:T(8,128)(2,1)S(1)}, bf16[640,1024]{1,0:T(8,128)(2,1)}) custom-call(s32[8]{0:T(128)S(1)} %broadcast_xor_fusion.order_ref, bf16[640,512]{1,0:T(8,128)(2,1)S(1)} %bitcast.71, bf16[640,512]{1,0:T(8,128)(2,1)S(1)} %copy-done.6, bf16[640,512]{1,0:T(8,128)(2,1)S(1)} %copy-done.4, bf16[640,512]{1,0:T(8,128)(2,1)} %collective-permute-done.6.x3, ...), custom_call_target="tpu_custom_call" | custom-call | flops 7046430720 | bytes 21495808 | tf_op jit(solution)/shard_map/ffn/pallas_call | solution.py:170
  79.3 2.2 %constant_dynamic-update-slice_fusion.2 = bf16[2048,512]{1,0:T(8,128)(2,1)} fusion(bf16[2048,512]{1,0:T(8,128)(2,1)} %constant_dynamic-update-slice_fusion.3, bf16[1024,512]{1,0:T(8,128)(2,1)} %collective-permute-done.3), kind=kLoop, calls=%fused_computation.39 | loop fusion | bytes 2097152 | tf_op jit(solution)/shard_map/concatenate | solution.py:38
  81.5 2.7 %fusion.37 = (bf16[2048,256]{1,0:T(8,128)(2,1)}, bf16[2048,256]{1,0:T(8,128)(2,1)S(1)}) fusion(bf16[2048,512]{1,0:T(8,128)(2,1)} %constant_dynamic-update-slice_fusion.2), kind=kLoop, calls=%fused_computation.64 | loop fusion | bytes 4194304 | tf_op jit(solution)/shard_map/slice | solution.py:54
  84.2 2.3 %copy.21 = bf16[2048,256]{0,1:T(8,128)(2,1)} copy(bf16[2048,256]{1,0:T(8,128)(2,1)} %get-tuple-element.10) | data formatting | bytes 2097152 | tf_op jit(solution)/shard_map/slice | solution.py:54
  86.5 7.5 %fusion.40 = (f32[2,2,256]{2,1,0:T(2,128)S(1)}, bf16[2,2,256,2048]{2,3,1,0:T(8,128)(2,1)}) fusion(bf16[2048,2,2,64]{0,3,2,1:T(8,128)(2,1)} %bitcast.75, bf16[256,2,2,64]{0,3,2,1:T(8,128)(2,1)S(1)} %bitcast.78, pred[256,2048]{0,1:T(8,128)(4,1)} %compare_and_fusion), kind=kOutput, calls=%fused_computation.67 | convolution fusion | flops 281020416 | bytes 5902336 | tf_op jit(solution)/shard_map/sub | solution.py:63
  95.4 3.2 %fusion.9 = f32[2,2,256,128]{2,3,1,0:T(8,128)S(1)} fusion(bf16[2048,2,128,1]{0,2,3,1:T(8,128)(2,1)} %bitcast.76, bf16[2,2,256,2048]{2,3,1,0:T(8,128)(2,1)} %get-tuple-element.21, f32[2,2,256]{2,1,0:T(2,128)S(1)} %get-tuple-element.20), kind=kOutput, calls=%fused_computation.14 | convolution fusion | flops 537001984 | bytes 5771264 | tf_op jit(solution)/shard_map/hmqk,khd->hmqd/dot_general | solution.py:65
  98.9 2.1 %add_convert_fusion.1 = bf16[640,512]{1,0:T(8,128)(2,1)} fusion(bf16[640,1024]{1,0:T(8,128)(2,1)} %collective-permute-done.7, bf16[640,1024]{1,0:T(8,128)(2,1)S(1)} %get-tuple-element.8), kind=kLoop, calls=%fused_computation.13 | loop fusion | flops 1310720 | bytes 1966080 | tf_op jit(solution)/shard_map/convert_element_type | solution.py:262
  103.1 3.5 %all-to-all-start.1 = ((bf16[4,64,2048]{2,1,0:T(8,128)(2,1)}), bf16[4,64,2048]{2,1,0:T(8,128)(2,1)S(1)}, u32[]{:S(2)}, u32[]{:S(2)}) async-start(bf16[4,64,2048]{2,1,0:T(8,128)(2,1)} %bitcast.72), calls=%async_computation.1 | async-start | bytes 2097152 | tf_op jit(solution)/shard_map/all_to_all | solution.py:254
  106.6 12.4 %collective-permute-done.8 = bf16[640,512]{1,0:T(8,128)(2,1)} collective-permute-done((bf16[640,512]{1,0:T(8,128)(2,1)}, bf16[640,512]{1,0:T(8,128)(2,1)}, u32[]{:S(2)}, u32[]{:S(2)}) %collective-permute-start.8) | collective-permute-done | bytes 655392 | tf_op jit(solution)/shard_map/ppermute | solution.py:17
  119.0 2.4 %add_convert_fusion = bf16[640,512]{1,0:T(8,128)(2,1)} fusion(bf16[640,512]{1,0:T(8,128)(2,1)} %collective-permute-done.8, bf16[640,1024]{1,0:T(8,128)(2,1)} %collective-permute-done.7, bf16[640,1024]{1,0:T(8,128)(2,1)S(1)} %get-tuple-element.8), kind=kLoop, calls=%fused_computation.12 | loop fusion | flops 1966080 | bytes 2621440 | tf_op jit(solution)/shard_map/convert_element_type | solution.py:265
  121.4 8.2 %all-to-all-done.1 = bf16[4,64,2048]{2,1,0:T(8,128)(2,1)S(1)} async-done(((bf16[4,64,2048]{2,1,0:T(8,128)(2,1)}), bf16[4,64,2048]{2,1,0:T(8,128)(2,1)S(1)}, u32[]{:S(2)}, u32[]{:S(2)}) %all-to-all-start.1) | async-done | bytes 1048608 | tf_op jit(solution)/shard_map/all_to_all | solution.py:254
  129.7 10.2 %all-to-all-start.2 = ((bf16[8,80,512]{2,1,0:T(8,128)(2,1)}), bf16[8,80,512]{2,1,0:T(8,128)(2,1)S(1)}, u32[]{:S(2)}, u32[]{:S(2)}) async-start(bf16[8,80,512]{2,1,0:T(8,128)(2,1)} %bitcast.73), calls=%async_computation.2 | async-start | bytes 1310720 | tf_op jit(solution)/shard_map/all_to_all | solution.py:266
  141.0 16.0 %all-to-all-done.2 = bf16[8,80,512]{2,1,0:T(8,128)(2,1)S(1)} async-done(((bf16[8,80,512]{2,1,0:T(8,128)(2,1)}), bf16[8,80,512]{2,1,0:T(8,128)(2,1)S(1)}, u32[]{:S(2)}, u32[]{:S(2)}) %all-to-all-start.2) | async-done | bytes 655392 | tf_op jit(solution)/shard_map/all_to_all | solution.py:266
  (69 shorter events, 21.5 us)
Async XLA Ops:
  0.6 101.0 %copy-start = (bf16[256,2048]{1,0:T(8,128)(2,1)S(1)}, bf16[256,2048]{1,0:T(8,128)(2,1)}, u32[]{:S(2)}) copy-start(bf16[256,2048]{1,0:T(8,128)(2,1)} %param.19) | copy-start | bytes 3145732
  0.6 29.6 %copy-start.9 = (bf16[256,256]{1,0:T(8,128)(2,1)S(1)}, bf16[256,256]{1,0:T(8,128)(2,1)}, u32[]{:S(2)}) copy-start(bf16[256,256]{1,0:T(8,128)(2,1)} %param.16) | copy-start | bytes 393220
  0.7 28.9 %copy-start.8 = (bf16[256,256]{1,0:T(8,128)(2,1)S(1)}, bf16[256,256]{1,0:T(8,128)(2,1)}, u32[]{:S(2)}) copy-start(bf16[256,256]{1,0:T(8,128)(2,1)} %param.15) | copy-start | bytes 393220
  3.3 50.2 %copy-start.15 = (s32[8]{0:T(128)S(1)}, s32[8]{0:T(128)}, u32[]{:S(2)}) copy-start(s32[8]{0:T(128)} %constant.39.clone) | copy-start | bytes 100
  3.3 24.7 %all-to-all-start = ((bf16[8,80,512]{2,1,0:T(8,128)(2,1)}), bf16[8,80,512]{2,1,0:T(8,128)(2,1)S(1)}, u32[]{:S(2)}, u32[]{:S(2)}) async-start(bf16[8,80,512]{2,1,0:T(8,128)(2,1)} %bitcast.74), calls=%async_computation | async-start | bytes 1310720 | tf_op jit(solution)/shard_map/all_to_all | solution.py:244
  28.1 15.0 %collective-permute-start.5 = (bf16[640,512]{1,0:T(8,128)(2,1)S(1)}, bf16[640,512]{1,0:T(8,128)(2,1)S(1)}, u32[]{:S(2)}, u32[]{:S(2)}) collective-permute-start(bf16[640,512]{1,0:T(8,128)(2,1)S(1)} %bitcast.69), channel_id=1, source_target_pairs={{0,2},{1,3},{2,0},{3,1},{4,6},{5,7},{6,4},{7,5},{8,10},{9,11},{10,... | collective-permute-start | bytes 1966088 | tf_op jit(solution)/shard_map/ppermute | solution.py:17
  30.9 12.2 %collective-permute-start.2 = (bf16[256,512]{1,0:T(8,128)(2,1)S(1)}, bf16[256,512]{1,0:T(8,128)(2,1)S(1)}, u32[]{:S(2)}, u32[]{:S(2)}) collective-permute-start(bf16[256,512]{1,0:T(8,128)(2,1)S(1)} %get-tuple-element.12), channel_id=1, source_target_pairs={{0,24},{4,28},{1,25},{5,29},{2,26},{6,30},{3,27},{7,31}} | collective-permute-start | bytes 786440 | tf_op jit(solution)/shard_map/ppermute | solution.py:22
  34.0 12.4 %collective-permute-start.1 = (bf16[256,512]{1,0:T(8,128)(2,1)S(1)}, bf16[256,512]{1,0:T(8,128)(2,1)S(1)}, u32[]{:S(2)}, u32[]{:S(2)}) collective-permute-start(bf16[256,512]{1,0:T(8,128)(2,1)S(1)} %get-tuple-element.12), channel_id=1, source_target_pairs={{0,16},{4,20},{8,24},{12,28},{1,17},{5,21},{9,25},{13,29},{2,18},{... | collective-permute-start | bytes 786440 | tf_op jit(solution)/shard_map/ppermute | solution.py:22
  35.3 15.0 %collective-permute-start = (bf16[256,512]{1,0:T(8,128)(2,1)S(1)}, bf16[256,512]{1,0:T(8,128)(2,1)S(1)}, u32[]{:S(2)}, u32[]{:S(2)}) collective-permute-start(bf16[256,512]{1,0:T(8,128)(2,1)S(1)} %get-tuple-element.12), channel_id=1, source_target_pairs={{0,8},{4,12},{8,16},{12,20},{16,24},{20,28},{1,9},{5,13},{9,17},{1... | collective-permute-start | bytes 786440 | tf_op jit(solution)/shard_map/ppermute | solution.py:22
  40.2 18.2 %collective-permute-start.4 = (bf16[640,512]{1,0:T(8,128)(2,1)S(1)}, bf16[640,512]{1,0:T(8,128)(2,1)S(1)}, u32[]{:S(2)}, u32[]{:S(2)}) collective-permute-start(bf16[640,512]{1,0:T(8,128)(2,1)S(1)} %bitcast.70), channel_id=1, source_target_pairs={{0,1},{1,0},{2,3},{3,2},{4,5},{5,4},{6,7},{7,6},{8,9},{9,8},{10,11... | collective-permute-start | bytes 1966088 | tf_op jit(solution)/shard_map/ppermute | solution.py:17
  43.1 15.3 %copy-start.3 = (bf16[640,512]{1,0:T(8,128)(2,1)}, bf16[640,512]{1,0:T(8,128)(2,1)S(1)}, u32[]{:S(2)}) copy-start(bf16[640,512]{1,0:T(8,128)(2,1)S(1)} %collective-permute-done.5.x2) | copy-start | bytes 1966084
  43.1 16.1 %collective-permute-start.6 = (bf16[640,512]{1,0:T(8,128)(2,1)S(1)}, bf16[640,512]{1,0:T(8,128)(2,1)}, u32[]{:S(2)}, u32[]{:S(2)}) collective-permute-start(bf16[640,512]{1,0:T(8,128)(2,1)S(1)} %collective-permute-done.5.x2), channel_id=1, source_target_pairs={{0,1},{1,0},{2,3},{3,2},{4,5},{5,4},{6,7},{7,6},{8,9},{9,8},{10,11... | collective-permute-start | bytes 1966088 | tf_op jit(solution)/shard_map/ppermute | solution.py:17
  51.4 27.9 %collective-permute-start.3 = (bf16[1024,512]{1,0:T(8,128)(2,1)}, bf16[1024,512]{1,0:T(8,128)(2,1)}, u32[]{:S(2)}, u32[]{:S(2)}) collective-permute-start(bf16[1024,512]{1,0:T(8,128)(2,1)} %pad_maximum_fusion), channel_id=1, source_target_pairs={{0,4},{4,0},{8,12},{12,8},{16,20},{20,16},{24,28},{28,24},{1,5},{5... | collective-permute-start | bytes 3145736 | tf_op jit(solution)/shard_map/ppermute | solution.py:17
  59.2 2.0 %copy-start.1 = (bf16[1,2048,896]{2,1,0:T(8,128)(2,1)S(1)}, bf16[1,2048,896]{2,1,0:T(8,128)(2,1)}, u32[]{:S(2)}) copy-start(bf16[1,2048,896]{2,1,0:T(8,128)(2,1)} %gate_ref.1) | copy-start | bytes 11010052
  61.3 2.0 %copy-start.2 = (bf16[1,2048,896]{2,1,0:T(8,128)(2,1)S(1)}, bf16[1,2048,896]{2,1,0:T(8,128)(2,1)}, u32[]{:S(2)}) copy-start(bf16[1,2048,896]{2,1,0:T(8,128)(2,1)} %up_ref.1) | copy-start | bytes 11010052
  79.3 19.7 %collective-permute-start.7 = (bf16[640,1024]{1,0:T(8,128)(2,1)}, bf16[640,1024]{1,0:T(8,128)(2,1)}, u32[]{:S(2)}, u32[]{:S(2)}) collective-permute-start(bf16[640,1024]{1,0:T(8,128)(2,1)} %get-tuple-element.9), channel_id=1, source_target_pairs={{0,1},{1,0},{2,3},{3,2},{4,5},{5,4},{6,7},{7,6},{8,9},{9,8},{10,11... | collective-permute-start | bytes 3932168 | tf_op jit(solution)/shard_map/ppermute | solution.py:17
  84.2 2.3 %copy-start.10 = (bf16[256,256]{0,1:T(8,128)(2,1)S(1)}, bf16[256,256]{0,1:T(8,128)(2,1)}, u32[]{:S(2)}) copy-start(bf16[256,256]{0,1:T(8,128)(2,1)} %copy.22) | copy-start | bytes 393220
  95.4 3.3 %copy-start.12 = (f32[2]{0:T(128)S(1)}, f32[2]{0:T(128)}, u32[]{:S(2)}) copy-start(f32[2]{0:T(128)} %param.17) | copy-start | bytes 28
  95.4 3.4 %copy-start.14 = (f32[128]{0:T(128)S(1)}, f32[128]{0:T(128)}, u32[]{:S(2)}) copy-start(f32[128]{0:T(128)} %param.18) | copy-start | bytes 1540
  101.1 17.9 %collective-permute-start.8 = (bf16[640,512]{1,0:T(8,128)(2,1)}, bf16[640,512]{1,0:T(8,128)(2,1)}, u32[]{:S(2)}, u32[]{:S(2)}) collective-permute-start(bf16[640,512]{1,0:T(8,128)(2,1)} %add_convert_fusion.1), channel_id=1, source_target_pairs={{0,2},{1,3},{2,0},{3,1},{4,6},{5,7},{6,4},{7,5},{8,10},{9,11},{10,... | collective-permute-start | bytes 1966088 | tf_op jit(solution)/shard_map/ppermute | solution.py:17
  103.1 26.6 %all-to-all-start.1 = ((bf16[4,64,2048]{2,1,0:T(8,128)(2,1)}), bf16[4,64,2048]{2,1,0:T(8,128)(2,1)S(1)}, u32[]{:S(2)}, u32[]{:S(2)}) async-start(bf16[4,64,2048]{2,1,0:T(8,128)(2,1)} %bitcast.72), calls=%async_computation.1 | async-start | bytes 2097152 | tf_op jit(solution)/shard_map/all_to_all | solution.py:254
  106.6 33.3 %copy-start.11 = (s32[192,2]{0,1:T(2,128)S(1)}, s32[192,2]{0,1:T(2,128)}, u32[]{:S(2)}) copy-start(s32[192,2]{0,1:T(2,128)} %param.22) | copy-start | bytes 4612
  106.6 33.3 %copy-start.13 = (f32[192,2]{0,1:T(2,128)S(1)}, f32[192,2]{0,1:T(2,128)}, u32[]{:S(2)}) copy-start(f32[192,2]{0,1:T(2,128)} %param.23) | copy-start | bytes 4612
  129.7 27.4 %all-to-all-start.2 = ((bf16[8,80,512]{2,1,0:T(8,128)(2,1)}), bf16[8,80,512]{2,1,0:T(8,128)(2,1)S(1)}, u32[]{:S(2)}, u32[]{:S(2)}) async-start(bf16[8,80,512]{2,1,0:T(8,128)(2,1)} %bitcast.73), calls=%async_computation.2 | async-start | bytes 1310720 | tf_op jit(solution)/shard_map/all_to_all | solution.py:266
  (4 other events, 4.1 us)

commit v2 on v1

--- a/solution.py
+++ b/solution.py
@@ -23,19 +23,10 @@
 
 
 def gathered_keys(key_rows, value_rows):
-    rows_here, width = key_rows.shape
     count = lax.axis_size("ep")
     own = jnp.concatenate([key_rows, value_rows], axis=1)
-    here = lax.axis_index("ep")
-    if count > 8 or count % 2:
-        both = lax.all_gather(own, "ep", axis=0, tiled=True)
-        return both, jnp.arange(count, dtype=jnp.int32)
-    pieces = [own] + [later(own, "ep", 2 * k) for k in range(1, count // 2)]
-    line = jnp.concatenate(pieces, axis=0)
-    other = swap(line, "ep", 1)
-    steps = 2 * jnp.arange(count // 2, dtype=jnp.int32)
-    places = jnp.concatenate([here - steps, (here ^ 1) - steps])
-    return jnp.concatenate([line, other], axis=0), places
+    both = lax.all_gather(own, "ep", axis=0, tiled=True)
+    return both, jnp.arange(count, dtype=jnp.int32)
 
 
 def attention(queries, both, places, head_lambda, sub_gain, out_weight):
@@ -74,10 +65,123 @@
     return jnp.dot(attended, out_weight, preferred_element_type=F32).astype(BF16)
 
 
+VMEM = pl.BlockSpec(memory_space=pltpu.VMEM)
+SMEM = pl.BlockSpec(memory_space=pltpu.SMEM)
+
+
+def half(index, size):
+    return pl.ds(pl.multiple_of(index * size, size), size)
+
+
+def pick_kernel(place_ref, query_ref, key_ref, value_ref, out_ref):
+    other = 1 - (place_ref[0] & 1)
+    at = 0
+    for ref in (query_ref, key_ref, value_ref):
+        wide = ref.shape[1] // 2
+        out_ref[:, at : at + wide] = ref[:, half(other, wide)]
+        at += wide
+
+
+def merge_kernel(place_ref, query_ref, key_ref, value_ref, got_ref, query_out, block_out):
+    mine = place_ref[0] & 1
+    rows = query_ref.shape[0]
+    pair, deep = key_ref.shape[1] // 2, value_ref.shape[1] // 2
+    own, other = half(mine, rows), half(1 - mine, rows)
+    query_out[own, :] = query_ref[:, half(mine, pair)]
+    query_out[other, :] = got_ref[:, :pair]
+    block_out[own, :pair] = key_ref[:, half(mine, pair)]
+    block_out[own, pair:] = value_ref[:, half(mine, deep)]
+    block_out[other, :] = got_ref[:, pair:]
+
+
+def attention_kernel(head_width, place_ref, lambda_ref, query_ref, own_ref, *rest):
+    lines = rest[:-4]
+    gain_ref, keep_ref, send_ref, attended = rest[-4:]
+    rows = query_ref.shape[0] // 2
+    pair = 2 * head_width
+    mine, line_place = place_ref[0] & 1, place_ref[0] >> 1
+    causal = lax.broadcasted_iota(jnp.int32, (rows, rows), 0) >= lax.broadcasted_iota(
+        jnp.int32, (rows, rows), 1
+    )
+    lane = lax.broadcasted_iota(jnp.int32, (rows, pair), 1)
+    scaling = head_width ** (-0.5)
+    lam = lambda_ref[mine]
+    for side in range(2):
+        query = query_ref[side * rows : (side + 1) * rows, :].astype(F32)
+        pieces = [(own_ref, side * rows, rows, None)]
+        if side:
+            pieces.append((own_ref, 0, rows, 0.0))
+        for k, ref in enumerate(lines):
+            bias = jnp.where(line_place >= k + 1, 0.0, -1e30).astype(F32)
+            pieces += [(ref, 0, rows, bias), (ref, rows, rows, bias)]
+        per_map = []
+        for m in range(2):
+            one = jnp.where(lane // head_width == m, query, 0.0).astype(BF16)
+            scores = []
+            for ref, first, count, bias in pieces:
+                s = scaling * lax.dot_general(
+                    one,
+                    ref[first : first + count, :pair],
+                    (((1,), (1,)), ((), ())),
+                    preferred_element_type=F32,
+                )
+                scores.append(jnp.where(causal, s, -1e30) if bias is None else s + bias)
+            top = jnp.max(functools.reduce(jnp.maximum, scores), axis=-1, keepdims=True)
+            weights = [jnp.exp(s - top) for s in scores]
+            row_sum = jnp.sum(functools.reduce(jnp.add, weights), axis=-1, keepdims=True)
+            numerator = functools.reduce(
+                jnp.add,
+                [
+                    jnp.dot(
+                        w.astype(BF16),
+                        ref[first : first + count, pair:],
+                        preferred_element_type=F32,
+                    )
+                    for w, (ref, first, count, _) in zip(weights, pieces)
+                ],
+            )
+            per_map.append(numerator / row_sum)
+        contrast = per_map[0] - lam * per_map[1]
+        square = jnp.mean(contrast * contrast, axis=-1, keepdims=True)
+        attended[side * rows : (side + 1) * rows, :] = (
+            contrast * lax.rsqrt(square + EPS) * gain_ref[...]
+        ).astype(BF16)
+    keep_ref[...] = attended[half(mine, rows), :]
+    send_ref[...] = attended[half(1 - mine, rows), :]
+
+
+def project_kernel(place_ref, own_ref, got_ref, weight_ref, keep_ref, send_ref, attended):
+    mine, place = place_ref[0] & 1, place_ref[1]
+    rows, deep = own_ref.shape
+    attended[:, half(mine, deep)] = own_ref[...]
+    attended[:, half(1 - mine, deep)] = got_ref[...]
+    group = rows // 4
+    for out_ref, masks in ((send_ref, (1, 3)), (keep_ref, (0, 2))):
+        picked = [attended[half(place ^ mask, group), :] for mask in masks]
+        out_ref[...] = jnp.dot(
+            jnp.concatenate(picked, axis=0), weight_ref[...], preferred_element_type=F32
+        ).astype(BF16)
+
+
+def local(kernel, outs, operands, smem=1, scratch=(), flops=1000000, limit=20):
+    size = sum(x.size for x in operands)
+    return pl.pallas_call(
+        kernel,
+        out_shape=[jax.ShapeDtypeStruct(shape, BF16) for shape in outs],
+        in_specs=[SMEM] * smem + [VMEM] * (len(operands) - smem),
+        out_specs=[VMEM] * len(outs),
+        scratch_shapes=list(scratch),
+        compiler_params=pltpu.CompilerParams(vmem_limit_bytes=limit * 1024 * 1024),
+        cost_estimate=pl.CostEstimate(
+            flops=flops, bytes_accessed=2 * size, transcendentals=0
+        ),
+    )(*operands)
+
+
 def dispatch_kernel(
     experts, capacity, place_ref, ids_ref, rows_ref, gain_ref, out_ref, onehot_ref
 ):
-    rows, width = rows_ref.shape
+    rows, _ = rows_ref.shape
     cols = out_ref.shape[1]
     first = pl.multiple_of(place_ref[0] * cols, cols)
     wide = rows_ref[...].astype(F32)
@@ -126,79 +230,121 @@
     )
 
 
+def fetch_kernel(gate, up, down, gate_w, up_w, down_w, sem):
+    copies = []
+    for n, (source, target) in enumerate(((gate, gate_w), (up, up_w), (down, down_w))):
+        part = target.shape[0] // 4
+        for k in range(4):
+            rows = slice(k * part, (k + 1) * part)
+            copies.append(
+                pltpu.make_async_copy(source.at[0, rows, :], target.at[rows, :], sem.at[4 * n + k])
+            )
+    for copy in copies:
+        copy.start()
+    for copy in copies:
+        copy.wait()
+
+
+def fetched(*weights):
+    hbm = pl.BlockSpec(memory_space=pltpu.HBM)
+    vmem = pl.BlockSpec(memory_space=pltpu.VMEM)
+    return pl.pallas_call(
+        fetch_kernel,
+        in_specs=[hbm] * 3,
+        out_specs=[vmem] * 3,
+        out_shape=[pltpu.VMEM(w.shape[1:], w.dtype) for w in weights],
+        scratch_shapes=[pltpu.SemaphoreType.DMA((12,))],
+        compiler_params=pltpu.CompilerParams(vmem_limit_bytes=24 * 1024 * 1024),
+        cost_estimate=pl.CostEstimate(
+            flops=sum(w.size for w in weights) * 100,
+            bytes_accessed=sum(w.size for w in weights) * 2,
+            transcendentals=0,
+        ),
+        name="fetch",
+    )(*(pltpu.with_memory_space_constraint(w, pltpu.HBM) for w in weights))
+
+
 def ffn_kernel(
-    order_ref, x0, x1, x2, x3, gate_ref, up_ref, down_ref, keep_ref, send_ref, acc_g, acc_u, hidden
+    first, order_ref, own, near, far, cross, gate_w, up_w, down_w, keep_ref, send_ref
 ):
-    step = pl.program_id(0)
-    for k, x_ref in enumerate((x0, x1, x2, x3)):
-
-        @pl.when(step == k)
-        def _(k=k, x_ref=x_ref):
-            gate = jnp.dot(x_ref[...], gate_ref[0], preferred_element_type=F32)
-            up = jnp.dot(x_ref[...], up_ref[0], preferred_element_type=F32)
-            if k:
-                gate += acc_g[...]
-                up += acc_u[...]
-            if k < 3:
-                acc_g[...] = gate
-                acc_u[...] = up
-            else:
-                hidden[...] = (gate / (1.0 + jnp.exp(-gate)) * up).astype(BF16)
-
-    @pl.when((step == 4) | (step == 5))
-    def _():
-        send_ref[...] = jnp.dot(hidden[...], down_ref[0], preferred_element_type=F32).astype(BF16)
-
-    @pl.when(step >= 6)
-    def _():
-        keep_ref[...] = jnp.dot(hidden[...], down_ref[0], preferred_element_type=F32).astype(BF16)
-
-
-def ffn(order, pieces, gate_weight, up_weight, down_weight):
-    rows, cols = pieces[0].shape
-    width, units = gate_weight.shape[1:]
-
-    def clamp(i, low, high):
-        return jnp.minimum(jnp.maximum(i, low), high)
-
-    def whole():
-        return pl.BlockSpec((rows, cols), lambda i, order: (0, 0))
-
-    def weight_in():
-        return pl.BlockSpec((1, cols, units), lambda i, order: (0, order[clamp(i, 0, 3)], 0))
-
+    rows, cols = far.shape
+    pieces = (own[first : first + rows, :], near[first : first + rows, :], far[...], cross[...])
+
+    def part(k):
+        return pl.ds(pl.multiple_of(order_ref[k] * cols, cols), cols)
+
+    def product(weight_w):
+        return functools.reduce(
+            jnp.add,
+            [
+                jnp.dot(piece, weight_w[part(k), :], preferred_element_type=F32)
+                for k, piece in enumerate(pieces)
+            ],
+        )
+
+    gate_act = product(gate_w)
+    up_act = product(up_w)
+    hidden = (gate_act / (1.0 + jnp.exp(-gate_act)) * up_act).astype(BF16)
+    for n, out_ref in enumerate((send_ref, keep_ref)):
+        for k in range(2):
+            out_ref[:, k * cols : (k + 1) * cols] = jnp.dot(
+                hidden, down_w[:, part(4 + 2 * n + k)], preferred_element_type=F32
+            ).astype(BF16)
+
+
+def ffn(order, first, own, near, far, cross, weights):
+    rows, cols = far.shape
+    width, units = weights[0].shape
+    vmem = pl.BlockSpec(memory_space=pltpu.VMEM)
     return pl.pallas_call(
-        ffn_kernel,
-        grid_spec=pltpu.PrefetchScalarGridSpec(
-            num_scalar_prefetch=1,
-            grid=(8,),
-            in_specs=[whole(), whole(), whole(), whole(), weight_in(), weight_in()]
-            + [
-                pl.BlockSpec(
-                    (1, units, cols), lambda i, order: (0, 0, order[4 + clamp(i - 4, 0, 3)])
-                )
-            ],
-            out_specs=[
-                pl.BlockSpec((rows, cols), lambda i, order: (0, clamp(i - 6, 0, 1))),
-                pl.BlockSpec((rows, cols), lambda i, order: (0, clamp(i - 4, 0, 1))),
-            ],
-            scratch_shapes=[
-                pltpu.VMEM((rows, units), F32),
-                pltpu.VMEM((rows, units), F32),
-                pltpu.VMEM((rows, units), BF16),
-            ],
-        ),
+        functools.partial(ffn_kernel, first),
+        in_specs=[pl.BlockSpec(memory_space=pltpu.SMEM)] + [vmem] * 7,
+        out_specs=[vmem, vmem],
         out_shape=[jax.ShapeDtypeStruct((rows, 2 * cols), BF16)] * 2,
-        compiler_params=pltpu.CompilerParams(
-            dimension_semantics=("arbitrary",), vmem_limit_bytes=40 * 1024 * 1024
-        ),
+        compiler_params=pltpu.CompilerParams(vmem_limit_bytes=30 * 1024 * 1024),
         cost_estimate=pl.CostEstimate(
             flops=6 * rows * width * units,
-            bytes_accessed=6 * width * units + 8 * rows * width,
+            bytes_accessed=6 * width * units + 4 * rows * width,
             transcendentals=rows * units,
         ),
         name="ffn",
-    )(order, *pieces, gate_weight, up_weight, down_weight)
+    )(
+        order,
+        own,
+        near,
+        far,
+        cross,
+        *(pltpu.with_memory_space_constraint(w, pltpu.VMEM) for w in weights),
+    )
+
+
+def total_kernel(*refs):
+    out_ref = refs[-1]
+    rows, _ = refs[2].shape
+    for i in range((len(refs) - 1) // 3):
+        keep_ref, got_ref, over_ref = refs[3 * i : 3 * i + 3]
+        out_ref[i * rows : (i + 1) * rows, :] = (
+            keep_ref[...].astype(F32)
+            + got_ref[...].astype(F32)
+            + over_ref[...].astype(F32)
+        ).astype(BF16)
+
+
+def total(mine, gots):
+    rows, cols = gots[0].shape
+    operands = [x for (keep, got), over in zip(mine, gots) for x in (keep, got, over)]
+    first = pl.BlockSpec((rows, cols), lambda i: (0, 0))
+    return pl.pallas_call(
+        total_kernel,
+        out_shape=jax.ShapeDtypeStruct((len(gots) * rows, cols), BF16),
+        grid=(1,),
+        in_specs=[first] * len(operands),
+        out_specs=pl.BlockSpec((len(gots) * rows, cols), lambda i: (0, 0)),
+        cost_estimate=pl.CostEstimate(
+            flops=4 * rows * cols, bytes_accessed=16 * rows * cols, transcendentals=0
+        ),
+        name="total",
+    )(*operands)
 
 
 def combine_weights(ids_across, weight_across, capacity):
@@ -240,29 +386,75 @@
     ids_across = route_ids.T
     weight_across = route_weight.T
 
+    weights = fetched(gate_weight, up_weight, down_weight)
     outgoing = dispatched(expert_input, norm_gain, ids_across, capacity)
     own = lax.all_to_all(
         outgoing.reshape(experts, capacity, cols), "ep", split_axis=0, concat_axis=0, tiled=True
     ).reshape(slots, cols)
-    far = swap(own, "tp", 2)
+    small = experts <= 8 and experts % 2 == 0 and head_lambda.shape[0] == 2
+    here = jnp.stack([lax.axis_index("ep"), lax.axis_index("tp")]).astype(jnp.int32)
+    if small:
+        rows_a, deep = queries.shape[0], value_rows.shape[1] // 2
+        pair = queries.shape[1] // 2
+        trio = (queries, key_rows, value_rows)
+        (picked,) = local(pick_kernel, [(rows_a, 2 * pair + deep)], (here, *trio))
+        got = swap(picked, "ep", 1)
+        query, block = local(
+            merge_kernel, [(2 * rows_a, pair), (2 * rows_a, pair + deep)], (here, *trio, got)
+        )
+        block, _ = lax.optimization_barrier((block, own))
     near = swap(own, "tp", 1)
-    near_far = swap(far, "tp", 1)
-
-    key_in, value_in, own_done = lax.optimization_barrier((key_rows, value_rows, own))
-    both, places = gathered_keys(key_in, value_in)
-    share = attention(queries, both, places, head_lambda, sub_gain, out_weight)
-    parts = lax.all_to_all(
-        share.reshape(lax.axis_size("tp"), -1, share.shape[1]), "tp", 0, 0, tiled=True
-    )
-    mixer_out = jnp.sum(parts.astype(F32), axis=0).astype(BF16)
-
+    halves = 2
+    part = slots // halves
     order = jnp.array([0, 1, 2, 3, 1, 3, 0, 2], jnp.int32) ^ place
-    keep, send = ffn(order, (own, near, far, near_far), gate_weight, up_weight, down_weight)
-    got = swap(send, "tp", 1)
-    across = (keep[:, cols:].astype(F32) + got[:, cols:].astype(F32)).astype(BF16)
-    got_across = swap(across, "tp", 2)
-    mine = keep[:, :cols].astype(F32) + got[:, :cols].astype(F32)
-    summed = (mine + got_across.astype(F32)).astype(BF16)
+    fars = [swap(own[i * part : (i + 1) * part], "tp", 2) for i in range(halves)]
+    if small:
+        blocks = [later(block, "ep", 2 * k) for k in range(1, experts // 2)]
+    mine, gots = [], []
+    for i in range(halves):
+        cross = swap(fars[i], "tp", 1)
+        keep, send = ffn(
+            order, i * part, own, near, fars[i], cross, weights
+        )
+        got = swap(send, "tp", 1)
+        across = (keep[:, cols:].astype(F32) + got[:, cols:].astype(F32)).astype(BF16)
+        gots.append(swap(across, "tp", 2))
+        mine.append((keep, got))
+    if small:
+        kept, sent = local(
+            functools.partial(attention_kernel, pair // 2),
+            [(rows_a, deep)] * 2,
+            (here, head_lambda, query, block, *blocks, sub_gain.reshape(1, -1)),
+            smem=2,
+            scratch=[pltpu.VMEM((2 * rows_a, deep), BF16)],
+            flops=16 * rows_a * rows_a * experts * pair,
+            limit=28,
+        )
+        got = swap(sent, "ep", 1)
+        model = out_weight.shape[1]
+        kept, sent = local(
+            project_kernel,
+            [(rows_a // 2, model)] * 2,
+            (here, kept, got, out_weight),
+            scratch=[pltpu.VMEM((rows_a, 2 * deep), BF16)],
+            flops=4 * rows_a * deep * model,
+        )
+        got = swap(sent, "tp", 1)
+        group = got.shape[0] // 2
+        across = (kept[group:].astype(F32) + got[group:].astype(F32)).astype(BF16)
+        last = swap(across, "tp", 2)
+        mixer_out = (
+            kept[:group].astype(F32) + got[:group].astype(F32) + last.astype(F32)
+        ).astype(BF16)
+    else:
+        key_rows, value_rows, _ = lax.optimization_barrier((key_rows, value_rows, own))
+        both, places = gathered_keys(key_rows, value_rows)
+        share = attention(queries, both, places, head_lambda, sub_gain, out_weight)
+        parts = lax.all_to_all(
+            share.reshape(lax.axis_size("tp"), -1, share.shape[1]), "tp", 0, 0, tiled=True
+        )
+        mixer_out = jnp.sum(parts.astype(F32), axis=0).astype(BF16)
+    summed = total(mine, gots)
     returned = lax.all_to_all(
         summed.reshape(experts, capacity, cols), "ep", split_axis=0, concat_axis=0, tiled=True
     ).reshape(slots, cols)
@@ -292,6 +484,7 @@
         P("ep", None, "tp"),
         P("ep", "tp", None),
     )
+
     return jax.shard_map(
         shards,
         mesh=mesh,

time: 159 us -> 127 us (0.80)
  blocking collectives: 0 us -> 24.9 us
  waiting for transfers between devices: 63.9 us -> 42.7 us
  local copies, waits for them, and re-layouts: 21.9 us -> 0.86 us
  matrix products: 13.8 us -> 1.63 us
  Pallas kernels: 16.5 us -> 25.5 us
  other arithmetic: 9.31 us -> 3.1 us
  starting transfers between devices: 32.3 us -> 27 us
    all_to_all x2 -> x0, waiting for transfers between devices: 25.3 us -> none  [the longest x1 17.1 us: shards(): lax.all_to_all(outgoing.reshape(experts, capacity, cols), 'ep', split_axi...]
    all_to_all x0 -> x1, blocking collectives: none -> 24.9 us  [shards(): lax.all_to_all(outgoing.reshape(experts, capacity, cols), 'ep', split_axi...]
    ppermute x6 -> x13, waiting for transfers between devices: 15.3 us -> 33.7 us  [swap(): return lax.ppermute(x, axis, [(i, i ^ mask) for i in range(count)])]
    unnamed x38 -> x28, local copies, waits for them, and re-layouts: 12.6 us -> 0.81 us
    all_to_all x2 -> x0, starting transfers between devices: 10.9 us -> none  [the longest x1 7.41 us: shards(): lax.all_to_all(outgoing.reshape(experts, capacity, cols), 'ep', split_axi...]
    all_to_all x1, waiting for transfers between devices: 16 us -> 6.69 us  [shards(): lax.all_to_all(summed.reshape(experts, capacity, cols), 'ep', split_axis=...]
    pallas_call x1 -> x8, Pallas kernels: 13.8 us -> 22.9 us  [the longest x2 9.7 us: ffn(): pl.pallas_call(functools.partial(ffn_kernel, first), in_specs=[pl.BlockSp...]
    sub x1 -> x0, matrix products: 7.5 us -> none  [attention(): weights = jnp.where(allowed, jnp.exp(scores - row_max[..., None]), 0.0)]
  transfers between devices with their start and end apart: 12 -> 17, of which waited for: 7 -> 8; matrix products, arithmetic and copies ran while one was open for 22% -> 3% of each run, Pallas kernels for 9% -> 18%
where the time goes in v2:
time: 127 us
  waiting for transfers between devices  42.7 us (34%)
  starting transfers between devices  27 us (21%)
  Pallas kernels  25.5 us (20%)
  blocking collectives  24.9 us (20%)
  other arithmetic  3.1 us (2%)
  matrix products  1.63 us (1%)
    ppermute x13, waiting for transfers between devices, swap(): return lax.ppermute(x, axis, [(i, i ^ mask) for i in range(count)])  33.7 us
    all_to_all x1, blocking collectives, shards(): lax.all_to_all(outgoing.reshape(experts, capacity, cols), 'ep', split_axi...  24.9 us
    all_to_all x1, starting transfers between devices, shards(): lax.all_to_all(summed.reshape(experts, capacity, cols), 'ep', split_axis=...  10.9 us
    pallas_call x2, Pallas kernels, ffn(): pl.pallas_call(functools.partial(ffn_kernel, first), in_specs=[pl.BlockSp...  9.7 us
    ppermute x13, starting transfers between devices, swap(): return lax.ppermute(x, axis, [(i, i ^ mask) for i in range(count)])  9.06 us
    ppermute x3, starting transfers between devices, later(): return lax.ppermute(x, axis, [(i, i + step) for i in range(count - step)])  7.02 us
    all_to_all x1, waiting for transfers between devices, shards(): lax.all_to_all(summed.reshape(experts, capacity, cols), 'ep', split_axis=...  6.69 us
    pallas_call x4, Pallas kernels, local(): pl.pallas_call(kernel, out_shape=[jax.ShapeDtypeStruct(shape, BF16) for s...  6.38 us
  transfers between devices with their start and end apart: 17, of which 8 were waited for; matrix products, arithmetic and copies ran while one was open for 3% of the time, Pallas kernels for 18%

profile of v2, /device:TPU:0, one launch (start us, length us, event | category | flops | bytes accessed | tf_op | source)
XLA Modules:
  0.0 126.6 jit_solution(12575662572914183718)
XLA Ops:
  0.7 2.6 %dispatch.1 = bf16[640,512]{1,0:T(8,128)(2,1)} custom-call(s32[1]{0:T(128)} %bitcast.1.place_ref, s32[2,192]{1,0:T(2,128)} %bitcast.35, bf16[192,2048]{1,0:T(8,128)(2,1)} %rows_ref.1, f32[1,2048]{1,0:T(1,128)} %bitcast.34), custom_call_target="tpu_custom_call" | custom-call | flops 125829120 | bytes 786432 | tf_op jit(solution)/shard_map/dispatch/pallas_call | solution.py:215
  3.3 24.9 %all_to_all.10 = bf16[8,80,512]{2,1,0:T(8,128)(2,1)S(1)} all-to-all(bf16[8,80,512]{2,1,0:T(8,128)(2,1)} %bitcast.24), channel_id=1, replica_groups=mesh['ep'=8,'tp'=4] {'ep'}, dimensions={0} | all-to-all | bytes 1310720 | tf_op jit(solution)/shard_map/all_to_all | solution.py:391
  28.3 1.6 %collective-permute-start.12 = (bf16[320,512]{1,0:T(8,128)(2,1)S(1)}, bf16[320,512]{1,0:T(8,128)(2,1)S(1)}, u32[]{:S(2)}, u32[]{:S(2)}) collective-permute-start(bf16[320,512]{1,0:T(8,128)(2,1)S(1)} %bitcast.27), channel_id=1, source_target_pairs={{0,2},{1,3},{2,0},{3,1},{4,6},{5,7},{6,4},{7,5},{8,10},{9,11},{10,... | collective-permute-start | bytes 983048 | tf_op jit(solution)/shard_map/ppermute | solution.py:17
  30.4 8.6 %collective-permute-done.12.far = bf16[320,512]{1,0:T(8,128)(2,1)S(1)} collective-permute-done((bf16[320,512]{1,0:T(8,128)(2,1)S(1)}, bf16[320,512]{1,0:T(8,128)(2,1)S(1)}, u32[]{:S(2)}, u32[]{:S(2)}) %collective-permute-start.12) | collective-permute-done | bytes 327712 | tf_op jit(solution)/shard_map/ppermute | solution.py:17
  40.8 4.2 %fetch.1 = (bf16[2048,896]{1,0:T(8,128)(2,1)S(1)}, bf16[2048,896]{1,0:T(8,128)(2,1)S(1)}, bf16[896,2048]{1,0:T(8,128)(2,1)S(1)}) custom-call(bf16[1,2048,896]{2,1,0:T(8,128)(2,1)} %gate.1, bf16[1,2048,896]{2,1,0:T(8,128)(2,1)} %up.1, bf16[1,896,2048]{2,1,0:T(8,128)(2,1)} %down.1), custom_call_target="tpu_custom_call" | custom-call | flops 550502400 | bytes 11010048 | tf_op jit(solution)/shard_map/fetch/pallas_call | solution.py:251
  45.0 1.9 %collective-permute-done.got_ref = bf16[256,384]{1,0:T(8,128)(2,1)S(1)} collective-permute-done((bf16[256,384]{1,0:T(8,128)(2,1)S(1)}, bf16[256,384]{1,0:T(8,128)(2,1)S(1)}, u32[]{:S(2)}, u32[]{:S(2)}) %collective-permute-start) | collective-permute-done | bytes 196640 | tf_op jit(solution)/shard_map/ppermute | solution.py:17
  47.6 3.2 %collective-permute-start.3 = (bf16[512,256]{1,0:T(8,128)(2,1)S(1)}, bf16[512,256]{1,0:T(8,128)(2,1)S(1)}, u32[]{:S(2)}, u32[]{:S(2)}) collective-permute-start(bf16[512,256]{1,0:T(8,128)(2,1)S(1)} %get-tuple-element.18.own_ref), channel_id=1, source_target_pairs={{0,24},{4,28},{1,25},{5,29},{2,26},{6,30},{3,27},{7,31}} | collective-permute-start | bytes 786440 | tf_op jit(solution)/shard_map/ppermute | solution.py:22
  50.8 1.3 %collective-permute-start.2 = (bf16[512,256]{1,0:T(8,128)(2,1)S(1)}, bf16[512,256]{1,0:T(8,128)(2,1)S(1)}, u32[]{:S(2)}, u32[]{:S(2)}) collective-permute-start(bf16[512,256]{1,0:T(8,128)(2,1)S(1)} %get-tuple-element.18.own_ref), channel_id=1, source_target_pairs={{0,16},{4,20},{8,24},{12,28},{1,17},{5,21},{9,25},{13,29},{2,18},{... | collective-permute-start | bytes 786440 | tf_op jit(solution)/shard_map/ppermute | solution.py:22
  52.2 2.5 %collective-permute-start.1 = (bf16[512,256]{1,0:T(8,128)(2,1)S(1)}, bf16[512,256]{1,0:T(8,128)(2,1)S(1)}, u32[]{:S(2)}, u32[]{:S(2)}) collective-permute-start(bf16[512,256]{1,0:T(8,128)(2,1)S(1)} %get-tuple-element.18.own_ref), channel_id=1, source_target_pairs={{0,8},{4,12},{8,16},{12,20},{16,24},{20,28},{1,9},{5,13},{9,17},{1... | collective-permute-start | bytes 786440 | tf_op jit(solution)/shard_map/ppermute | solution.py:22
  54.8 4.9 %ffn.3 = (bf16[320,1024]{1,0:T(8,128)(2,1)S(1)}, bf16[320,1024]{1,0:T(8,128)(2,1)S(1)}) custom-call(s32[8]{0:T(128)S(1)} %broadcast_xor_fusion.order_ref, bf16[640,512]{1,0:T(8,128)(2,1)S(1)} %bitcast.21, bf16[640,512]{1,0:T(8,128)(2,1)S(1)} %collective-permute-done.7.near, bf16[320,512]{1,0:T(8,128)(2,1)S(1)} %collective-permute-done.12.far, ...), custom_call_target="tpu_custom_call" | custom-call | flops 3523215360 | bytes 13631488 | tf_op jit(solution)/shard_map/ffn/pallas_call | solution.py:299
  60.2 4.9 %ffn.2 = (bf16[320,1024]{1,0:T(8,128)(2,1)S(1)}, bf16[320,1024]{1,0:T(8,128)(2,1)S(1)}) custom-call(s32[8]{0:T(128)S(1)} %broadcast_xor_fusion.order_ref, bf16[640,512]{1,0:T(8,128)(2,1)S(1)} %bitcast.22, bf16[640,512]{1,0:T(8,128)(2,1)S(1)} %collective-permute-done.7.near, bf16[320,512]{1,0:T(8,128)(2,1)S(1)} %collective-permute-done.8.far, ...), custom_call_target="tpu_custom_call" | custom-call | flops 3523215360 | bytes 13631488 | tf_op jit(solution)/shard_map/ffn/pallas_call | solution.py:299
  65.2 2.3 %collective-permute-done.1.rest_0_ = bf16[512,256]{1,0:T(8,128)(2,1)S(1)} collective-permute-done((bf16[512,256]{1,0:T(8,128)(2,1)S(1)}, bf16[512,256]{1,0:T(8,128)(2,1)S(1)}, u32[]{:S(2)}, u32[]{:S(2)}) %collective-permute-start.1) | collective-permute-done | bytes 262176 | tf_op jit(solution)/shard_map/ppermute | solution.py:22
  67.5 4.2 %shard_map.151 = (bf16[256,128]{1,0:T(8,128)(2,1)S(1)}, bf16[256,128]{1,0:T(8,128)(2,1)S(1)}) custom-call(s32[2]{0:T(128)S(1)} %pad_add_fusion.place_ref, f32[2]{0:T(128)S(1)} %copy-done.6, bf16[512,128]{1,0:T(8,128)(2,1)S(1)} %get-tuple-element.16.query_ref, bf16[512,256]{1,0:T(8,128)(2,1)S(1)} %get-tuple-element.18.own_ref, ...), custom_call_target="tpu_custom_call" | custom-call | flops 1073741824 | bytes 1179912 | tf_op jit(solution)/shard_map/pallas_call | solution.py:168
  73.0 3.0 %collective-permute-done.4.got_ref = bf16[256,128]{1,0:T(8,128)(2,1)S(1)} collective-permute-done((bf16[256,128]{1,0:T(8,128)(2,1)S(1)}, bf16[256,128]{1,0:T(8,128)(2,1)S(1)}, u32[]{:S(2)}, u32[]{:S(2)}) %collective-permute-start.4) | collective-permute-done | bytes 65568 | tf_op jit(solution)/shard_map/ppermute | solution.py:17
  77.3 1.6 %collective-permute-start.15 = (bf16[320,512]{1,0:T(8,128)(2,1)S(1)}, bf16[320,512]{1,0:T(8,128)(2,1)S(1)}, u32[]{:S(2)}, u32[]{:S(2)}) collective-permute-start(bf16[320,512]{1,0:T(8,128)(2,1)S(1)} %add_convert_fusion), channel_id=1, source_target_pairs={{0,2},{1,3},{2,0},{3,1},{4,6},{5,7},{6,4},{7,5},{8,10},{9,11},{10,... | collective-permute-start | bytes 983048 | tf_op jit(solution)/shard_map/ppermute | solution.py:17
  79.7 8.2 %collective-permute-done.15.refs_5_ = bf16[320,512]{1,0:T(8,128)(2,1)S(1)} collective-permute-done((bf16[320,512]{1,0:T(8,128)(2,1)S(1)}, bf16[320,512]{1,0:T(8,128)(2,1)S(1)}, u32[]{:S(2)}, u32[]{:S(2)}) %collective-permute-start.15) | collective-permute-done | bytes 327712 | tf_op jit(solution)/shard_map/ppermute | solution.py:17
  88.7 5.9 %collective-permute-done.11.refs_2_ = bf16[320,512]{1,0:T(8,128)(2,1)} collective-permute-done((bf16[320,512]{1,0:T(8,128)(2,1)S(1)}, bf16[320,512]{1,0:T(8,128)(2,1)}, u32[]{:S(2)}, u32[]{:S(2)}) %collective-permute-start.11) | collective-permute-done | bytes 327712 | tf_op jit(solution)/shard_map/ppermute | solution.py:17
  94.6 2.5 %total.1 = bf16[640,512]{1,0:T(8,128)(2,1)} custom-call(bf16[320,1024]{1,0:T(8,128)(2,1)} %copy-done.1, bf16[320,1024]{1,0:T(8,128)(2,1)} %copy-done.9, bf16[320,512]{1,0:T(8,128)(2,1)} %collective-permute-done.11.refs_2_, bf16[320,1024]{1,0:T(8,128)(2,1)} %copy-done, bf16[320,1024]{1,0:T(8,128)(2,1)} %copy-done.8, bf16[320,512]{1,0:T(8,128)(2,1)} %copy-done.10), custom_call_target="tpu_custom_call" | custom-call | flops 655360 | bytes 2621440 | tf_op jit(solution)/shard_map/total/pallas_call | solution.py:337
  97.1 10.9 %all-to-all-start.1 = ((bf16[8,80,512]{2,1,0:T(8,128)(2,1)}), bf16[8,80,512]{2,1,0:T(8,128)(2,1)S(1)}, u32[]{:S(2)}, u32[]{:S(2)}) async-start(bf16[8,80,512]{2,1,0:T(8,128)(2,1)} %bitcast.25), calls=%async_computation.1 | async-start | bytes 1310720 | tf_op jit(solution)/shard_map/all_to_all | solution.py:458
  109.0 1.6 %collective-permute-start.6 = (bf16[64,2048]{1,0:T(8,128)(2,1)S(1)}, bf16[64,2048]{1,0:T(8,128)(2,1)S(1)}, u32[]{:S(2)}, u32[]{:S(2)}) collective-permute-start(bf16[64,2048]{1,0:T(8,128)(2,1)S(1)} %add_convert_fusion.3), channel_id=1, source_target_pairs={{0,2},{1,3},{2,0},{3,1},{4,6},{5,7},{6,4},{7,5},{8,10},{9,11},{10,... | collective-permute-start | bytes 786440 | tf_op jit(solution)/shard_map/ppermute | solution.py:17
  110.6 6.0 %collective-permute-done.6 = bf16[64,2048]{1,0:T(8,128)(2,1)S(1)} collective-permute-done((bf16[64,2048]{1,0:T(8,128)(2,1)S(1)}, bf16[64,2048]{1,0:T(8,128)(2,1)S(1)}, u32[]{:S(2)}, u32[]{:S(2)}) %collective-permute-start.6) | collective-permute-done | bytes 262176 | tf_op jit(solution)/shard_map/ppermute | solution.py:17
  116.7 1.8 %add_convert_fusion.2 = bf16[64,2048]{1,0:T(8,128)(2,1)} fusion(bf16[64,2048]{1,0:T(8,128)(2,1)S(1)} %collective-permute-done.6, bf16[128,2048]{1,0:T(8,128)(2,1)} %collective-permute-done.5, bf16[128,2048]{1,0:T(8,128)(2,1)S(1)} %get-tuple-element.21), kind=kLoop, calls=%fused_computation.7 | loop fusion | flops 786432 | bytes 1048576 | tf_op jit(solution)/shard_map/convert_element_type | solution.py:448
  118.4 6.7 %all-to-all-done.1 = bf16[8,80,512]{2,1,0:T(8,128)(2,1)S(1)} async-done(((bf16[8,80,512]{2,1,0:T(8,128)(2,1)}), bf16[8,80,512]{2,1,0:T(8,128)(2,1)S(1)}, u32[]{:S(2)}, u32[]{:S(2)}) %all-to-all-start.1) | async-done | bytes 655392 | tf_op jit(solution)/shard_map/all_to_all | solution.py:458
  125.1 1.5 %fusion = bf16[192,512]{1,0:T(8,128)(2,1)} fusion(bf16[8,80,512]{2,1,0:T(8,128)(2,1)S(1)} %all-to-all-done.1, f32[8,192]{1,0:T(8,128)S(1)} %select_add_fusion, f32[8,192]{1,0:T(8,128)S(1)} %fusion.10, f32[80]{0:T(128)S(1)} %iota_convert_fusion, pred[8,192]{1,0:T(8,128)(4,1)S(1)} %fusion.14), kind=kOutput, calls=%fused_computation.1 | convolution fusion | flops 755441664 | bytes 866112 | tf_op jit(solution)/shard_map/dot_general | solution.py:461
  (62 shorter events, 8.8 us)
Async XLA Ops:
  0.6 38.4 %copy-start.5 = (bf16[256,256]{1,0:T(8,128)(2,1)S(1)}, bf16[256,256]{1,0:T(8,128)(2,1)}, u32[]{:S(2)}) copy-start(bf16[256,256]{1,0:T(8,128)(2,1)} %value_ref.3) | copy-start | bytes 393220
  0.6 38.4 %copy-start.4 = (bf16[256,256]{1,0:T(8,128)(2,1)S(1)}, bf16[256,256]{1,0:T(8,128)(2,1)}, u32[]{:S(2)}) copy-start(bf16[256,256]{1,0:T(8,128)(2,1)} %key_ref.3) | copy-start | bytes 393220
  0.7 38.3 %copy-start.3 = (bf16[256,256]{1,0:T(8,128)(2,1)S(1)}, bf16[256,256]{1,0:T(8,128)(2,1)}, u32[]{:S(2)}) copy-start(bf16[256,256]{1,0:T(8,128)(2,1)} %query_ref.3) | copy-start | bytes 393220
  28.3 10.6 %collective-permute-start.12 = (bf16[320,512]{1,0:T(8,128)(2,1)S(1)}, bf16[320,512]{1,0:T(8,128)(2,1)S(1)}, u32[]{:S(2)}, u32[]{:S(2)}) collective-permute-start(bf16[320,512]{1,0:T(8,128)(2,1)S(1)} %bitcast.27), channel_id=1, source_target_pairs={{0,2},{1,3},{2,0},{3,1},{4,6},{5,7},{6,4},{7,5},{8,10},{9,11},{10,... | collective-permute-start | bytes 983048 | tf_op jit(solution)/shard_map/ppermute | solution.py:17
  29.9 24.9 %collective-permute-start.7 = (bf16[640,512]{1,0:T(8,128)(2,1)S(1)}, bf16[640,512]{1,0:T(8,128)(2,1)S(1)}, u32[]{:S(2)}, u32[]{:S(2)}) collective-permute-start(bf16[640,512]{1,0:T(8,128)(2,1)S(1)} %bitcast.20), channel_id=1, source_target_pairs={{0,1},{1,0},{2,3},{3,2},{4,5},{5,4},{6,7},{7,6},{8,9},{9,8},{10,11... | collective-permute-start | bytes 1966088 | tf_op jit(solution)/shard_map/ppermute | solution.py:17
  29.9 22.3 %collective-permute-start.8 = (bf16[320,512]{1,0:T(8,128)(2,1)S(1)}, bf16[320,512]{1,0:T(8,128)(2,1)S(1)}, u32[]{:S(2)}, u32[]{:S(2)}) collective-permute-start(bf16[320,512]{1,0:T(8,128)(2,1)S(1)} %bitcast.26), channel_id=1, source_target_pairs={{0,2},{1,3},{2,0},{3,1},{4,6},{5,7},{6,4},{7,5},{8,10},{9,11},{10,... | collective-permute-start | bytes 983048 | tf_op jit(solution)/shard_map/ppermute | solution.py:17
  38.9 15.7 %collective-permute-start.13 = (bf16[320,512]{1,0:T(8,128)(2,1)S(1)}, bf16[320,512]{1,0:T(8,128)(2,1)S(1)}, u32[]{:S(2)}, u32[]{:S(2)}) collective-permute-start(bf16[320,512]{1,0:T(8,128)(2,1)S(1)} %collective-permute-done.12.far), channel_id=1, source_target_pairs={{0,1},{1,0},{2,3},{3,2},{4,5},{5,4},{6,7},{7,6},{8,9},{9,8},{10,11... | collective-permute-start | bytes 983048 | tf_op jit(solution)/shard_map/ppermute | solution.py:17
  39.6 7.4 %collective-permute-start = (bf16[256,384]{1,0:T(8,128)(2,1)S(1)}, bf16[256,384]{1,0:T(8,128)(2,1)S(1)}, u32[]{:S(2)}, u32[]{:S(2)}) collective-permute-start(bf16[256,384]{1,0:T(8,128)(2,1)S(1)} %shard_map.149), channel_id=1, source_target_pairs={{0,4},{4,0},{8,12},{12,8},{16,20},{20,16},{24,28},{28,24},{1,5},{5... | collective-permute-start | bytes 589832 | tf_op jit(solution)/shard_map/ppermute | solution.py:17
  47.6 17.6 %collective-permute-start.3 = (bf16[512,256]{1,0:T(8,128)(2,1)S(1)}, bf16[512,256]{1,0:T(8,128)(2,1)S(1)}, u32[]{:S(2)}, u32[]{:S(2)}) collective-permute-start(bf16[512,256]{1,0:T(8,128)(2,1)S(1)} %get-tuple-element.18.own_ref), channel_id=1, source_target_pairs={{0,24},{4,28},{1,25},{5,29},{2,26},{6,30},{3,27},{7,31}} | collective-permute-start | bytes 786440 | tf_op jit(solution)/shard_map/ppermute | solution.py:22
  50.8 14.4 %collective-permute-start.2 = (bf16[512,256]{1,0:T(8,128)(2,1)S(1)}, bf16[512,256]{1,0:T(8,128)(2,1)S(1)}, u32[]{:S(2)}, u32[]{:S(2)}) collective-permute-start(bf16[512,256]{1,0:T(8,128)(2,1)S(1)} %get-tuple-element.18.own_ref), channel_id=1, source_target_pairs={{0,16},{4,20},{8,24},{12,28},{1,17},{5,21},{9,25},{13,29},{2,18},{... | collective-permute-start | bytes 786440 | tf_op jit(solution)/shard_map/ppermute | solution.py:22
  52.2 15.3 %collective-permute-start.1 = (bf16[512,256]{1,0:T(8,128)(2,1)S(1)}, bf16[512,256]{1,0:T(8,128)(2,1)S(1)}, u32[]{:S(2)}, u32[]{:S(2)}) collective-permute-start(bf16[512,256]{1,0:T(8,128)(2,1)S(1)} %get-tuple-element.18.own_ref), channel_id=1, source_target_pairs={{0,8},{4,12},{8,16},{12,20},{16,24},{20,28},{1,9},{5,13},{9,17},{1... | collective-permute-start | bytes 786440 | tf_op jit(solution)/shard_map/ppermute | solution.py:22
  54.7 5.5 %collective-permute-start.9 = (bf16[320,512]{1,0:T(8,128)(2,1)S(1)}, bf16[320,512]{1,0:T(8,128)(2,1)S(1)}, u32[]{:S(2)}, u32[]{:S(2)}) collective-permute-start(bf16[320,512]{1,0:T(8,128)(2,1)S(1)} %collective-permute-done.8.far), channel_id=1, source_target_pairs={{0,1},{1,0},{2,3},{3,2},{4,5},{5,4},{6,7},{7,6},{8,9},{9,8},{10,11... | collective-permute-start | bytes 983048 | tf_op jit(solution)/shard_map/ppermute | solution.py:17
  59.6 17.5 %copy-start = (bf16[320,1024]{1,0:T(8,128)(2,1)}, bf16[320,1024]{1,0:T(8,128)(2,1)S(1)}, u32[]{:S(2)}) copy-start(bf16[320,1024]{1,0:T(8,128)(2,1)S(1)} %get-tuple-element.28.refs_3_) | copy-start | bytes 1966084
  59.7 17.5 %collective-permute-start.14 = (bf16[320,1024]{1,0:T(8,128)(2,1)S(1)}, bf16[320,1024]{1,0:T(8,128)(2,1)S(1)}, u32[]{:S(2)}, u32[]{:S(2)}) collective-permute-start(bf16[320,1024]{1,0:T(8,128)(2,1)S(1)} %get-tuple-element.29), channel_id=1, source_target_pairs={{0,1},{1,0},{2,3},{3,2},{4,5},{5,4},{6,7},{7,6},{8,9},{9,8},{10,11... | collective-permute-start | bytes 1966088 | tf_op jit(solution)/shard_map/ppermute | solution.py:17
  65.1 29.5 %copy-start.1 = (bf16[320,1024]{1,0:T(8,128)(2,1)}, bf16[320,1024]{1,0:T(8,128)(2,1)S(1)}, u32[]{:S(2)}) copy-start(bf16[320,1024]{1,0:T(8,128)(2,1)S(1)} %get-tuple-element.26.refs_0_) | copy-start | bytes 1966084
  65.1 13.8 %collective-permute-start.10 = (bf16[320,1024]{1,0:T(8,128)(2,1)S(1)}, bf16[320,1024]{1,0:T(8,128)(2,1)S(1)}, u32[]{:S(2)}, u32[]{:S(2)}) collective-permute-start(bf16[320,1024]{1,0:T(8,128)(2,1)S(1)} %get-tuple-element.27), channel_id=1, source_target_pairs={{0,1},{1,0},{2,3},{3,2},{4,5},{5,4},{6,7},{7,6},{8,9},{9,8},{10,11... | collective-permute-start | bytes 1966088 | tf_op jit(solution)/shard_map/ppermute | solution.py:17
  71.7 4.3 %collective-permute-start.4 = (bf16[256,128]{1,0:T(8,128)(2,1)S(1)}, bf16[256,128]{1,0:T(8,128)(2,1)S(1)}, u32[]{:S(2)}, u32[]{:S(2)}) collective-permute-start(bf16[256,128]{1,0:T(8,128)(2,1)S(1)} %get-tuple-element.20), channel_id=1, source_target_pairs={{0,4},{4,0},{8,12},{12,8},{16,20},{20,16},{24,28},{28,24},{1,5},{5... | collective-permute-start | bytes 196616 | tf_op jit(solution)/shard_map/ppermute | solution.py:17
  77.1 31.0 %collective-permute-start.5 = (bf16[128,2048]{1,0:T(8,128)(2,1)S(1)}, bf16[128,2048]{1,0:T(8,128)(2,1)}, u32[]{:S(2)}, u32[]{:S(2)}) collective-permute-start(bf16[128,2048]{1,0:T(8,128)(2,1)S(1)} %get-tuple-element.22), channel_id=1, source_target_pairs={{0,1},{1,0},{2,3},{3,2},{4,5},{5,4},{6,7},{7,6},{8,9},{9,8},{10,11... | collective-permute-start | bytes 1572872 | tf_op jit(solution)/shard_map/ppermute | solution.py:17
  77.1 17.4 %copy-start.8 = (bf16[320,1024]{1,0:T(8,128)(2,1)}, bf16[320,1024]{1,0:T(8,128)(2,1)S(1)}, u32[]{:S(2)}) copy-start(bf16[320,1024]{1,0:T(8,128)(2,1)S(1)} %collective-permute-done.14.refs_4_) | copy-start | bytes 1966084
  77.3 10.6 %collective-permute-start.15 = (bf16[320,512]{1,0:T(8,128)(2,1)S(1)}, bf16[320,512]{1,0:T(8,128)(2,1)S(1)}, u32[]{:S(2)}, u32[]{:S(2)}) collective-permute-start(bf16[320,512]{1,0:T(8,128)(2,1)S(1)} %add_convert_fusion), channel_id=1, source_target_pairs={{0,2},{1,3},{2,0},{3,1},{4,6},{5,7},{6,4},{7,5},{8,10},{9,11},{10,... | collective-permute-start | bytes 983048 | tf_op jit(solution)/shard_map/ppermute | solution.py:17
  78.9 15.7 %copy-start.9 = (bf16[320,1024]{1,0:T(8,128)(2,1)}, bf16[320,1024]{1,0:T(8,128)(2,1)S(1)}, u32[]{:S(2)}) copy-start(bf16[320,1024]{1,0:T(8,128)(2,1)S(1)} %collective-permute-done.10.refs_1_) | copy-start | bytes 1966084
  79.0 15.6 %collective-permute-start.11 = (bf16[320,512]{1,0:T(8,128)(2,1)S(1)}, bf16[320,512]{1,0:T(8,128)(2,1)}, u32[]{:S(2)}, u32[]{:S(2)}) collective-permute-start(bf16[320,512]{1,0:T(8,128)(2,1)S(1)} %add_convert_fusion.1), channel_id=1, source_target_pairs={{0,2},{1,3},{2,0},{3,1},{4,6},{5,7},{6,4},{7,5},{8,10},{9,11},{10,... | collective-permute-start | bytes 983048 | tf_op jit(solution)/shard_map/ppermute | solution.py:17
  97.1 28.0 %all-to-all-start.1 = ((bf16[8,80,512]{2,1,0:T(8,128)(2,1)}), bf16[8,80,512]{2,1,0:T(8,128)(2,1)S(1)}, u32[]{:S(2)}, u32[]{:S(2)}) async-start(bf16[8,80,512]{2,1,0:T(8,128)(2,1)} %bitcast.25), calls=%async_computation.1 | async-start | bytes 1310720 | tf_op jit(solution)/shard_map/all_to_all | solution.py:458
  109.0 7.6 %collective-permute-start.6 = (bf16[64,2048]{1,0:T(8,128)(2,1)S(1)}, bf16[64,2048]{1,0:T(8,128)(2,1)S(1)}, u32[]{:S(2)}, u32[]{:S(2)}) collective-permute-start(bf16[64,2048]{1,0:T(8,128)(2,1)S(1)} %add_convert_fusion.3), channel_id=1, source_target_pairs={{0,2},{1,3},{2,0},{3,1},{4,6},{5,7},{6,4},{7,5},{8,10},{9,11},{10,... | collective-permute-start | bytes 786440 | tf_op jit(solution)/shard_map/ppermute | solution.py:17
  (7 other events, 46.4 us)

commit v3 on v2

--- a/solution.py
+++ b/solution.py
@@ -17,9 +17,17 @@
     return lax.ppermute(x, axis, [(i, i ^ mask) for i in range(count)])
 
 
-def later(x, axis, step):
+def ep_of(here_ref):
+    return lax.div(here_ref[0], lax.axis_size("tp"))
+
+
+def tp_of(here_ref):
+    return lax.rem(here_ref[0], lax.axis_size("tp"))
+
+
+def onward(x, axis, step, first):
     count = lax.axis_size(axis)
-    return lax.ppermute(x, axis, [(i, i + step) for i in range(count - step)])
+    return lax.ppermute(x, axis, [(i, i + step) for i in range(first, count - step)])
 
 
 def gathered_keys(key_rows, value_rows):
@@ -74,7 +82,7 @@
 
 
 def pick_kernel(place_ref, query_ref, key_ref, value_ref, out_ref):
-    other = 1 - (place_ref[0] & 1)
+    other = 1 - (ep_of(place_ref) & 1)
     at = 0
     for ref in (query_ref, key_ref, value_ref):
         wide = ref.shape[1] // 2
@@ -83,7 +91,7 @@
 
 
 def merge_kernel(place_ref, query_ref, key_ref, value_ref, got_ref, query_out, block_out):
-    mine = place_ref[0] & 1
+    mine = ep_of(place_ref) & 1
     rows = query_ref.shape[0]
     pair, deep = key_ref.shape[1] // 2, value_ref.shape[1] // 2
     own, other = half(mine, rows), half(1 - mine, rows)
@@ -99,7 +107,7 @@
     gain_ref, keep_ref, send_ref, attended = rest[-4:]
     rows = query_ref.shape[0] // 2
     pair = 2 * head_width
-    mine, line_place = place_ref[0] & 1, place_ref[0] >> 1
+    mine, line_place = ep_of(place_ref) & 1, ep_of(place_ref) >> 1
     causal = lax.broadcasted_iota(jnp.int32, (rows, rows), 0) >= lax.broadcasted_iota(
         jnp.int32, (rows, rows), 1
     )
@@ -151,7 +159,7 @@
 
 
 def project_kernel(place_ref, own_ref, got_ref, weight_ref, keep_ref, send_ref, attended):
-    mine, place = place_ref[0] & 1, place_ref[1]
+    mine, place = ep_of(place_ref) & 1, tp_of(place_ref)
     rows, deep = own_ref.shape
     attended[:, half(mine, deep)] = own_ref[...]
     attended[:, half(1 - mine, deep)] = got_ref[...]
@@ -163,13 +171,24 @@
         ).astype(BF16)
 
 
-def local(kernel, outs, operands, smem=1, scratch=(), flops=1000000, limit=20):
+def local(kernel, outs, operands, smem=1, scratch=(), flops=1000000, limit=12, far=0):
     size = sum(x.size for x in operands)
+    operands = list(operands)
+    specs, options = [VMEM] * (len(operands) - smem), {}
+    outs_specs = [VMEM] * len(outs)
+    if far:
+        for n in range(smem, smem + far):
+            operands[n] = pltpu.with_memory_space_constraint(operands[n], pltpu.HBM)
+        whole = lambda i: (0, 0)
+        options["grid"] = (1,)
+        specs = [pl.BlockSpec(x.shape, whole) for x in operands[smem:]]
+        outs_specs = [pl.BlockSpec(shape, whole) for shape in outs]
     return pl.pallas_call(
         kernel,
         out_shape=[jax.ShapeDtypeStruct(shape, BF16) for shape in outs],
-        in_specs=[SMEM] * smem + [VMEM] * (len(operands) - smem),
-        out_specs=[VMEM] * len(outs),
+        in_specs=[SMEM] * smem + specs,
+        out_specs=outs_specs,
+        **options,
         scratch_shapes=list(scratch),
         compiler_params=pltpu.CompilerParams(vmem_limit_bytes=limit * 1024 * 1024),
         cost_estimate=pl.CostEstimate(
@@ -178,12 +197,11 @@
     )(*operands)
 
 
-def dispatch_kernel(
-    experts, capacity, place_ref, ids_ref, rows_ref, gain_ref, out_ref, onehot_ref
-):
+def dispatch_kernel(experts, capacity, here_ref, ids_ref, rows_ref, gain_ref, *rest):
+    outs, onehot_ref, rank_ref = rest[:-2], rest[-2], rest[-1]
     rows, _ = rows_ref.shape
-    cols = out_ref.shape[1]
-    first = pl.multiple_of(place_ref[0] * cols, cols)
+    cols = outs[0].shape[1]
+    first = pl.multiple_of(tp_of(here_ref) * cols, cols)
     wide = rows_ref[...].astype(F32)
     scale = lax.rsqrt(jnp.mean(wide * wide, axis=-1, keepdims=True) + EPS)
     part = rows_ref[:, pl.ds(first, cols)].astype(F32)
@@ -195,39 +213,44 @@
         < lax.broadcasted_iota(jnp.int32, (rows, rows), 1)
     ).astype(F32).astype(BF16)
     rank = jnp.dot(named.astype(F32).astype(BF16), before, preferred_element_type=F32)
-    rank = jnp.where(named, rank, -1.0)
+    rank_ref[...] = jnp.where(named, rank, -1.0)
     slot = lax.broadcasted_iota(jnp.int32, (capacity, rows), 0).astype(F32)
-    for e in range(experts):
-        onehot_ref[e * capacity : (e + 1) * capacity, :] = (
-            rank[e : e + 1, :] == slot
+    for k in range(experts):
+        e = ep_of(here_ref) ^ k if len(outs) > 1 else k
+        onehot_ref[k * capacity : (k + 1) * capacity, :] = (
+            rank_ref[pl.ds(e, 1), :] == slot
         ).astype(F32)
-    out_ref[...] = jnp.dot(
-        onehot_ref[...].astype(BF16), normed, preferred_element_type=F32
-    ).astype(BF16)
-
-
-def dispatched(expert_input, norm_gain, ids_across, capacity):
+    count = onehot_ref.shape[0] // len(outs)
+    for k, out_ref in enumerate(outs):
+        out_ref[...] = jnp.dot(
+            onehot_ref[k * count : (k + 1) * count, :].astype(BF16),
+            normed,
+            preferred_element_type=F32,
+        ).astype(BF16)
+
+
+def dispatched(here, expert_input, norm_gain, ids_across, capacity, pieces):
     rows, width = expert_input.shape
     experts = lax.axis_size("ep")
     cols = width // lax.axis_size("tp")
     slots = experts * capacity
-    vmem = pl.BlockSpec(memory_space=pltpu.VMEM)
     return pl.pallas_call(
         functools.partial(dispatch_kernel, experts, capacity),
-        out_shape=jax.ShapeDtypeStruct((slots, cols), BF16),
-        in_specs=[pl.BlockSpec(memory_space=pltpu.SMEM), vmem, vmem, vmem],
-        out_specs=vmem,
-        scratch_shapes=[pltpu.VMEM((slots, rows), F32)],
+        out_shape=[jax.ShapeDtypeStruct((slots // pieces, cols), BF16)] * pieces,
+        in_specs=[SMEM, VMEM, VMEM, VMEM],
+        out_specs=[VMEM] * pieces,
+        scratch_shapes=[pltpu.VMEM((slots, rows), F32), pltpu.VMEM((experts, rows), F32)],
         cost_estimate=pl.CostEstimate(
             flops=2 * slots * rows * cols, bytes_accessed=2 * rows * width, transcendentals=rows
         ),
         name="dispatch",
-    )(
-        lax.axis_index("tp").astype(jnp.int32).reshape(1),
-        ids_across,
-        expert_input,
-        norm_gain.reshape(1, width),
-    )
+    )(here, ids_across, expert_input, norm_gain.reshape(1, width))
+
+
+def arrange_kernel(here_ref, *refs):
+    out_ref = refs[-1]
+    for k, ref in enumerate(refs[:-1]):
+        out_ref[half(ep_of(here_ref) ^ k, ref.shape[0]), :] = ref[...]
 
 
 def fetch_kernel(gate, up, down, gate_w, up_w, down_w, sem):
@@ -254,7 +277,7 @@
         out_specs=[vmem] * 3,
         out_shape=[pltpu.VMEM(w.shape[1:], w.dtype) for w in weights],
         scratch_shapes=[pltpu.SemaphoreType.DMA((12,))],
-        compiler_params=pltpu.CompilerParams(vmem_limit_bytes=24 * 1024 * 1024),
+        compiler_params=pltpu.CompilerParams(vmem_limit_bytes=4 * 1024 * 1024),
         cost_estimate=pl.CostEstimate(
             flops=sum(w.size for w in weights) * 100,
             bytes_accessed=sum(w.size for w in weights) * 2,
@@ -301,7 +324,7 @@
         in_specs=[pl.BlockSpec(memory_space=pltpu.SMEM)] + [vmem] * 7,
         out_specs=[vmem, vmem],
         out_shape=[jax.ShapeDtypeStruct((rows, 2 * cols), BF16)] * 2,
-        compiler_params=pltpu.CompilerParams(vmem_limit_bytes=30 * 1024 * 1024),
+        compiler_params=pltpu.CompilerParams(vmem_limit_bytes=16 * 1024 * 1024),
         cost_estimate=pl.CostEstimate(
             flops=6 * rows * width * units,
             bytes_accessed=6 * width * units + 4 * rows * width,
@@ -318,28 +341,29 @@
     )
 
 
-def total_kernel(*refs):
-    out_ref = refs[-1]
-    rows, _ = refs[2].shape
-    for i in range((len(refs) - 1) // 3):
-        keep_ref, got_ref, over_ref = refs[3 * i : 3 * i + 3]
-        out_ref[i * rows : (i + 1) * rows, :] = (
-            keep_ref[...].astype(F32)
-            + got_ref[...].astype(F32)
-            + over_ref[...].astype(F32)
-        ).astype(BF16)
-
-
-def total(mine, gots):
-    rows, cols = gots[0].shape
-    operands = [x for (keep, got), over in zip(mine, gots) for x in (keep, got, over)]
-    first = pl.BlockSpec((rows, cols), lambda i: (0, 0))
+def total_kernel(first, keep_ref, got_ref, over_ref, *rest):
+    out_ref, part, sem = rest[-3:]
+    rows, cols = part.shape
+    part[...] = (
+        keep_ref[:, :cols].astype(F32) + got_ref[:, :cols].astype(F32) + over_ref[...].astype(F32)
+    ).astype(BF16)
+    copy = pltpu.make_async_copy(part, out_ref.at[first : first + rows, :], sem)
+    copy.start()
+    copy.wait()
+
+
+def total(slots, first, keep, got, over, held=None):
+    rows, cols = over.shape
+    hbm = pl.BlockSpec(memory_space=pltpu.HBM)
+    operands = [keep, got, over] + ([] if held is None else [held])
     return pl.pallas_call(
-        total_kernel,
-        out_shape=jax.ShapeDtypeStruct((len(gots) * rows, cols), BF16),
-        grid=(1,),
-        in_specs=[first] * len(operands),
-        out_specs=pl.BlockSpec((len(gots) * rows, cols), lambda i: (0, 0)),
+        functools.partial(total_kernel, first),
+        out_shape=jax.ShapeDtypeStruct((slots, cols), BF16),
+        in_specs=[VMEM] * 3 + [hbm] * (len(operands) - 3),
+        out_specs=hbm,
+        scratch_shapes=[pltpu.VMEM((rows, cols), BF16), pltpu.SemaphoreType.DMA],
+        input_output_aliases={} if held is None else {3: 0},
+        compiler_params=pltpu.CompilerParams(vmem_limit_bytes=8 * 1024 * 1024),
         cost_estimate=pl.CostEstimate(
             flops=4 * rows * cols, bytes_accessed=16 * rows * cols, transcendentals=0
         ),
@@ -387,35 +411,42 @@
     weight_across = route_weight.T
 
     weights = fetched(gate_weight, up_weight, down_weight)
-    outgoing = dispatched(expert_input, norm_gain, ids_across, capacity)
-    own = lax.all_to_all(
-        outgoing.reshape(experts, capacity, cols), "ep", split_axis=0, concat_axis=0, tiled=True
-    ).reshape(slots, cols)
-    small = experts <= 8 and experts % 2 == 0 and head_lambda.shape[0] == 2
-    here = jnp.stack([lax.axis_index("ep"), lax.axis_index("tp")]).astype(jnp.int32)
+    small = experts <= 8 and experts & (experts - 1) == 0 and head_lambda.shape[0] == 2
+    here = lax.axis_index("ep") * lax.axis_size("tp") + lax.axis_index("tp")
+    here = here.astype(jnp.int32).reshape(1)
+    outgoing = dispatched(
+        here, expert_input, norm_gain, ids_across, capacity, experts if small else 1
+    )
+    if small:
+        arrived = [outgoing[0]] + [swap(outgoing[k], "ep", k) for k in range(1, experts)]
+        (own,) = local(arrange_kernel, [(slots, cols)], (here, *arrived))
+    else:
+        own = lax.all_to_all(
+            outgoing[0].reshape(experts, capacity, cols), "ep", 0, 0, tiled=True
+        ).reshape(slots, cols)
     if small:
         rows_a, deep = queries.shape[0], value_rows.shape[1] // 2
         pair = queries.shape[1] // 2
         trio = (queries, key_rows, value_rows)
-        (picked,) = local(pick_kernel, [(rows_a, 2 * pair + deep)], (here, *trio))
+        (picked,) = local(pick_kernel, [(rows_a, 2 * pair + deep)], (here, *trio), far=3)
         got = swap(picked, "ep", 1)
         query, block = local(
-            merge_kernel, [(2 * rows_a, pair), (2 * rows_a, pair + deep)], (here, *trio, got)
+            merge_kernel, [(2 * rows_a, pair), (2 * rows_a, pair + deep)], (here, *trio, got), far=3
         )
-        block, _ = lax.optimization_barrier((block, own))
     near = swap(own, "tp", 1)
     halves = 2
     part = slots // halves
     order = jnp.array([0, 1, 2, 3, 1, 3, 0, 2], jnp.int32) ^ place
     fars = [swap(own[i * part : (i + 1) * part], "tp", 2) for i in range(halves)]
     if small:
-        blocks = [later(block, "ep", 2 * k) for k in range(1, experts // 2)]
+        blocks = []
+        for k in range(1, experts // 2):
+            moving = blocks[k - 3] if k > 2 else block
+            blocks.append(onward(moving, "ep", 2 * min(k, 2), 2 * max(k - 2, 0)))
     mine, gots = [], []
     for i in range(halves):
         cross = swap(fars[i], "tp", 1)
-        keep, send = ffn(
-            order, i * part, own, near, fars[i], cross, weights
-        )
+        keep, send = ffn(order, i * part, own, near, fars[i], cross, weights)
         got = swap(send, "tp", 1)
         across = (keep[:, cols:].astype(F32) + got[:, cols:].astype(F32)).astype(BF16)
         gots.append(swap(across, "tp", 2))
@@ -428,7 +459,7 @@
             smem=2,
             scratch=[pltpu.VMEM((2 * rows_a, deep), BF16)],
             flops=16 * rows_a * rows_a * experts * pair,
-            limit=28,
+            limit=20,
         )
         got = swap(sent, "ep", 1)
         model = out_weight.shape[1]
@@ -454,7 +485,9 @@
             share.reshape(lax.axis_size("tp"), -1, share.shape[1]), "tp", 0, 0, tiled=True
         )
         mixer_out = jnp.sum(parts.astype(F32), axis=0).astype(BF16)
-    summed = total(mine, gots)
+    summed = None
+    for i, ((keep, got), over) in enumerate(zip(mine, gots)):
+        summed = total(slots, i * part, keep, got, over, summed)
     returned = lax.all_to_all(
         summed.reshape(experts, capacity, cols), "ep", split_axis=0, concat_axis=0, tiled=True
     ).reshape(slots, cols)

time: 127 us -> 117 us (0.921)
  blocking collectives: 24.9 us -> 0 us
  starting transfers between devices: 27 us -> 40.2 us
  waiting for transfers between devices: 42.7 us -> 47.1 us
  other arithmetic: 3.1 us -> 1.13 us
    all_to_all x1 -> x0, blocking collectives: 24.9 us -> none  [shards(): lax.all_to_all(outgoing.reshape(experts, capacity, cols), 'ep', split_axi...]
    ppermute x13 -> x20, starting transfers between devices: 9.06 us -> 22.2 us  [swap(): return lax.ppermute(x, axis, [(i, i ^ mask) for i in range(count)])]
    ppermute x13 -> x20, waiting for transfers between devices: 33.7 us -> 38.5 us  [swap(): return lax.ppermute(x, axis, [(i, i ^ mask) for i in range(count)])]
    ppermute x3, waiting for transfers between devices: 2.3 us -> 0.01 us  [onward(): lax.ppermute(x, axis, [(i, i + step) for i in range(first, count - step)])]
    all_to_all x1, waiting for transfers between devices: 6.69 us -> 8.58 us  [shards(): lax.all_to_all(summed.reshape(experts, capacity, cols), 'ep', split_axis=...]
    ppermute x3, starting transfers between devices: 7.02 us -> 8.54 us  [onward(): lax.ppermute(x, axis, [(i, i + step) for i in range(first, count - step)])]
    all_to_all x1, starting transfers between devices: 10.9 us -> 9.45 us  [shards(): lax.all_to_all(summed.reshape(experts, capacity, cols), 'ep', split_axis=...]
    pallas_call x1 -> x2, Pallas kernels: 2.55 us -> 1.73 us  [total(): pl.pallas_call(functools.partial(total_kernel, first), out_shape=jax.Shap...]
  transfers between devices with their start and end apart: 17 -> 24, of which waited for: 8 -> 10; matrix products, arithmetic and copies ran while one was open for 3% -> 1% of each run, Pallas kernels for 18% -> 19%
where the time goes in v3:
time: 117 us
  waiting for transfers between devices  47.1 us (40%)
  starting transfers between devices  40.2 us (34%)
  Pallas kernels  24.9 us (21%)
  matrix products  1.63 us (1%)
    ppermute x20, waiting for transfers between devices, swap(): return lax.ppermute(x, axis, [(i, i ^ mask) for i in range(count)])  38.5 us
    ppermute x20, starting transfers between devices, swap(): return lax.ppermute(x, axis, [(i, i ^ mask) for i in range(count)])  22.2 us
    pallas_call x2, Pallas kernels, ffn(): pl.pallas_call(functools.partial(ffn_kernel, first), in_specs=[pl.BlockSp...  9.73 us
    all_to_all x1, starting transfers between devices, shards(): lax.all_to_all(summed.reshape(experts, capacity, cols), 'ep', split_axis=...  9.45 us
    all_to_all x1, waiting for transfers between devices, shards(): lax.all_to_all(summed.reshape(experts, capacity, cols), 'ep', split_axis=...  8.58 us
    ppermute x3, starting transfers between devices, onward(): lax.ppermute(x, axis, [(i, i + step) for i in range(first, count - step)])  8.54 us
    pallas_call x5, Pallas kernels, local(): pl.pallas_call(kernel, out_shape=[jax.ShapeDtypeStruct(shape, BF16) for s...  6.79 us
    pallas_call x1, Pallas kernels, fetched(): pl.pallas_call(fetch_kernel, in_specs=[hbm] * 3, out_specs=[vmem] * 3, ou...  4.25 us
  transfers between devices with their start and end apart: 24, of which 10 were waited for; matrix products, arithmetic and copies ran while one was open for 1% of the time, Pallas kernels for 19%

profile of v3, /device:TPU:0, one launch (start us, length us, event | category | flops | bytes accessed | tf_op | source)
XLA Modules:
  0.0 116.9 jit_solution(8204943784996496689)
XLA Ops:
  0.6 2.4 %dispatch.1 = (bf16[80,512]{1,0:T(8,128)(2,1)}, bf16[80,512]{1,0:T(8,128)(2,1)}, bf16[80,512]{1,0:T(8,128)(2,1)}, bf16[80,512]{1,0:T(8,128)(2,1)}, bf16[80,512]{...) custom-call(s32[1]{0:T(128)} %bitcast.place_ref.here_ref, ...), custom_call_target="tpu_custom_call" | custom-call | flops 125829120 | bytes 786432 | tf_op jit(solution)/shard_map/dispatch/pallas_call | solution.py:237
  3.0 4.1 %collective-permute-start.10 = (bf16[80,512]{1,0:T(8,128)(2,1)}, bf16[80,512]{1,0:T(8,128)(2,1)S(1)}, u32[]{:S(2)}, u32[]{:S(2)}) collective-permute-start(bf16[80,512]{1,0:T(8,128)(2,1)} %get-tuple-element.33), channel_id=1, source_target_pairs={{0,16},{4,20},{8,24},{12,28},{16,0},{20,4},{24,8},{28,12},{1,17},{... | collective-permute-start | bytes 245768 | tf_op jit(solution)/shard_map/ppermute | solution.py:17
  8.4 3.6 %collective-permute-start.12 = (bf16[80,512]{1,0:T(8,128)(2,1)}, bf16[80,512]{1,0:T(8,128)(2,1)S(1)}, u32[]{:S(2)}, u32[]{:S(2)}) collective-permute-start(bf16[80,512]{1,0:T(8,128)(2,1)} %get-tuple-element.35), channel_id=1, source_target_pairs={{0,24},{4,28},{8,16},{12,20},{16,8},{20,12},{24,0},{28,4},{1,25},{... | collective-permute-start | bytes 245768 | tf_op jit(solution)/shard_map/ppermute | solution.py:17
  12.0 1.7 %collective-permute-start.7 = (bf16[80,512]{1,0:T(8,128)(2,1)}, bf16[80,512]{1,0:T(8,128)(2,1)S(1)}, u32[]{:S(2)}, u32[]{:S(2)}) collective-permute-start(bf16[80,512]{1,0:T(8,128)(2,1)} %get-tuple-element.30), channel_id=1, source_target_pairs={{0,4},{4,0},{8,12},{12,8},{16,20},{20,16},{24,28},{28,24},{1,5},{5... | collective-permute-start | bytes 245768 | tf_op jit(solution)/shard_map/ppermute | solution.py:17
  13.7 4.0 %collective-permute-start.8 = (bf16[80,512]{1,0:T(8,128)(2,1)}, bf16[80,512]{1,0:T(8,128)(2,1)S(1)}, u32[]{:S(2)}, u32[]{:S(2)}) collective-permute-start(bf16[80,512]{1,0:T(8,128)(2,1)} %get-tuple-element.31), channel_id=1, source_target_pairs={{0,8},{4,12},{8,0},{12,4},{16,24},{20,28},{24,16},{28,20},{1,9},{5... | collective-permute-start | bytes 245768 | tf_op jit(solution)/shard_map/ppermute | solution.py:17
  17.7 2.5 %collective-permute-done.11.refs_5_ = bf16[80,512]{1,0:T(8,128)(2,1)S(1)} collective-permute-done((bf16[80,512]{1,0:T(8,128)(2,1)}, bf16[80,512]{1,0:T(8,128)(2,1)S(1)}, u32[]{:S(2)}, u32[]{:S(2)}) %collective-permute-start.11) | collective-permute-done | bytes 81952 | tf_op jit(solution)/shard_map/ppermute | solution.py:17
  20.7 5.1 %collective-permute-done.9.refs_3_ = bf16[80,512]{1,0:T(8,128)(2,1)S(1)} collective-permute-done((bf16[80,512]{1,0:T(8,128)(2,1)}, bf16[80,512]{1,0:T(8,128)(2,1)S(1)}, u32[]{:S(2)}, u32[]{:S(2)}) %collective-permute-start.9) | collective-permute-done | bytes 81952 | tf_op jit(solution)/shard_map/ppermute | solution.py:17
  26.8 1.6 %collective-permute-start.19 = (bf16[320,512]{1,0:T(8,128)(2,1)S(1)}, bf16[320,512]{1,0:T(8,128)(2,1)S(1)}, u32[]{:S(2)}, u32[]{:S(2)}) collective-permute-start(bf16[320,512]{1,0:T(8,128)(2,1)S(1)} %get-tuple-element.44), channel_id=1, source_target_pairs={{0,2},{1,3},{2,0},{3,1},{4,6},{5,7},{6,4},{7,5},{8,10},{9,11},{10,... | collective-permute-start | bytes 983048 | tf_op jit(solution)/shard_map/ppermute | solution.py:17
  30.6 4.3 %collective-permute-done.19.far = bf16[320,512]{1,0:T(8,128)(2,1)S(1)} collective-permute-done((bf16[320,512]{1,0:T(8,128)(2,1)S(1)}, bf16[320,512]{1,0:T(8,128)(2,1)S(1)}, u32[]{:S(2)}, u32[]{:S(2)}) %collective-permute-start.19) | collective-permute-done | bytes 327712 | tf_op jit(solution)/shard_map/ppermute | solution.py:17
  34.9 1.9 %collective-permute-done.got_ref = bf16[256,384]{1,0:T(8,128)(2,1)S(1)} collective-permute-done((bf16[256,384]{1,0:T(8,128)(2,1)S(1)}, bf16[256,384]{1,0:T(8,128)(2,1)S(1)}, u32[]{:S(2)}, u32[]{:S(2)}) %collective-permute-start) | collective-permute-done | bytes 196640 | tf_op jit(solution)/shard_map/ppermute | solution.py:17
  37.9 2.2 %collective-permute-start.1 = (bf16[512,256]{1,0:T(8,128)(2,1)S(1)}, bf16[512,256]{1,0:T(8,128)(2,1)S(1)}, u32[]{:S(2)}, u32[]{:S(2)}) collective-permute-start(bf16[512,256]{1,0:T(8,128)(2,1)S(1)} %get-tuple-element.24.own_ref), channel_id=1, source_target_pairs={{0,8},{4,12},{8,16},{12,20},{16,24},{20,28},{1,9},{5,13},{9,17},{1... | collective-permute-start | bytes 786440 | tf_op jit(solution)/shard_map/ppermute | solution.py:30
  40.1 4.3 %fetch.1 = (bf16[2048,896]{1,0:T(8,128)(2,1)S(1)}, bf16[2048,896]{1,0:T(8,128)(2,1)S(1)}, bf16[896,2048]{1,0:T(8,128)(2,1)S(1)}) custom-call(bf16[1,2048,896]{2,1,0:T(8,128)(2,1)} %gate.1, bf16[1,2048,896]{2,1,0:T(8,128)(2,1)} %up.1, bf16[1,896,2048]{2,1,0:T(8,128)(2,1)} %down.1), custom_call_target="tpu_custom_call" | custom-call | flops 550502400 | bytes 11010048 | tf_op jit(solution)/shard_map/fetch/pallas_call | solution.py:274
  44.4 5.6 %collective-permute-start.2 = (bf16[512,256]{1,0:T(8,128)(2,1)S(1)}, bf16[512,256]{1,0:T(8,128)(2,1)S(1)}, u32[]{:S(2)}, u32[]{:S(2)}) collective-permute-start(bf16[512,256]{1,0:T(8,128)(2,1)S(1)} %get-tuple-element.24.own_ref), channel_id=1, source_target_pairs={{0,16},{4,20},{8,24},{12,28},{1,17},{5,21},{9,25},{13,29},{2,18},{... | collective-permute-start | bytes 786440 | tf_op jit(solution)/shard_map/ppermute | solution.py:30
  50.9 4.9 %ffn.3 = (bf16[320,1024]{1,0:T(8,128)(2,1)S(1)}, bf16[320,1024]{1,0:T(8,128)(2,1)S(1)}) custom-call(s32[8]{0:T(128)S(1)} %broadcast_xor_fusion.order_ref, bf16[640,512]{1,0:T(8,128)(2,1)S(1)} %shard_map.153.own, bf16[640,512]{1,0:T(8,128)(2,1)S(1)} %collective-permute-done.14.near, bf16[320,512]{1,0:T(8,128)(2,1)S(1)} %collective-permute-done.19.far, ...), custom_call_target="tpu_custom_call" | custom-call | flops 3523215360 | bytes 13631488 | tf_op jit(solution)/shard_map/ffn/pallas_call | solution.py:322
  56.3 4.9 %ffn.2 = (bf16[320,1024]{1,0:T(8,128)(2,1)S(1)}, bf16[320,1024]{1,0:T(8,128)(2,1)S(1)}) custom-call(s32[8]{0:T(128)S(1)} %broadcast_xor_fusion.order_ref, bf16[640,512]{1,0:T(8,128)(2,1)S(1)} %shard_map.153.own, bf16[640,512]{1,0:T(8,128)(2,1)S(1)} %collective-permute-done.14.near, bf16[320,512]{1,0:T(8,128)(2,1)S(1)} %collective-permute-done.15.far, ...), custom_call_target="tpu_custom_call" | custom-call | flops 3523215360 | bytes 13631488 | tf_op jit(solution)/shard_map/ffn/pallas_call | solution.py:322
  61.3 4.1 %shard_map.151 = (bf16[256,128]{1,0:T(8,128)(2,1)S(1)}, bf16[256,128]{1,0:T(8,128)(2,1)S(1)}) custom-call(s32[1]{0:T(128)} %bitcast.place_ref.here_ref, f32[2]{0:T(128)S(1)} %copy-done.2, bf16[512,128]{1,0:T(8,128)(2,1)S(1)} %get-tuple-element.23.query_ref, bf16[512,256]{1,0:T(8,128)(2,1)S(1)} %get-tuple-element.24.own_ref, ...), custom_call_target="tpu_custom_call" | custom-call | flops 1073741824 | bytes 1179910 | tf_op jit(solution)/shard_map/pallas_call | solution.py:186
  65.6 4.4 %collective-permute-done.4.got_ref = bf16[256,128]{1,0:T(8,128)(2,1)S(1)} collective-permute-done((bf16[256,128]{1,0:T(8,128)(2,1)S(1)}, bf16[256,128]{1,0:T(8,128)(2,1)S(1)}, u32[]{:S(2)}, u32[]{:S(2)}) %collective-permute-start.4) | collective-permute-done | bytes 65568 | tf_op jit(solution)/shard_map/ppermute | solution.py:17
  70.7 1.6 %collective-permute-start.22 = (bf16[320,512]{1,0:T(8,128)(2,1)S(1)}, bf16[320,512]{1,0:T(8,128)(2,1)S(1)}, u32[]{:S(2)}, u32[]{:S(2)}) collective-permute-start(bf16[320,512]{1,0:T(8,128)(2,1)S(1)} %add_convert_fusion), channel_id=1, source_target_pairs={{0,2},{1,3},{2,0},{3,1},{4,6},{5,7},{6,4},{7,5},{8,10},{9,11},{10,... | collective-permute-start | bytes 983048 | tf_op jit(solution)/shard_map/ppermute | solution.py:17
  73.1 8.2 %collective-permute-done.22.over_ref = bf16[320,512]{1,0:T(8,128)(2,1)S(1)} collective-permute-done((bf16[320,512]{1,0:T(8,128)(2,1)S(1)}, bf16[320,512]{1,0:T(8,128)(2,1)S(1)}, u32[]{:S(2)}, u32[]{:S(2)}) %collective-permute-start.22) | collective-permute-done | bytes 327712 | tf_op jit(solution)/shard_map/ppermute | solution.py:17
  82.2 5.7 %collective-permute-done.18.over_ref = bf16[320,512]{1,0:T(8,128)(2,1)S(1)} collective-permute-done((bf16[320,512]{1,0:T(8,128)(2,1)S(1)}, bf16[320,512]{1,0:T(8,128)(2,1)S(1)}, u32[]{:S(2)}, u32[]{:S(2)}) %collective-permute-start.18) | collective-permute-done | bytes 327712 | tf_op jit(solution)/shard_map/ppermute | solution.py:17
  88.8 9.4 %all-to-all-start = ((bf16[8,80,512]{2,1,0:T(8,128)(2,1)}), bf16[8,80,512]{2,1,0:T(8,128)(2,1)S(1)}, u32[]{:S(2)}, u32[]{:S(2)}) async-start(bf16[8,80,512]{2,1,0:T(8,128)(2,1)} %bitcast.9), calls=%async_computation | async-start | bytes 1310720 | tf_op jit(solution)/shard_map/all_to_all | solution.py:491
  98.3 1.6 %collective-permute-start.6 = (bf16[64,2048]{1,0:T(8,128)(2,1)S(1)}, bf16[64,2048]{1,0:T(8,128)(2,1)S(1)}, u32[]{:S(2)}, u32[]{:S(2)}) collective-permute-start(bf16[64,2048]{1,0:T(8,128)(2,1)S(1)} %add_convert_fusion.3), channel_id=1, source_target_pairs={{0,2},{1,3},{2,0},{3,1},{4,6},{5,7},{6,4},{7,5},{8,10},{9,11},{10,... | collective-permute-start | bytes 786440 | tf_op jit(solution)/shard_map/ppermute | solution.py:17
  99.9 6.1 %collective-permute-done.6 = bf16[64,2048]{1,0:T(8,128)(2,1)S(1)} collective-permute-done((bf16[64,2048]{1,0:T(8,128)(2,1)S(1)}, bf16[64,2048]{1,0:T(8,128)(2,1)S(1)}, u32[]{:S(2)}, u32[]{:S(2)}) %collective-permute-start.6) | collective-permute-done | bytes 262176 | tf_op jit(solution)/shard_map/ppermute | solution.py:17
  106.8 8.6 %all-to-all-done = bf16[8,80,512]{2,1,0:T(8,128)(2,1)S(1)} async-done(((bf16[8,80,512]{2,1,0:T(8,128)(2,1)}), bf16[8,80,512]{2,1,0:T(8,128)(2,1)S(1)}, u32[]{:S(2)}, u32[]{:S(2)}) %all-to-all-start) | async-done | bytes 655392 | tf_op jit(solution)/shard_map/all_to_all | solution.py:491
  (62 shorter events, 13.2 us)
Async XLA Ops:
  3.0 10.6 %collective-permute-start.10 = (bf16[80,512]{1,0:T(8,128)(2,1)}, bf16[80,512]{1,0:T(8,128)(2,1)S(1)}, u32[]{:S(2)}, u32[]{:S(2)}) collective-permute-start(bf16[80,512]{1,0:T(8,128)(2,1)} %get-tuple-element.33), channel_id=1, source_target_pairs={{0,16},{4,20},{8,24},{12,28},{16,0},{20,4},{24,8},{28,12},{1,17},{... | collective-permute-start | bytes 245768 | tf_op jit(solution)/shard_map/ppermute | solution.py:17
  7.1 13.1 %collective-permute-start.11 = (bf16[80,512]{1,0:T(8,128)(2,1)}, bf16[80,512]{1,0:T(8,128)(2,1)S(1)}, u32[]{:S(2)}, u32[]{:S(2)}) collective-permute-start(bf16[80,512]{1,0:T(8,128)(2,1)} %get-tuple-element.34), channel_id=1, source_target_pairs={{0,20},{4,16},{8,28},{12,24},{16,4},{20,0},{24,12},{28,8},{1,21},{... | collective-permute-start | bytes 245768 | tf_op jit(solution)/shard_map/ppermute | solution.py:17
  8.4 12.0 %collective-permute-start.12 = (bf16[80,512]{1,0:T(8,128)(2,1)}, bf16[80,512]{1,0:T(8,128)(2,1)S(1)}, u32[]{:S(2)}, u32[]{:S(2)}) collective-permute-start(bf16[80,512]{1,0:T(8,128)(2,1)} %get-tuple-element.35), channel_id=1, source_target_pairs={{0,24},{4,28},{8,16},{12,20},{16,8},{20,12},{24,0},{28,4},{1,25},{... | collective-permute-start | bytes 245768 | tf_op jit(solution)/shard_map/ppermute | solution.py:17
  12.0 8.4 %collective-permute-start.13 = (bf16[80,512]{1,0:T(8,128)(2,1)}, bf16[80,512]{1,0:T(8,128)(2,1)S(1)}, u32[]{:S(2)}, u32[]{:S(2)}) collective-permute-start(bf16[80,512]{1,0:T(8,128)(2,1)} %get-tuple-element.36), channel_id=1, source_target_pairs={{0,28},{4,24},{8,20},{12,16},{16,12},{20,8},{24,4},{28,0},{1,29},{... | collective-permute-start | bytes 245768 | tf_op jit(solution)/shard_map/ppermute | solution.py:17
  12.0 8.4 %collective-permute-start.7 = (bf16[80,512]{1,0:T(8,128)(2,1)}, bf16[80,512]{1,0:T(8,128)(2,1)S(1)}, u32[]{:S(2)}, u32[]{:S(2)}) collective-permute-start(bf16[80,512]{1,0:T(8,128)(2,1)} %get-tuple-element.30), channel_id=1, source_target_pairs={{0,4},{4,0},{8,12},{12,8},{16,20},{20,16},{24,28},{28,24},{1,5},{5... | collective-permute-start | bytes 245768 | tf_op jit(solution)/shard_map/ppermute | solution.py:17
  13.7 7.1 %collective-permute-start.8 = (bf16[80,512]{1,0:T(8,128)(2,1)}, bf16[80,512]{1,0:T(8,128)(2,1)S(1)}, u32[]{:S(2)}, u32[]{:S(2)}) collective-permute-start(bf16[80,512]{1,0:T(8,128)(2,1)} %get-tuple-element.31), channel_id=1, source_target_pairs={{0,8},{4,12},{8,0},{12,4},{16,24},{20,28},{24,16},{28,20},{1,9},{5... | collective-permute-start | bytes 245768 | tf_op jit(solution)/shard_map/ppermute | solution.py:17
  20.2 5.6 %collective-permute-start.9 = (bf16[80,512]{1,0:T(8,128)(2,1)}, bf16[80,512]{1,0:T(8,128)(2,1)S(1)}, u32[]{:S(2)}, u32[]{:S(2)}) collective-permute-start(bf16[80,512]{1,0:T(8,128)(2,1)} %get-tuple-element.32), channel_id=1, source_target_pairs={{0,12},{4,8},{8,4},{12,0},{16,28},{20,24},{24,20},{28,16},{1,13},{... | collective-permute-start | bytes 245768 | tf_op jit(solution)/shard_map/ppermute | solution.py:17
  26.8 8.1 %collective-permute-start.19 = (bf16[320,512]{1,0:T(8,128)(2,1)S(1)}, bf16[320,512]{1,0:T(8,128)(2,1)S(1)}, u32[]{:S(2)}, u32[]{:S(2)}) collective-permute-start(bf16[320,512]{1,0:T(8,128)(2,1)S(1)} %get-tuple-element.44), channel_id=1, source_target_pairs={{0,2},{1,3},{2,0},{3,1},{4,6},{5,7},{6,4},{7,5},{8,10},{9,11},{10,... | collective-permute-start | bytes 983048 | tf_op jit(solution)/shard_map/ppermute | solution.py:17
  28.4 22.5 %collective-permute-start.14 = (bf16[640,512]{1,0:T(8,128)(2,1)S(1)}, bf16[640,512]{1,0:T(8,128)(2,1)S(1)}, u32[]{:S(2)}, u32[]{:S(2)}) collective-permute-start(bf16[640,512]{1,0:T(8,128)(2,1)S(1)} %shard_map.153.own), channel_id=1, source_target_pairs={{0,1},{1,0},{2,3},{3,2},{4,5},{5,4},{6,7},{7,6},{8,9},{9,8},{10,11... | collective-permute-start | bytes 1966088 | tf_op jit(solution)/shard_map/ppermute | solution.py:17
  29.4 7.4 %collective-permute-start = (bf16[256,384]{1,0:T(8,128)(2,1)S(1)}, bf16[256,384]{1,0:T(8,128)(2,1)S(1)}, u32[]{:S(2)}, u32[]{:S(2)}) collective-permute-start(bf16[256,384]{1,0:T(8,128)(2,1)S(1)} %shard_map.149), channel_id=1, source_target_pairs={{0,4},{4,0},{8,12},{12,8},{16,20},{20,16},{24,28},{28,24},{1,5},{5... | collective-permute-start | bytes 589832 | tf_op jit(solution)/shard_map/ppermute | solution.py:17
  30.1 19.9 %collective-permute-start.15 = (bf16[320,512]{1,0:T(8,128)(2,1)S(1)}, bf16[320,512]{1,0:T(8,128)(2,1)S(1)}, u32[]{:S(2)}, u32[]{:S(2)}) collective-permute-start(bf16[320,512]{1,0:T(8,128)(2,1)S(1)} %get-tuple-element.45), channel_id=1, source_target_pairs={{0,2},{1,3},{2,0},{3,1},{4,6},{5,7},{6,4},{7,5},{8,10},{9,11},{10,... | collective-permute-start | bytes 983048 | tf_op jit(solution)/shard_map/ppermute | solution.py:17
  34.9 15.9 %collective-permute-start.20 = (bf16[320,512]{1,0:T(8,128)(2,1)S(1)}, bf16[320,512]{1,0:T(8,128)(2,1)S(1)}, u32[]{:S(2)}, u32[]{:S(2)}) collective-permute-start(bf16[320,512]{1,0:T(8,128)(2,1)S(1)} %collective-permute-done.19.far), channel_id=1, source_target_pairs={{0,1},{1,0},{2,3},{3,2},{4,5},{5,4},{6,7},{7,6},{8,9},{9,8},{10,11... | collective-permute-start | bytes 983048 | tf_op jit(solution)/shard_map/ppermute | solution.py:17
  37.9 12.3 %collective-permute-start.1 = (bf16[512,256]{1,0:T(8,128)(2,1)S(1)}, bf16[512,256]{1,0:T(8,128)(2,1)S(1)}, u32[]{:S(2)}, u32[]{:S(2)}) collective-permute-start(bf16[512,256]{1,0:T(8,128)(2,1)S(1)} %get-tuple-element.24.own_ref), channel_id=1, source_target_pairs={{0,8},{4,12},{8,16},{12,20},{16,24},{20,28},{1,9},{5,13},{9,17},{1... | collective-permute-start | bytes 786440 | tf_op jit(solution)/shard_map/ppermute | solution.py:30
  44.4 16.9 %collective-permute-start.2 = (bf16[512,256]{1,0:T(8,128)(2,1)S(1)}, bf16[512,256]{1,0:T(8,128)(2,1)S(1)}, u32[]{:S(2)}, u32[]{:S(2)}) collective-permute-start(bf16[512,256]{1,0:T(8,128)(2,1)S(1)} %get-tuple-element.24.own_ref), channel_id=1, source_target_pairs={{0,16},{4,20},{8,24},{12,28},{1,17},{5,21},{9,25},{13,29},{2,18},{... | collective-permute-start | bytes 786440 | tf_op jit(solution)/shard_map/ppermute | solution.py:30
  50.1 6.2 %collective-permute-start.16 = (bf16[320,512]{1,0:T(8,128)(2,1)S(1)}, bf16[320,512]{1,0:T(8,128)(2,1)S(1)}, u32[]{:S(2)}, u32[]{:S(2)}) collective-permute-start(bf16[320,512]{1,0:T(8,128)(2,1)S(1)} %collective-permute-done.15.far), channel_id=1, source_target_pairs={{0,1},{1,0},{2,3},{3,2},{4,5},{5,4},{6,7},{7,6},{8,9},{9,8},{10,11... | collective-permute-start | bytes 983048 | tf_op jit(solution)/shard_map/ppermute | solution.py:17
  50.2 11.1 %collective-permute-start.3 = (bf16[512,256]{1,0:T(8,128)(2,1)S(1)}, bf16[512,256]{1,0:T(8,128)(2,1)S(1)}, u32[]{:S(2)}, u32[]{:S(2)}) collective-permute-start(bf16[512,256]{1,0:T(8,128)(2,1)S(1)} %collective-permute-done.1.rest_0_), channel_id=1, source_target_pairs={{8,24},{12,28},{9,25},{13,29},{10,26},{14,30},{11,27},{15,31}} | collective-permute-start | bytes 786440 | tf_op jit(solution)/shard_map/ppermute | solution.py:30
  55.8 14.8 %collective-permute-start.21 = (bf16[320,1024]{1,0:T(8,128)(2,1)S(1)}, bf16[320,1024]{1,0:T(8,128)(2,1)S(1)}, u32[]{:S(2)}, u32[]{:S(2)}) collective-permute-start(bf16[320,1024]{1,0:T(8,128)(2,1)S(1)} %get-tuple-element.43), channel_id=1, source_target_pairs={{0,1},{1,0},{2,3},{3,2},{4,5},{5,4},{6,7},{7,6},{8,9},{9,8},{10,11... | collective-permute-start | bytes 1966088 | tf_op jit(solution)/shard_map/ppermute | solution.py:17
  61.2 11.1 %collective-permute-start.17 = (bf16[320,1024]{1,0:T(8,128)(2,1)S(1)}, bf16[320,1024]{1,0:T(8,128)(2,1)S(1)}, u32[]{:S(2)}, u32[]{:S(2)}) collective-permute-start(bf16[320,1024]{1,0:T(8,128)(2,1)S(1)} %get-tuple-element.41), channel_id=1, source_target_pairs={{0,1},{1,0},{2,3},{3,2},{4,5},{5,4},{6,7},{7,6},{8,9},{9,8},{10,11... | collective-permute-start | bytes 1966088 | tf_op jit(solution)/shard_map/ppermute | solution.py:17
  65.5 4.5 %collective-permute-start.4 = (bf16[256,128]{1,0:T(8,128)(2,1)S(1)}, bf16[256,128]{1,0:T(8,128)(2,1)S(1)}, u32[]{:S(2)}, u32[]{:S(2)}) collective-permute-start(bf16[256,128]{1,0:T(8,128)(2,1)S(1)} %get-tuple-element.26), channel_id=1, source_target_pairs={{0,4},{4,0},{8,12},{12,8},{16,20},{20,16},{24,28},{28,24},{1,5},{5... | collective-permute-start | bytes 196616 | tf_op jit(solution)/shard_map/ppermute | solution.py:17
  70.5 27.7 %collective-permute-start.5 = (bf16[128,2048]{1,0:T(8,128)(2,1)S(1)}, bf16[128,2048]{1,0:T(8,128)(2,1)S(1)}, u32[]{:S(2)}, u32[]{:S(2)}) collective-permute-start(bf16[128,2048]{1,0:T(8,128)(2,1)S(1)} %get-tuple-element.28), channel_id=1, source_target_pairs={{0,1},{1,0},{2,3},{3,2},{4,5},{5,4},{6,7},{7,6},{8,9},{9,8},{10,11... | collective-permute-start | bytes 1572872 | tf_op jit(solution)/shard_map/ppermute | solution.py:17
  70.7 10.6 %collective-permute-start.22 = (bf16[320,512]{1,0:T(8,128)(2,1)S(1)}, bf16[320,512]{1,0:T(8,128)(2,1)S(1)}, u32[]{:S(2)}, u32[]{:S(2)}) collective-permute-start(bf16[320,512]{1,0:T(8,128)(2,1)S(1)} %add_convert_fusion), channel_id=1, source_target_pairs={{0,2},{1,3},{2,0},{3,1},{4,6},{5,7},{6,4},{7,5},{8,10},{9,11},{10,... | collective-permute-start | bytes 983048 | tf_op jit(solution)/shard_map/ppermute | solution.py:17
  72.4 15.5 %collective-permute-start.18 = (bf16[320,512]{1,0:T(8,128)(2,1)S(1)}, bf16[320,512]{1,0:T(8,128)(2,1)S(1)}, u32[]{:S(2)}, u32[]{:S(2)}) collective-permute-start(bf16[320,512]{1,0:T(8,128)(2,1)S(1)} %add_convert_fusion.1), channel_id=1, source_target_pairs={{0,2},{1,3},{2,0},{3,1},{4,6},{5,7},{6,4},{7,5},{8,10},{9,11},{10,... | collective-permute-start | bytes 983048 | tf_op jit(solution)/shard_map/ppermute | solution.py:17
  88.8 26.6 %all-to-all-start = ((bf16[8,80,512]{2,1,0:T(8,128)(2,1)}), bf16[8,80,512]{2,1,0:T(8,128)(2,1)S(1)}, u32[]{:S(2)}, u32[]{:S(2)}) async-start(bf16[8,80,512]{2,1,0:T(8,128)(2,1)} %bitcast.9), calls=%async_computation | async-start | bytes 1310720 | tf_op jit(solution)/shard_map/all_to_all | solution.py:491
  98.3 7.7 %collective-permute-start.6 = (bf16[64,2048]{1,0:T(8,128)(2,1)S(1)}, bf16[64,2048]{1,0:T(8,128)(2,1)S(1)}, u32[]{:S(2)}, u32[]{:S(2)}) collective-permute-start(bf16[64,2048]{1,0:T(8,128)(2,1)S(1)} %add_convert_fusion.3), channel_id=1, source_target_pairs={{0,2},{1,3},{2,0},{3,1},{4,6},{5,7},{6,4},{7,5},{8,10},{9,11},{10,... | collective-permute-start | bytes 786440 | tf_op jit(solution)/shard_map/ppermute | solution.py:17
  (7 other events, 37.3 us)

commit v4 on v3

--- a/solution.py
+++ b/solution.py
@@ -288,10 +288,11 @@
 
 
 def ffn_kernel(
-    first, order_ref, own, near, far, cross, gate_w, up_w, down_w, keep_ref, send_ref
+    index, order_ref, own, near, far, cross, gate_w, up_w, down_w, keep_ref, send_ref
 ):
     rows, cols = far.shape
-    pieces = (own[first : first + rows, :], near[first : first + rows, :], far[...], cross[...])
+    mine = pl.ds(pl.multiple_of(order_ref[8 + index], rows), rows)
+    pieces = (own[mine, :], near[mine, :], far[...], cross[...])
 
     def part(k):
         return pl.ds(pl.multiple_of(order_ref[k] * cols, cols), cols)
@@ -315,12 +316,12 @@
             ).astype(BF16)
 
 
-def ffn(order, first, own, near, far, cross, weights):
+def ffn(order, index, own, near, far, cross, weights):
     rows, cols = far.shape
     width, units = weights[0].shape
     vmem = pl.BlockSpec(memory_space=pltpu.VMEM)
     return pl.pallas_call(
-        functools.partial(ffn_kernel, first),
+        functools.partial(ffn_kernel, index),
         in_specs=[pl.BlockSpec(memory_space=pltpu.SMEM)] + [vmem] * 7,
         out_specs=[vmem, vmem],
         out_shape=[jax.ShapeDtypeStruct((rows, 2 * cols), BF16)] * 2,
@@ -341,40 +342,39 @@
     )
 
 
-def total_kernel(first, keep_ref, got_ref, over_ref, *rest):
-    out_ref, part, sem = rest[-3:]
-    rows, cols = part.shape
+def total_kernel(here_ref, keep_ref, got_ref, over_ref, *rest):
+    outs, part = rest[:-1], rest[-1]
+    cols = over_ref.shape[1]
+    capacity = outs[0].shape[0]
     part[...] = (
         keep_ref[:, :cols].astype(F32) + got_ref[:, :cols].astype(F32) + over_ref[...].astype(F32)
-    ).astype(BF16)
-    copy = pltpu.make_async_copy(part, out_ref.at[first : first + rows, :], sem)
-    copy.start()
-    copy.wait()
-
-
-def total(slots, first, keep, got, over, held=None):
-    rows, cols = over.shape
-    hbm = pl.BlockSpec(memory_space=pltpu.HBM)
-    operands = [keep, got, over] + ([] if held is None else [held])
-    return pl.pallas_call(
-        functools.partial(total_kernel, first),
-        out_shape=jax.ShapeDtypeStruct((slots, cols), BF16),
-        in_specs=[VMEM] * 3 + [hbm] * (len(operands) - 3),
-        out_specs=hbm,
-        scratch_shapes=[pltpu.VMEM((rows, cols), BF16), pltpu.SemaphoreType.DMA],
-        input_output_aliases={} if held is None else {3: 0},
-        compiler_params=pltpu.CompilerParams(vmem_limit_bytes=8 * 1024 * 1024),
-        cost_estimate=pl.CostEstimate(
-            flops=4 * rows * cols, bytes_accessed=16 * rows * cols, transcendentals=0
-        ),
-        name="total",
-    )(*operands)
-
-
-def combine_weights(ids_across, weight_across, capacity):
-    experts = lax.axis_size("ep")
+    )
+    mine = lax.rem(ep_of(here_ref), len(outs))
+    for k, out_ref in enumerate(outs):
+        out_ref[...] = part[half(mine ^ k, capacity), :].astype(BF16)
+
+
+def mix_kernel(weight_ref, *rest):
+    pieces, out_ref, held = rest[:-2], rest[-2], rest[-1]
+    count = pieces[0].shape[0]
+    for k, piece in enumerate(pieces):
+        held[k * count : (k + 1) * count, :] = piece[...]
+    left = weight_ref[...]
+    sums = None
+    for _ in range(3):
+        high = left.astype(BF16)
+        left = left - high.astype(F32)
+        one = lax.dot_general(
+            high, held[...], (((0,), (0,)), ((), ())), preferred_element_type=F32
+        )
+        sums = one if sums is None else sums + one
+    out_ref[...] = sums.astype(BF16)
+
+
+def combine_weights(ids_across, weight_across, capacity, numbers):
+    experts = numbers.shape[0]
     rows = ids_across.shape[1]
-    numbers = jnp.arange(experts, dtype=jnp.int32)[:, None]
+    numbers = numbers[:, None]
     first = ids_across[0:1] == numbers
     second = ids_across[1:2] == numbers
     named = first | second
@@ -436,8 +436,13 @@
     near = swap(own, "tp", 1)
     halves = 2
     part = slots // halves
-    order = jnp.array([0, 1, 2, 3, 1, 3, 0, 2], jnp.int32) ^ place
-    fars = [swap(own[i * part : (i + 1) * part], "tp", 2) for i in range(halves)]
+    at = lax.axis_index("ep").astype(jnp.int32)
+    side = at // (experts // 2)
+    firsts = [(1 - side) * part, side * part]
+    order = jnp.concatenate(
+        [jnp.array([0, 1, 2, 3, 1, 3, 0, 2], jnp.int32) ^ place, jnp.stack(firsts)]
+    )
+    fars = [swap(lax.dynamic_slice_in_dim(own, first, part), "tp", 2) for first in firsts]
     if small:
         blocks = []
         for k in range(1, experts // 2):
@@ -446,7 +451,7 @@
     mine, gots = [], []
     for i in range(halves):
         cross = swap(fars[i], "tp", 1)
-        keep, send = ffn(order, i * part, own, near, fars[i], cross, weights)
+        keep, send = ffn(order, i, own, near, fars[i], cross, weights)
         got = swap(send, "tp", 1)
         across = (keep[:, cols:].astype(F32) + got[:, cols:].astype(F32)).astype(BF16)
         gots.append(swap(across, "tp", 2))
@@ -485,20 +490,44 @@
             share.reshape(lax.axis_size("tp"), -1, share.shape[1]), "tp", 0, 0, tiled=True
         )
         mixer_out = jnp.sum(parts.astype(F32), axis=0).astype(BF16)
-    summed = None
+    steps = jnp.arange(experts, dtype=jnp.int32)
+    if not small:
+        summed = jnp.zeros((slots, cols), BF16)
+        for (keep, got), over, first in zip(mine, gots, firsts):
+            one = keep[:, :cols].astype(F32) + got[:, :cols].astype(F32) + over.astype(F32)
+            summed = lax.dynamic_update_slice_in_dim(summed, one.astype(BF16), first, 0)
+        returned = lax.all_to_all(
+            summed.reshape(experts, capacity, cols), "ep", split_axis=0, concat_axis=0, tiled=True
+        ).reshape(slots, cols)
+        mixed = lax.dot_general(
+            combine_weights(ids_across, weight_across, capacity, steps),
+            returned.astype(F32),
+            (((0,), (0,)), ((), ())),
+            precision=lax.Precision.HIGHEST,
+            preferred_element_type=F32,
+        )
+        return (mixer_out, mixed.astype(BF16))
+    count = experts // 2
+    pieces = [None] * experts
     for i, ((keep, got), over) in enumerate(zip(mine, gots)):
-        summed = total(slots, i * part, keep, got, over, summed)
-    returned = lax.all_to_all(
-        summed.reshape(experts, capacity, cols), "ep", split_axis=0, concat_axis=0, tiled=True
-    ).reshape(slots, cols)
-    mixed = lax.dot_general(
-        combine_weights(ids_across, weight_across, capacity),
-        returned.astype(F32),
-        (((0,), (0,)), ((), ())),
-        precision=lax.Precision.HIGHEST,
-        preferred_element_type=F32,
-    )
-    return (mixer_out, mixed.astype(BF16))
+        outs = local(
+            total_kernel,
+            [(capacity, cols)] * count,
+            (here, keep, got, over),
+            scratch=[pltpu.VMEM((part, cols), F32)],
+        )
+        for k, piece in enumerate(outs):
+            k += (1 - i) * count
+            pieces[k] = swap(piece, "ep", k) if k else piece
+    (mixed,) = local(
+        mix_kernel,
+        [(rows_b, cols)],
+        (combine_weights(ids_across, weight_across, capacity, at ^ steps), *pieces),
+        smem=0,
+        scratch=[pltpu.VMEM((slots, cols), BF16)],
+        flops=6 * slots * rows_b * cols,
+    )
+    return (mixer_out, mixed)
 
 
 def solution(mesh):

time: 117 us -> 112 us (0.957)
  waiting for transfers between devices: 47.1 us -> 25.6 us
  starting transfers between devices: 40.2 us -> 54 us
  other arithmetic: 1.13 us -> 3.16 us
  local copies, waits for them, and re-layouts: 0.98 us -> 2.56 us
  matrix products: 1.63 us -> 0.13 us
    ppermute x20 -> x27, starting transfers between devices: 22.2 us -> 45.4 us  [swap(): return lax.ppermute(x, axis, [(i, i ^ mask) for i in range(count)])]
    ppermute x20 -> x27, waiting for transfers between devices: 38.5 us -> 21 us  [swap(): return lax.ppermute(x, axis, [(i, i ^ mask) for i in range(count)])]
    all_to_all x1 -> x0, starting transfers between devices: 9.45 us -> none  [shards(): lax.all_to_all(summed.reshape(experts, capacity, cols), 'ep', split_axis=...]
    all_to_all x1 -> x0, waiting for transfers between devices: 8.58 us -> none  [shards(): lax.all_to_all(summed.reshape(experts, capacity, cols), 'ep', split_axis=...]
    ppermute x3, waiting for transfers between devices: 0.01 us -> 4.6 us  [onward(): lax.ppermute(x, axis, [(i, i + step) for i in range(first, count - step)])]
    pallas_call x5 -> x8, Pallas kernels: 6.79 us -> 8.69 us  [local(): pl.pallas_call(kernel, out_shape=[jax.ShapeDtypeStruct(shape, BF16) for s...]
    pallas_call x4 -> x2, Pallas kernels: 11.5 us -> 9.71 us  [ffn(): pl.pallas_call(functools.partial(ffn_kernel, index), in_specs=[pl.BlockSp...]
    dot_general x1 -> x0, matrix products: 1.49 us -> none  [shards(): lax.dot_general(combine_weights(ids_across, weight_across, capacity), ret...]
  transfers between devices with their start and end apart: 24 -> 30, of which waited for: 10 -> 8; matrix products, arithmetic and copies ran while one was open for 1% -> 4% of each run, Pallas kernels for 19% -> 18%
where the time goes in v4:
time: 112 us; the launch traced here: 111 us
  starting transfers between devices  54 us (48%)
  waiting for transfers between devices  25.6 us (23%)
  Pallas kernels  25.1 us (22%)
  other arithmetic  3.16 us (3%)
  local copies, waits for them, and re-layouts  2.56 us (2%)
    ppermute x27, starting transfers between devices, swap(): return lax.ppermute(x, axis, [(i, i ^ mask) for i in range(count)])  45.4 us
    ppermute x27, waiting for transfers between devices, swap(): return lax.ppermute(x, axis, [(i, i ^ mask) for i in range(count)])  21 us
    pallas_call x2, Pallas kernels, ffn(): pl.pallas_call(functools.partial(ffn_kernel, index), in_specs=[pl.BlockSp...  9.71 us
    pallas_call x8, Pallas kernels, local(): pl.pallas_call(kernel, out_shape=[jax.ShapeDtypeStruct(shape, BF16) for s...  8.69 us
    ppermute x3, starting transfers between devices, onward(): lax.ppermute(x, axis, [(i, i + step) for i in range(first, count - step)])  8.56 us
    ppermute x3, waiting for transfers between devices, onward(): lax.ppermute(x, axis, [(i, i + step) for i in range(first, count - step)])  4.6 us
    pallas_call x1, Pallas kernels, fetched(): pl.pallas_call(fetch_kernel, in_specs=[hbm] * 3, out_specs=[vmem] * 3, ou...  4.33 us
    pallas_call x1, Pallas kernels, dispatched(): pl.pallas_call(functools.partial(dispatch_kernel, experts, capacity), out...  2.42 us
  transfers between devices with their start and end apart: 30, of which 8 were waited for; matrix products, arithmetic and copies ran while one was open for 4% of the time, Pallas kernels for 18%

profile of v4, /device:TPU:0, one launch (start us, length us, event | category | flops | bytes accessed | tf_op | source)
XLA Modules:
  0.0 111.4 jit_solution(17865637532098249859)
XLA Ops:
  0.7 2.4 %dispatch.1 = (bf16[80,512]{1,0:T(8,128)(2,1)}, bf16[80,512]{1,0:T(8,128)(2,1)}, bf16[80,512]{1,0:T(8,128)(2,1)}, bf16[80,512]{1,0:T(8,128)(2,1)}, bf16[80,512]{...) custom-call(s32[1]{0:T(128)} %bitcast.place_ref.here_ref, ...), custom_call_target="tpu_custom_call" | custom-call | flops 125829120 | bytes 786432 | tf_op jit(solution)/shard_map/dispatch/pallas_call | solution.py:237
  3.1 4.1 %collective-permute-start.10 = (bf16[80,512]{1,0:T(8,128)(2,1)}, bf16[80,512]{1,0:T(8,128)(2,1)S(1)}, u32[]{:S(2)}, u32[]{:S(2)}) collective-permute-start(bf16[80,512]{1,0:T(8,128)(2,1)} %get-tuple-element.41), channel_id=1, source_target_pairs={{0,16},{4,20},{8,24},{12,28},{16,0},{20,4},{24,8},{28,12},{1,17},{... | collective-permute-start | bytes 245768 | tf_op jit(solution)/shard_map/ppermute | solution.py:17
  8.4 3.6 %collective-permute-start.12 = (bf16[80,512]{1,0:T(8,128)(2,1)}, bf16[80,512]{1,0:T(8,128)(2,1)S(1)}, u32[]{:S(2)}, u32[]{:S(2)}) collective-permute-start(bf16[80,512]{1,0:T(8,128)(2,1)} %get-tuple-element.43), channel_id=1, source_target_pairs={{0,24},{4,28},{8,16},{12,20},{16,8},{20,12},{24,0},{28,4},{1,25},{... | collective-permute-start | bytes 245768 | tf_op jit(solution)/shard_map/ppermute | solution.py:17
  13.1 1.7 %collective-permute-start = (bf16[256,384]{1,0:T(8,128)(2,1)S(1)}, bf16[256,384]{1,0:T(8,128)(2,1)S(1)}, u32[]{:S(2)}, u32[]{:S(2)}) collective-permute-start(bf16[256,384]{1,0:T(8,128)(2,1)S(1)} %shard_map.149), channel_id=1, source_target_pairs={{0,4},{4,0},{8,12},{12,8},{16,20},{20,16},{24,28},{28,24},{1,5},{5... | collective-permute-start | bytes 589832 | tf_op jit(solution)/shard_map/ppermute | solution.py:17
  16.3 1.9 %collective-permute-start.7 = (bf16[80,512]{1,0:T(8,128)(2,1)}, bf16[80,512]{1,0:T(8,128)(2,1)S(1)}, u32[]{:S(2)}, u32[]{:S(2)}) collective-permute-start(bf16[80,512]{1,0:T(8,128)(2,1)} %get-tuple-element.38), channel_id=1, source_target_pairs={{0,4},{4,0},{8,12},{12,8},{16,20},{20,16},{24,28},{28,24},{1,5},{5... | collective-permute-start | bytes 245768 | tf_op jit(solution)/shard_map/ppermute | solution.py:17
  18.3 2.1 %collective-permute-done.11.refs_5_ = bf16[80,512]{1,0:T(8,128)(2,1)S(1)} collective-permute-done((bf16[80,512]{1,0:T(8,128)(2,1)}, bf16[80,512]{1,0:T(8,128)(2,1)S(1)}, u32[]{:S(2)}, u32[]{:S(2)}) %collective-permute-start.11) | collective-permute-done | bytes 81952 | tf_op jit(solution)/shard_map/ppermute | solution.py:17
  20.3 2.3 %collective-permute-start.9 = (bf16[80,512]{1,0:T(8,128)(2,1)}, bf16[80,512]{1,0:T(8,128)(2,1)S(1)}, u32[]{:S(2)}, u32[]{:S(2)}) collective-permute-start(bf16[80,512]{1,0:T(8,128)(2,1)} %get-tuple-element.40), channel_id=1, source_target_pairs={{0,12},{4,8},{8,4},{12,0},{16,28},{20,24},{24,20},{28,16},{1,13},{... | collective-permute-start | bytes 245768 | tf_op jit(solution)/shard_map/ppermute | solution.py:17
  22.7 2.3 %collective-permute-done.7.refs_1_ = bf16[80,512]{1,0:T(8,128)(2,1)S(1)} collective-permute-done((bf16[80,512]{1,0:T(8,128)(2,1)}, bf16[80,512]{1,0:T(8,128)(2,1)S(1)}, u32[]{:S(2)}, u32[]{:S(2)}) %collective-permute-start.7) | collective-permute-done | bytes 81952 | tf_op jit(solution)/shard_map/ppermute | solution.py:17
  27.9 3.9 %collective-permute-start.1 = (bf16[512,256]{1,0:T(8,128)(2,1)S(1)}, bf16[512,256]{1,0:T(8,128)(2,1)S(1)}, u32[]{:S(2)}, u32[]{:S(2)}) collective-permute-start(bf16[512,256]{1,0:T(8,128)(2,1)S(1)} %get-tuple-element.32.own_ref), channel_id=1, source_target_pairs={{0,8},{4,12},{8,16},{12,20},{16,24},{20,28},{1,9},{5,13},{9,17},{1... | collective-permute-start | bytes 786440 | tf_op jit(solution)/shard_map/ppermute | solution.py:30
  32.0 1.6 %collective-permute-start.22 = (bf16[320,512]{1,0:T(8,128)(2,1)S(1)}, bf16[320,512]{1,0:T(8,128)(2,1)S(1)}, u32[]{:S(2)}, u32[]{:S(2)}) collective-permute-start(bf16[320,512]{1,0:T(8,128)(2,1)S(1)} %get-tuple-element.60), channel_id=1, source_target_pairs={{0,2},{1,3},{2,0},{3,1},{4,6},{5,7},{6,4},{7,5},{8,10},{9,11},{10,... | collective-permute-start | bytes 983048 | tf_op jit(solution)/shard_map/ppermute | solution.py:17
  33.6 3.9 %collective-permute-start.2 = (bf16[512,256]{1,0:T(8,128)(2,1)S(1)}, bf16[512,256]{1,0:T(8,128)(2,1)S(1)}, u32[]{:S(2)}, u32[]{:S(2)}) collective-permute-start(bf16[512,256]{1,0:T(8,128)(2,1)S(1)} %get-tuple-element.32.own_ref), channel_id=1, source_target_pairs={{0,16},{4,20},{8,24},{12,28},{1,17},{5,21},{9,25},{13,29},{2,18},{... | collective-permute-start | bytes 786440 | tf_op jit(solution)/shard_map/ppermute | solution.py:30
  39.2 4.6 %collective-permute-done.2.rest_1_ = bf16[512,256]{1,0:T(8,128)(2,1)S(1)} collective-permute-done((bf16[512,256]{1,0:T(8,128)(2,1)S(1)}, bf16[512,256]{1,0:T(8,128)(2,1)S(1)}, u32[]{:S(2)}, u32[]{:S(2)}) %collective-permute-start.2) | collective-permute-done | bytes 262176 | tf_op jit(solution)/shard_map/ppermute | solution.py:30
  43.8 4.2 %shard_map.151 = (bf16[256,128]{1,0:T(8,128)(2,1)S(1)}, bf16[256,128]{1,0:T(8,128)(2,1)S(1)}) custom-call(s32[1]{0:T(128)} %bitcast.place_ref.here_ref, f32[2]{0:T(128)S(1)} %copy-done.2, bf16[512,128]{1,0:T(8,128)(2,1)S(1)} %get-tuple-element.31.query_ref, bf16[512,256]{1,0:T(8,128)(2,1)S(1)} %get-tuple-element.32.own_ref, ...), custom_call_target="tpu_custom_call" | custom-call | flops 1073741824 | bytes 1179910 | tf_op jit(solution)/shard_map/pallas_call | solution.py:186
  48.1 1.5 %collective-permute-start.4 = (bf16[256,128]{1,0:T(8,128)(2,1)S(1)}, bf16[256,128]{1,0:T(8,128)(2,1)S(1)}, u32[]{:S(2)}, u32[]{:S(2)}) collective-permute-start(bf16[256,128]{1,0:T(8,128)(2,1)S(1)} %get-tuple-element.34), channel_id=1, source_target_pairs={{0,4},{4,0},{8,12},{12,8},{16,20},{20,16},{24,28},{28,24},{1,5},{5... | collective-permute-start | bytes 196616 | tf_op jit(solution)/shard_map/ppermute | solution.py:17
  49.6 4.3 %fetch.1 = (bf16[2048,896]{1,0:T(8,128)(2,1)S(1)}, bf16[2048,896]{1,0:T(8,128)(2,1)S(1)}, bf16[896,2048]{1,0:T(8,128)(2,1)S(1)}) custom-call(bf16[1,2048,896]{2,1,0:T(8,128)(2,1)} %gate.1, bf16[1,2048,896]{2,1,0:T(8,128)(2,1)} %up.1, bf16[1,896,2048]{2,1,0:T(8,128)(2,1)} %down.1), custom_call_target="tpu_custom_call" | custom-call | flops 550502400 | bytes 11010048 | tf_op jit(solution)/shard_map/fetch/pallas_call | solution.py:274
  55.1 4.9 %ffn.3 = (bf16[320,1024]{1,0:T(8,128)(2,1)S(1)}, bf16[320,1024]{1,0:T(8,128)(2,1)S(1)}) custom-call(s32[10]{0:T(128)S(1)} %pad_add_fusion.order_ref, bf16[640,512]{1,0:T(8,128)(2,1)S(1)} %shard_map.153.own, bf16[640,512]{1,0:T(8,128)(2,1)S(1)} %collective-permute-done.14.near, bf16[320,512]{1,0:T(8,128)(2,1)S(1)} %collective-permute-done.22.far, ...), custom_call_target="tpu_custom_call" | custom-call | flops 3523215360 | bytes 13631488 | tf_op jit(solution)/shard_map/ffn/pallas_call | solution.py:323
  60.1 4.9 %ffn.2 = (bf16[320,1024]{1,0:T(8,128)(2,1)S(1)}, bf16[320,1024]{1,0:T(8,128)(2,1)S(1)}) custom-call(s32[10]{0:T(128)S(1)} %pad_add_fusion.order_ref, bf16[640,512]{1,0:T(8,128)(2,1)S(1)} %shard_map.153.own, bf16[640,512]{1,0:T(8,128)(2,1)S(1)} %collective-permute-done.14.near, bf16[320,512]{1,0:T(8,128)(2,1)S(1)} %collective-permute-done.15.far, ...), custom_call_target="tpu_custom_call" | custom-call | flops 3523215360 | bytes 13631488 | tf_op jit(solution)/shard_map/ffn/pallas_call | solution.py:323
  66.9 1.6 %collective-permute-start.25 = (bf16[320,512]{1,0:T(8,128)(2,1)S(1)}, bf16[320,512]{1,0:T(8,128)(2,1)S(1)}, u32[]{:S(2)}, u32[]{:S(2)}) collective-permute-start(bf16[320,512]{1,0:T(8,128)(2,1)S(1)} %add_convert_fusion), channel_id=1, source_target_pairs={{0,2},{1,3},{2,0},{3,1},{4,6},{5,7},{6,4},{7,5},{8,10},{9,11},{10,... | collective-permute-start | bytes 983048 | tf_op jit(solution)/shard_map/ppermute | solution.py:17
  69.3 13.4 %collective-permute-done.25.over_ref = bf16[320,512]{1,0:T(8,128)(2,1)S(1)} collective-permute-done((bf16[320,512]{1,0:T(8,128)(2,1)S(1)}, bf16[320,512]{1,0:T(8,128)(2,1)S(1)}, u32[]{:S(2)}, u32[]{:S(2)}) %collective-permute-start.25) | collective-permute-done | bytes 327712 | tf_op jit(solution)/shard_map/ppermute | solution.py:17
  82.9 5.0 %collective-permute-start.26 = (bf16[80,512]{1,0:T(8,128)(2,1)S(1)}, bf16[80,512]{1,0:T(8,128)(2,1)S(1)}, u32[]{:S(2)}, u32[]{:S(2)}) collective-permute-start(bf16[80,512]{1,0:T(8,128)(2,1)S(1)} %get-tuple-element.56), channel_id=1, source_target_pairs={{0,16},{4,20},{8,24},{12,28},{16,0},{20,4},{24,8},{28,12},{1,17},{... | collective-permute-start | bytes 245768 | tf_op jit(solution)/shard_map/ppermute | solution.py:17
  88.7 11.4 %collective-permute-start.28 = (bf16[80,512]{1,0:T(8,128)(2,1)S(1)}, bf16[80,512]{1,0:T(8,128)(2,1)S(1)}, u32[]{:S(2)}, u32[]{:S(2)}) collective-permute-start(bf16[80,512]{1,0:T(8,128)(2,1)S(1)} %get-tuple-element.58), channel_id=1, source_target_pairs={{0,24},{4,28},{8,16},{12,20},{16,8},{20,12},{24,0},{28,4},{1,25},{... | collective-permute-start | bytes 245768 | tf_op jit(solution)/shard_map/ppermute | solution.py:17
  100.1 2.5 %collective-permute-start.29 = (bf16[80,512]{1,0:T(8,128)(2,1)S(1)}, bf16[80,512]{1,0:T(8,128)(2,1)S(1)}, u32[]{:S(2)}, u32[]{:S(2)}) collective-permute-start(bf16[80,512]{1,0:T(8,128)(2,1)S(1)} %get-tuple-element.59), channel_id=1, source_target_pairs={{0,28},{4,24},{8,20},{12,16},{16,12},{20,8},{24,4},{28,0},{1,29},{... | collective-permute-start | bytes 245768 | tf_op jit(solution)/shard_map/ppermute | solution.py:17
  104.0 2.4 %collective-permute-start.21 = (bf16[80,512]{1,0:T(8,128)(2,1)S(1)}, bf16[80,512]{1,0:T(8,128)(2,1)S(1)}, u32[]{:S(2)}, u32[]{:S(2)}) collective-permute-start(bf16[80,512]{1,0:T(8,128)(2,1)S(1)} %get-tuple-element.53), channel_id=1, source_target_pairs={{0,12},{4,8},{8,4},{12,0},{16,28},{20,24},{24,20},{28,16},{1,13},{... | collective-permute-start | bytes 245768 | tf_op jit(solution)/shard_map/ppermute | solution.py:17
  106.4 1.7 %add_convert_fusion.2 = bf16[64,2048]{1,0:T(8,128)(2,1)} fusion(bf16[64,2048]{1,0:T(8,128)(2,1)} %collective-permute-done.6, bf16[128,2048]{1,0:T(8,128)(2,1)S(1)} %collective-permute-done.5, bf16[128,2048]{1,0:T(8,128)(2,1)S(1)} %get-tuple-element.35), kind=kLoop, calls=%fused_computation.5 | loop fusion | flops 786432 | bytes 1048576 | tf_op jit(solution)/shard_map/convert_element_type | solution.py:484
  (75 shorter events, 18.3 us)
Async XLA Ops:
  3.1 13.3 %collective-permute-start.10 = (bf16[80,512]{1,0:T(8,128)(2,1)}, bf16[80,512]{1,0:T(8,128)(2,1)S(1)}, u32[]{:S(2)}, u32[]{:S(2)}) collective-permute-start(bf16[80,512]{1,0:T(8,128)(2,1)} %get-tuple-element.41), channel_id=1, source_target_pairs={{0,16},{4,20},{8,24},{12,28},{16,0},{20,4},{24,8},{28,12},{1,17},{... | collective-permute-start | bytes 245768 | tf_op jit(solution)/shard_map/ppermute | solution.py:17
  7.2 13.2 %collective-permute-start.11 = (bf16[80,512]{1,0:T(8,128)(2,1)}, bf16[80,512]{1,0:T(8,128)(2,1)S(1)}, u32[]{:S(2)}, u32[]{:S(2)}) collective-permute-start(bf16[80,512]{1,0:T(8,128)(2,1)} %get-tuple-element.42), channel_id=1, source_target_pairs={{0,20},{4,16},{8,28},{12,24},{16,4},{20,0},{24,12},{28,8},{1,21},{... | collective-permute-start | bytes 245768 | tf_op jit(solution)/shard_map/ppermute | solution.py:17
  8.4 11.9 %collective-permute-start.12 = (bf16[80,512]{1,0:T(8,128)(2,1)}, bf16[80,512]{1,0:T(8,128)(2,1)S(1)}, u32[]{:S(2)}, u32[]{:S(2)}) collective-permute-start(bf16[80,512]{1,0:T(8,128)(2,1)} %get-tuple-element.43), channel_id=1, source_target_pairs={{0,24},{4,28},{8,16},{12,20},{16,8},{20,12},{24,0},{28,4},{1,25},{... | collective-permute-start | bytes 245768 | tf_op jit(solution)/shard_map/ppermute | solution.py:17
  12.0 10.6 %collective-permute-start.13 = (bf16[80,512]{1,0:T(8,128)(2,1)}, bf16[80,512]{1,0:T(8,128)(2,1)S(1)}, u32[]{:S(2)}, u32[]{:S(2)}) collective-permute-start(bf16[80,512]{1,0:T(8,128)(2,1)} %get-tuple-element.44), channel_id=1, source_target_pairs={{0,28},{4,24},{8,20},{12,16},{16,12},{20,8},{24,4},{28,0},{1,29},{... | collective-permute-start | bytes 245768 | tf_op jit(solution)/shard_map/ppermute | solution.py:17
  13.1 13.8 %collective-permute-start = (bf16[256,384]{1,0:T(8,128)(2,1)S(1)}, bf16[256,384]{1,0:T(8,128)(2,1)S(1)}, u32[]{:S(2)}, u32[]{:S(2)}) collective-permute-start(bf16[256,384]{1,0:T(8,128)(2,1)S(1)} %shard_map.149), channel_id=1, source_target_pairs={{0,4},{4,0},{8,12},{12,8},{16,20},{20,16},{24,28},{28,24},{1,5},{5... | collective-permute-start | bytes 589832 | tf_op jit(solution)/shard_map/ppermute | solution.py:17
  16.3 8.6 %collective-permute-start.7 = (bf16[80,512]{1,0:T(8,128)(2,1)}, bf16[80,512]{1,0:T(8,128)(2,1)S(1)}, u32[]{:S(2)}, u32[]{:S(2)}) collective-permute-start(bf16[80,512]{1,0:T(8,128)(2,1)} %get-tuple-element.38), channel_id=1, source_target_pairs={{0,4},{4,0},{8,12},{12,8},{16,20},{20,16},{24,28},{28,24},{1,5},{5... | collective-permute-start | bytes 245768 | tf_op jit(solution)/shard_map/ppermute | solution.py:17
  27.9 9.6 %collective-permute-start.1 = (bf16[512,256]{1,0:T(8,128)(2,1)S(1)}, bf16[512,256]{1,0:T(8,128)(2,1)S(1)}, u32[]{:S(2)}, u32[]{:S(2)}) collective-permute-start(bf16[512,256]{1,0:T(8,128)(2,1)S(1)} %get-tuple-element.32.own_ref), channel_id=1, source_target_pairs={{0,8},{4,12},{8,16},{12,20},{16,24},{20,28},{1,9},{5,13},{9,17},{1... | collective-permute-start | bytes 786440 | tf_op jit(solution)/shard_map/ppermute | solution.py:30
  32.0 7.3 %collective-permute-start.22 = (bf16[320,512]{1,0:T(8,128)(2,1)S(1)}, bf16[320,512]{1,0:T(8,128)(2,1)S(1)}, u32[]{:S(2)}, u32[]{:S(2)}) collective-permute-start(bf16[320,512]{1,0:T(8,128)(2,1)S(1)} %get-tuple-element.60), channel_id=1, source_target_pairs={{0,2},{1,3},{2,0},{3,1},{4,6},{5,7},{6,4},{7,5},{8,10},{9,11},{10,... | collective-permute-start | bytes 983048 | tf_op jit(solution)/shard_map/ppermute | solution.py:17
  33.6 21.5 %collective-permute-start.14 = (bf16[640,512]{1,0:T(8,128)(2,1)S(1)}, bf16[640,512]{1,0:T(8,128)(2,1)S(1)}, u32[]{:S(2)}, u32[]{:S(2)}) collective-permute-start(bf16[640,512]{1,0:T(8,128)(2,1)S(1)} %shard_map.153.own), channel_id=1, source_target_pairs={{0,1},{1,0},{2,3},{3,2},{4,5},{5,4},{6,7},{7,6},{8,9},{9,8},{10,11... | collective-permute-start | bytes 1966088 | tf_op jit(solution)/shard_map/ppermute | solution.py:17
  33.6 10.2 %collective-permute-start.2 = (bf16[512,256]{1,0:T(8,128)(2,1)S(1)}, bf16[512,256]{1,0:T(8,128)(2,1)S(1)}, u32[]{:S(2)}, u32[]{:S(2)}) collective-permute-start(bf16[512,256]{1,0:T(8,128)(2,1)S(1)} %get-tuple-element.32.own_ref), channel_id=1, source_target_pairs={{0,16},{4,20},{8,24},{12,28},{1,17},{5,21},{9,25},{13,29},{2,18},{... | collective-permute-start | bytes 786440 | tf_op jit(solution)/shard_map/ppermute | solution.py:30
  37.6 6.2 %collective-permute-start.3 = (bf16[512,256]{1,0:T(8,128)(2,1)S(1)}, bf16[512,256]{1,0:T(8,128)(2,1)S(1)}, u32[]{:S(2)}, u32[]{:S(2)}) collective-permute-start(bf16[512,256]{1,0:T(8,128)(2,1)S(1)} %collective-permute-done.1.rest_0_), channel_id=1, source_target_pairs={{8,24},{12,28},{9,25},{13,29},{10,26},{14,30},{11,27},{15,31}} | collective-permute-start | bytes 786440 | tf_op jit(solution)/shard_map/ppermute | solution.py:30
  38.4 15.6 %collective-permute-start.15 = (bf16[320,512]{1,0:T(8,128)(2,1)S(1)}, bf16[320,512]{1,0:T(8,128)(2,1)S(1)}, u32[]{:S(2)}, u32[]{:S(2)}) collective-permute-start(bf16[320,512]{1,0:T(8,128)(2,1)S(1)} %get-tuple-element.61), channel_id=1, source_target_pairs={{0,2},{1,3},{2,0},{3,1},{4,6},{5,7},{6,4},{7,5},{8,10},{9,11},{10,... | collective-permute-start | bytes 983048 | tf_op jit(solution)/shard_map/ppermute | solution.py:17
  39.2 15.9 %collective-permute-start.23 = (bf16[320,512]{1,0:T(8,128)(2,1)S(1)}, bf16[320,512]{1,0:T(8,128)(2,1)S(1)}, u32[]{:S(2)}, u32[]{:S(2)}) collective-permute-start(bf16[320,512]{1,0:T(8,128)(2,1)S(1)} %collective-permute-done.22.far), channel_id=1, source_target_pairs={{0,1},{1,0},{2,3},{3,2},{4,5},{5,4},{6,7},{7,6},{8,9},{9,8},{10,11... | collective-permute-start | bytes 983048 | tf_op jit(solution)/shard_map/ppermute | solution.py:17
  54.0 6.1 %collective-permute-start.16 = (bf16[320,512]{1,0:T(8,128)(2,1)S(1)}, bf16[320,512]{1,0:T(8,128)(2,1)S(1)}, u32[]{:S(2)}, u32[]{:S(2)}) collective-permute-start(bf16[320,512]{1,0:T(8,128)(2,1)S(1)} %collective-permute-done.15.far), channel_id=1, source_target_pairs={{0,1},{1,0},{2,3},{3,2},{4,5},{5,4},{6,7},{7,6},{8,9},{9,8},{10,11... | collective-permute-start | bytes 983048 | tf_op jit(solution)/shard_map/ppermute | solution.py:17
  54.6 10.9 %collective-permute-start.5 = (bf16[128,2048]{1,0:T(8,128)(2,1)S(1)}, bf16[128,2048]{1,0:T(8,128)(2,1)S(1)}, u32[]{:S(2)}, u32[]{:S(2)}) collective-permute-start(bf16[128,2048]{1,0:T(8,128)(2,1)S(1)} %get-tuple-element.36), channel_id=1, source_target_pairs={{0,1},{1,0},{2,3},{3,2},{4,5},{5,4},{6,7},{7,6},{8,9},{9,8},{10,11... | collective-permute-start | bytes 1572872 | tf_op jit(solution)/shard_map/ppermute | solution.py:17
  60.0 6.8 %collective-permute-start.24 = (bf16[320,1024]{1,0:T(8,128)(2,1)S(1)}, bf16[320,1024]{1,0:T(8,128)(2,1)S(1)}, u32[]{:S(2)}, u32[]{:S(2)}) collective-permute-start(bf16[320,1024]{1,0:T(8,128)(2,1)S(1)} %get-tuple-element.55), channel_id=1, source_target_pairs={{0,1},{1,0},{2,3},{3,2},{4,5},{5,4},{6,7},{7,6},{8,9},{9,8},{10,11... | collective-permute-start | bytes 1966088 | tf_op jit(solution)/shard_map/ppermute | solution.py:17
  66.2 36.6 %collective-permute-start.6 = (bf16[64,2048]{1,0:T(8,128)(2,1)}, bf16[64,2048]{1,0:T(8,128)(2,1)}, u32[]{:S(2)}, u32[]{:S(2)}) collective-permute-start(bf16[64,2048]{1,0:T(8,128)(2,1)} %add_convert_fusion.3), channel_id=1, source_target_pairs={{0,2},{1,3},{2,0},{3,1},{4,6},{5,7},{6,4},{7,5},{8,10},{9,11},{10,... | collective-permute-start | bytes 786440 | tf_op jit(solution)/shard_map/ppermute | solution.py:17
  66.9 15.8 %collective-permute-start.25 = (bf16[320,512]{1,0:T(8,128)(2,1)S(1)}, bf16[320,512]{1,0:T(8,128)(2,1)S(1)}, u32[]{:S(2)}, u32[]{:S(2)}) collective-permute-start(bf16[320,512]{1,0:T(8,128)(2,1)S(1)} %add_convert_fusion), channel_id=1, source_target_pairs={{0,2},{1,3},{2,0},{3,1},{4,6},{5,7},{6,4},{7,5},{8,10},{9,11},{10,... | collective-permute-start | bytes 983048 | tf_op jit(solution)/shard_map/ppermute | solution.py:17
  68.6 31.5 %collective-permute-start.18 = (bf16[320,512]{1,0:T(8,128)(2,1)S(1)}, bf16[320,512]{1,0:T(8,128)(2,1)S(1)}, u32[]{:S(2)}, u32[]{:S(2)}) collective-permute-start(bf16[320,512]{1,0:T(8,128)(2,1)S(1)} %add_convert_fusion.1), channel_id=1, source_target_pairs={{0,2},{1,3},{2,0},{3,1},{4,6},{5,7},{6,4},{7,5},{8,10},{9,11},{10,... | collective-permute-start | bytes 983048 | tf_op jit(solution)/shard_map/ppermute | solution.py:17
  82.9 21.1 %collective-permute-start.26 = (bf16[80,512]{1,0:T(8,128)(2,1)S(1)}, bf16[80,512]{1,0:T(8,128)(2,1)S(1)}, u32[]{:S(2)}, u32[]{:S(2)}) collective-permute-start(bf16[80,512]{1,0:T(8,128)(2,1)S(1)} %get-tuple-element.56), channel_id=1, source_target_pairs={{0,16},{4,20},{8,24},{12,28},{16,0},{20,4},{24,8},{28,12},{1,17},{... | collective-permute-start | bytes 245768 | tf_op jit(solution)/shard_map/ppermute | solution.py:17
  87.8 16.2 %collective-permute-start.27 = (bf16[80,512]{1,0:T(8,128)(2,1)S(1)}, bf16[80,512]{1,0:T(8,128)(2,1)S(1)}, u32[]{:S(2)}, u32[]{:S(2)}) collective-permute-start(bf16[80,512]{1,0:T(8,128)(2,1)S(1)} %get-tuple-element.57), channel_id=1, source_target_pairs={{0,20},{4,16},{8,28},{12,24},{16,4},{20,0},{24,12},{28,8},{1,21},{... | collective-permute-start | bytes 245768 | tf_op jit(solution)/shard_map/ppermute | solution.py:17
  88.7 19.5 %collective-permute-start.28 = (bf16[80,512]{1,0:T(8,128)(2,1)S(1)}, bf16[80,512]{1,0:T(8,128)(2,1)S(1)}, u32[]{:S(2)}, u32[]{:S(2)}) collective-permute-start(bf16[80,512]{1,0:T(8,128)(2,1)S(1)} %get-tuple-element.58), channel_id=1, source_target_pairs={{0,24},{4,28},{8,16},{12,20},{16,8},{20,12},{24,0},{28,4},{1,25},{... | collective-permute-start | bytes 245768 | tf_op jit(solution)/shard_map/ppermute | solution.py:17
  100.1 8.1 %collective-permute-start.29 = (bf16[80,512]{1,0:T(8,128)(2,1)S(1)}, bf16[80,512]{1,0:T(8,128)(2,1)S(1)}, u32[]{:S(2)}, u32[]{:S(2)}) collective-permute-start(bf16[80,512]{1,0:T(8,128)(2,1)S(1)} %get-tuple-element.59), channel_id=1, source_target_pairs={{0,28},{4,24},{8,20},{12,16},{16,12},{20,8},{24,4},{28,0},{1,29},{... | collective-permute-start | bytes 245768 | tf_op jit(solution)/shard_map/ppermute | solution.py:17
  102.8 6.2 %collective-permute-start.19 = (bf16[80,512]{1,0:T(8,128)(2,1)S(1)}, bf16[80,512]{1,0:T(8,128)(2,1)S(1)}, u32[]{:S(2)}, u32[]{:S(2)}) collective-permute-start(bf16[80,512]{1,0:T(8,128)(2,1)S(1)} %get-tuple-element.51), channel_id=1, source_target_pairs={{0,4},{4,0},{8,12},{12,8},{16,20},{20,16},{24,28},{28,24},{1,5},{5... | collective-permute-start | bytes 245768 | tf_op jit(solution)/shard_map/ppermute | solution.py:17
  (11 other events, 161.0 us)

commit v5 on v4

--- a/solution.py
+++ b/solution.py
@@ -171,6 +171,13 @@
         ).astype(BF16)
 
 
+def close_kernel(keep_ref, got_ref, last_ref, out_ref):
+    rows = last_ref.shape[0]
+    out_ref[...] = (
+        keep_ref[:rows, :].astype(F32) + got_ref[:rows, :].astype(F32) + last_ref[...].astype(F32)
+    ).astype(BF16)
+
+
 def local(kernel, outs, operands, smem=1, scratch=(), flops=1000000, limit=12, far=0):
     size = sum(x.size for x in operands)
     operands = list(operands)
@@ -479,9 +486,7 @@
         group = got.shape[0] // 2
         across = (kept[group:].astype(F32) + got[group:].astype(F32)).astype(BF16)
         last = swap(across, "tp", 2)
-        mixer_out = (
-            kept[:group].astype(F32) + got[:group].astype(F32) + last.astype(F32)
-        ).astype(BF16)
+        (mixer_out,) = local(close_kernel, [last.shape], (kept, got, last), smem=0)
     else:
         key_rows, value_rows, _ = lax.optimization_barrier((key_rows, value_rows, own))
         both, places = gathered_keys(key_rows, value_rows)

time: 112 us -> 112 us (level)
  waiting for transfers between devices: 25.6 us -> 28.4 us
  other arithmetic: 3.16 us -> 0.71 us
    ppermute x27, waiting for transfers between devices: 21 us -> 23.4 us  [swap(): return lax.ppermute(x, axis, [(i, i ^ mask) for i in range(count)])]
    convert_element_type x1 -> x0, other arithmetic: 1.75 us -> none  [shards(): mixer_out = (kept[:group].astype(F32) + got[:group].astype(F32) + last.as...]
    pallas_call x8 -> x9, Pallas kernels: 8.69 us -> 9.41 us  [local(): pl.pallas_call(kernel, out_shape=[jax.ShapeDtypeStruct(shape, BF16) for s...]
  transfers between devices with their start and end apart: 30 -> 30, of which waited for: 8 -> 8; matrix products, arithmetic and copies ran while one was open for 4% -> 2% of each run, Pallas kernels for 18% -> 20%
where the time goes in v5:
time: 112 us
  starting transfers between devices  53.4 us (48%)
  waiting for transfers between devices  28.4 us (25%)
  Pallas kernels  25.8 us (23%)
  local copies, waits for them, and re-layouts  2.56 us (2%)
    ppermute x27, starting transfers between devices, swap(): return lax.ppermute(x, axis, [(i, i ^ mask) for i in range(count)])  45.4 us
    ppermute x27, waiting for transfers between devices, swap(): return lax.ppermute(x, axis, [(i, i ^ mask) for i in range(count)])  23.4 us
    pallas_call x2, Pallas kernels, ffn(): pl.pallas_call(functools.partial(ffn_kernel, index), in_specs=[pl.BlockSp...  9.65 us
    pallas_call x9, Pallas kernels, local(): pl.pallas_call(kernel, out_shape=[jax.ShapeDtypeStruct(shape, BF16) for s...  9.41 us
    ppermute x3, starting transfers between devices, onward(): lax.ppermute(x, axis, [(i, i + step) for i in range(first, count - step)])  7.97 us
    ppermute x3, waiting for transfers between devices, onward(): lax.ppermute(x, axis, [(i, i + step) for i in range(first, count - step)])  4.95 us
    pallas_call x1, Pallas kernels, fetched(): pl.pallas_call(fetch_kernel, in_specs=[hbm] * 3, out_specs=[vmem] * 3, ou...  4.33 us
    pallas_call x1, Pallas kernels, dispatched(): pl.pallas_call(functools.partial(dispatch_kernel, experts, capacity), out...  2.42 us
  transfers between devices with their start and end apart: 30, of which 8 were waited for; matrix products, arithmetic and copies ran while one was open for 2% of the time, Pallas kernels for 20%

profile of v5, /device:TPU:0, one launch (start us, length us, event | category | flops | bytes accessed | tf_op | source)
XLA Modules:
  0.0 111.9 jit_solution(785702635908291578)
XLA Ops:
  0.7 2.4 %dispatch.1 = (bf16[80,512]{1,0:T(8,128)(2,1)}, bf16[80,512]{1,0:T(8,128)(2,1)}, bf16[80,512]{1,0:T(8,128)(2,1)}, bf16[80,512]{1,0:T(8,128)(2,1)}, bf16[80,512]{...) custom-call(s32[1]{0:T(128)} %bitcast.place_ref.here_ref, ...), custom_call_target="tpu_custom_call" | custom-call | flops 125829120 | bytes 786432 | tf_op jit(solution)/shard_map/dispatch/pallas_call | solution.py:244
  3.1 4.1 %collective-permute-start.10 = (bf16[80,512]{1,0:T(8,128)(2,1)}, bf16[80,512]{1,0:T(8,128)(2,1)S(1)}, u32[]{:S(2)}, u32[]{:S(2)}) collective-permute-start(bf16[80,512]{1,0:T(8,128)(2,1)} %get-tuple-element.41), channel_id=1, source_target_pairs={{0,16},{4,20},{8,24},{12,28},{16,0},{20,4},{24,8},{28,12},{1,17},{... | collective-permute-start | bytes 245768 | tf_op jit(solution)/shard_map/ppermute | solution.py:17
  7.2 1.2 %collective-permute-start.11 = (bf16[80,512]{1,0:T(8,128)(2,1)}, bf16[80,512]{1,0:T(8,128)(2,1)S(1)}, u32[]{:S(2)}, u32[]{:S(2)}) collective-permute-start(bf16[80,512]{1,0:T(8,128)(2,1)} %get-tuple-element.42), channel_id=1, source_target_pairs={{0,20},{4,16},{8,28},{12,24},{16,4},{20,0},{24,12},{28,8},{1,21},{... | collective-permute-start | bytes 245768 | tf_op jit(solution)/shard_map/ppermute | solution.py:17
  8.4 3.6 %collective-permute-start.12 = (bf16[80,512]{1,0:T(8,128)(2,1)}, bf16[80,512]{1,0:T(8,128)(2,1)S(1)}, u32[]{:S(2)}, u32[]{:S(2)}) collective-permute-start(bf16[80,512]{1,0:T(8,128)(2,1)} %get-tuple-element.43), channel_id=1, source_target_pairs={{0,24},{4,28},{8,16},{12,20},{16,8},{20,12},{24,0},{28,4},{1,25},{... | collective-permute-start | bytes 245768 | tf_op jit(solution)/shard_map/ppermute | solution.py:17
  13.1 1.7 %collective-permute-start = (bf16[256,384]{1,0:T(8,128)(2,1)S(1)}, bf16[256,384]{1,0:T(8,128)(2,1)S(1)}, u32[]{:S(2)}, u32[]{:S(2)}) collective-permute-start(bf16[256,384]{1,0:T(8,128)(2,1)S(1)} %shard_map.149), channel_id=1, source_target_pairs={{0,4},{4,0},{8,12},{12,8},{16,20},{20,16},{24,28},{28,24},{1,5},{5... | collective-permute-start | bytes 589832 | tf_op jit(solution)/shard_map/ppermute | solution.py:17
  15.6 6.8 %collective-permute-done.got_ref = bf16[256,384]{1,0:T(8,128)(2,1)S(1)} collective-permute-done((bf16[256,384]{1,0:T(8,128)(2,1)S(1)}, bf16[256,384]{1,0:T(8,128)(2,1)S(1)}, u32[]{:S(2)}, u32[]{:S(2)}) %collective-permute-start) | collective-permute-done | bytes 196640 | tf_op jit(solution)/shard_map/ppermute | solution.py:17
  23.1 1.1 shard_map.150
  24.2 2.7 %collective-permute-start.9 = (bf16[80,512]{1,0:T(8,128)(2,1)}, bf16[80,512]{1,0:T(8,128)(2,1)S(1)}, u32[]{:S(2)}, u32[]{:S(2)}) collective-permute-start(bf16[80,512]{1,0:T(8,128)(2,1)} %get-tuple-element.40), channel_id=1, source_target_pairs={{0,12},{4,8},{8,4},{12,0},{16,28},{20,24},{24,20},{28,16},{1,13},{... | collective-permute-start | bytes 245768 | tf_op jit(solution)/shard_map/ppermute | solution.py:17
  27.0 2.0 %collective-permute-start.1 = (bf16[512,256]{1,0:T(8,128)(2,1)S(1)}, bf16[512,256]{1,0:T(8,128)(2,1)S(1)}, u32[]{:S(2)}, u32[]{:S(2)}) collective-permute-start(bf16[512,256]{1,0:T(8,128)(2,1)S(1)} %get-tuple-element.32.own_ref), channel_id=1, source_target_pairs={{0,8},{4,12},{8,16},{12,20},{16,24},{20,28},{1,9},{5,13},{9,17},{1... | collective-permute-start | bytes 786440 | tf_op jit(solution)/shard_map/ppermute | solution.py:30
  31.5 1.6 %collective-permute-start.22 = (bf16[320,512]{1,0:T(8,128)(2,1)S(1)}, bf16[320,512]{1,0:T(8,128)(2,1)S(1)}, u32[]{:S(2)}, u32[]{:S(2)}) collective-permute-start(bf16[320,512]{1,0:T(8,128)(2,1)S(1)} %get-tuple-element.60), channel_id=1, source_target_pairs={{0,2},{1,3},{2,0},{3,1},{4,6},{5,7},{6,4},{7,5},{8,10},{9,11},{10,... | collective-permute-start | bytes 983048 | tf_op jit(solution)/shard_map/ppermute | solution.py:17
  33.1 5.3 %collective-permute-start.2 = (bf16[512,256]{1,0:T(8,128)(2,1)S(1)}, bf16[512,256]{1,0:T(8,128)(2,1)S(1)}, u32[]{:S(2)}, u32[]{:S(2)}) collective-permute-start(bf16[512,256]{1,0:T(8,128)(2,1)S(1)} %get-tuple-element.32.own_ref), channel_id=1, source_target_pairs={{0,16},{4,20},{8,24},{12,28},{1,17},{5,21},{9,25},{13,29},{2,18},{... | collective-permute-start | bytes 786440 | tf_op jit(solution)/shard_map/ppermute | solution.py:30
  39.7 4.9 %collective-permute-done.2.rest_1_ = bf16[512,256]{1,0:T(8,128)(2,1)S(1)} collective-permute-done((bf16[512,256]{1,0:T(8,128)(2,1)S(1)}, bf16[512,256]{1,0:T(8,128)(2,1)S(1)}, u32[]{:S(2)}, u32[]{:S(2)}) %collective-permute-start.2) | collective-permute-done | bytes 262176 | tf_op jit(solution)/shard_map/ppermute | solution.py:30
  44.7 4.2 %shard_map.151 = (bf16[256,128]{1,0:T(8,128)(2,1)S(1)}, bf16[256,128]{1,0:T(8,128)(2,1)S(1)}) custom-call(s32[1]{0:T(128)} %bitcast.place_ref.here_ref, f32[2]{0:T(128)S(1)} %copy-done.2, bf16[512,128]{1,0:T(8,128)(2,1)S(1)} %get-tuple-element.31.query_ref, bf16[512,256]{1,0:T(8,128)(2,1)S(1)} %get-tuple-element.32.own_ref, ...), custom_call_target="tpu_custom_call" | custom-call | flops 1073741824 | bytes 1179910 | tf_op jit(solution)/shard_map/pallas_call | solution.py:193
  49.6 4.3 %fetch.1 = (bf16[2048,896]{1,0:T(8,128)(2,1)S(1)}, bf16[2048,896]{1,0:T(8,128)(2,1)S(1)}, bf16[896,2048]{1,0:T(8,128)(2,1)S(1)}) custom-call(bf16[1,2048,896]{2,1,0:T(8,128)(2,1)} %gate.1, bf16[1,2048,896]{2,1,0:T(8,128)(2,1)} %up.1, bf16[1,896,2048]{2,1,0:T(8,128)(2,1)} %down.1), custom_call_target="tpu_custom_call" | custom-call | flops 550502400 | bytes 11010048 | tf_op jit(solution)/shard_map/fetch/pallas_call | solution.py:281
  55.1 4.8 %ffn.3 = (bf16[320,1024]{1,0:T(8,128)(2,1)S(1)}, bf16[320,1024]{1,0:T(8,128)(2,1)S(1)}) custom-call(s32[10]{0:T(128)S(1)} %pad_add_fusion.order_ref, bf16[640,512]{1,0:T(8,128)(2,1)S(1)} %shard_map.154.own, bf16[640,512]{1,0:T(8,128)(2,1)S(1)} %collective-permute-done.14.near, bf16[320,512]{1,0:T(8,128)(2,1)S(1)} %collective-permute-done.22.far, ...), custom_call_target="tpu_custom_call" | custom-call | flops 3523215360 | bytes 13631488 | tf_op jit(solution)/shard_map/ffn/pallas_call | solution.py:330
  60.0 4.8 %ffn.2 = (bf16[320,1024]{1,0:T(8,128)(2,1)S(1)}, bf16[320,1024]{1,0:T(8,128)(2,1)S(1)}) custom-call(s32[10]{0:T(128)S(1)} %pad_add_fusion.order_ref, bf16[640,512]{1,0:T(8,128)(2,1)S(1)} %shard_map.154.own, bf16[640,512]{1,0:T(8,128)(2,1)S(1)} %collective-permute-done.14.near, bf16[320,512]{1,0:T(8,128)(2,1)S(1)} %collective-permute-done.15.far, ...), custom_call_target="tpu_custom_call" | custom-call | flops 3523215360 | bytes 13631488 | tf_op jit(solution)/shard_map/ffn/pallas_call | solution.py:330
  66.2 1.6 %collective-permute-start.25 = (bf16[320,512]{1,0:T(8,128)(2,1)S(1)}, bf16[320,512]{1,0:T(8,128)(2,1)S(1)}, u32[]{:S(2)}, u32[]{:S(2)}) collective-permute-start(bf16[320,512]{1,0:T(8,128)(2,1)S(1)} %add_convert_fusion), channel_id=1, source_target_pairs={{0,2},{1,3},{2,0},{3,1},{4,6},{5,7},{6,4},{7,5},{8,10},{9,11},{10,... | collective-permute-start | bytes 983048 | tf_op jit(solution)/shard_map/ppermute | solution.py:17
  68.5 13.2 %collective-permute-done.25.over_ref = bf16[320,512]{1,0:T(8,128)(2,1)S(1)} collective-permute-done((bf16[320,512]{1,0:T(8,128)(2,1)S(1)}, bf16[320,512]{1,0:T(8,128)(2,1)S(1)}, u32[]{:S(2)}, u32[]{:S(2)}) %collective-permute-start.25) | collective-permute-done | bytes 327712 | tf_op jit(solution)/shard_map/ppermute | solution.py:17
  82.0 3.5 %collective-permute-start.26 = (bf16[80,512]{1,0:T(8,128)(2,1)S(1)}, bf16[80,512]{1,0:T(8,128)(2,1)S(1)}, u32[]{:S(2)}, u32[]{:S(2)}) collective-permute-start(bf16[80,512]{1,0:T(8,128)(2,1)S(1)} %get-tuple-element.56), channel_id=1, source_target_pairs={{0,16},{4,20},{8,24},{12,28},{16,0},{20,4},{24,8},{28,12},{1,17},{... | collective-permute-start | bytes 245768 | tf_op jit(solution)/shard_map/ppermute | solution.py:17
  86.5 13.7 %collective-permute-start.28 = (bf16[80,512]{1,0:T(8,128)(2,1)S(1)}, bf16[80,512]{1,0:T(8,128)(2,1)S(1)}, u32[]{:S(2)}, u32[]{:S(2)}) collective-permute-start(bf16[80,512]{1,0:T(8,128)(2,1)S(1)} %get-tuple-element.58), channel_id=1, source_target_pairs={{0,24},{4,28},{8,16},{12,20},{16,8},{20,12},{24,0},{28,4},{1,25},{... | collective-permute-start | bytes 245768 | tf_op jit(solution)/shard_map/ppermute | solution.py:17
  100.3 2.7 %collective-permute-start.29 = (bf16[80,512]{1,0:T(8,128)(2,1)S(1)}, bf16[80,512]{1,0:T(8,128)(2,1)S(1)}, u32[]{:S(2)}, u32[]{:S(2)}) collective-permute-start(bf16[80,512]{1,0:T(8,128)(2,1)S(1)} %get-tuple-element.59), channel_id=1, source_target_pairs={{0,28},{4,24},{8,20},{12,16},{16,12},{20,8},{24,4},{28,0},{1,29},{... | collective-permute-start | bytes 245768 | tf_op jit(solution)/shard_map/ppermute | solution.py:17
  103.2 1.8 %collective-permute-start.19 = (bf16[80,512]{1,0:T(8,128)(2,1)S(1)}, bf16[80,512]{1,0:T(8,128)(2,1)S(1)}, u32[]{:S(2)}, u32[]{:S(2)}) collective-permute-start(bf16[80,512]{1,0:T(8,128)(2,1)S(1)} %get-tuple-element.51), channel_id=1, source_target_pairs={{0,4},{4,0},{8,12},{12,8},{16,20},{20,16},{24,28},{28,24},{1,5},{5... | collective-permute-start | bytes 245768 | tf_op jit(solution)/shard_map/ppermute | solution.py:17
  105.1 1.7 %collective-permute-start.21 = (bf16[80,512]{1,0:T(8,128)(2,1)S(1)}, bf16[80,512]{1,0:T(8,128)(2,1)S(1)}, u32[]{:S(2)}, u32[]{:S(2)}) collective-permute-start(bf16[80,512]{1,0:T(8,128)(2,1)S(1)} %get-tuple-element.53), channel_id=1, source_target_pairs={{0,12},{4,8},{8,4},{12,0},{16,28},{20,24},{24,20},{28,16},{1,13},{... | collective-permute-start | bytes 245768 | tf_op jit(solution)/shard_map/ppermute | solution.py:17
  110.6 1.3 %shard_map.157 = bf16[192,512]{1,0:T(8,128)(2,1)} custom-call(f32[640,192]{1,0:T(8,128)S(1)} %bitcast_select_fusion.weight_ref, bf16[80,512]{1,0:T(8,128)(2,1)S(1)} %get-tuple-element.50.rest_0_, bf16[80,512]{1,0:T(8,128)(2,1)S(1)} %collective-permute-done.19.rest_1_, bf16[80,512]{1,0:T(8,128)(2,1)S(1)} %collective-permute-done.20.rest_2_, ...), custom_call_target="tpu_custom_call" | custom-call | flops 377487360 | bytes 901120 | tf_op jit(solution)/shard_map/pallas_call | solution.py:193
  (75 shorter events, 15.7 us)
Async XLA Ops:
  3.1 21.1 %collective-permute-start.10 = (bf16[80,512]{1,0:T(8,128)(2,1)}, bf16[80,512]{1,0:T(8,128)(2,1)S(1)}, u32[]{:S(2)}, u32[]{:S(2)}) collective-permute-start(bf16[80,512]{1,0:T(8,128)(2,1)} %get-tuple-element.41), channel_id=1, source_target_pairs={{0,16},{4,20},{8,24},{12,28},{16,0},{20,4},{24,8},{28,12},{1,17},{... | collective-permute-start | bytes 245768 | tf_op jit(solution)/shard_map/ppermute | solution.py:17
  7.2 17.1 %collective-permute-start.11 = (bf16[80,512]{1,0:T(8,128)(2,1)}, bf16[80,512]{1,0:T(8,128)(2,1)S(1)}, u32[]{:S(2)}, u32[]{:S(2)}) collective-permute-start(bf16[80,512]{1,0:T(8,128)(2,1)} %get-tuple-element.42), channel_id=1, source_target_pairs={{0,20},{4,16},{8,28},{12,24},{16,4},{20,0},{24,12},{28,8},{1,21},{... | collective-permute-start | bytes 245768 | tf_op jit(solution)/shard_map/ppermute | solution.py:17
  8.4 18.6 %collective-permute-start.12 = (bf16[80,512]{1,0:T(8,128)(2,1)}, bf16[80,512]{1,0:T(8,128)(2,1)S(1)}, u32[]{:S(2)}, u32[]{:S(2)}) collective-permute-start(bf16[80,512]{1,0:T(8,128)(2,1)} %get-tuple-element.43), channel_id=1, source_target_pairs={{0,24},{4,28},{8,16},{12,20},{16,8},{20,12},{24,0},{28,4},{1,25},{... | collective-permute-start | bytes 245768 | tf_op jit(solution)/shard_map/ppermute | solution.py:17
  12.0 17.7 %collective-permute-start.13 = (bf16[80,512]{1,0:T(8,128)(2,1)}, bf16[80,512]{1,0:T(8,128)(2,1)S(1)}, u32[]{:S(2)}, u32[]{:S(2)}) collective-permute-start(bf16[80,512]{1,0:T(8,128)(2,1)} %get-tuple-element.44), channel_id=1, source_target_pairs={{0,28},{4,24},{8,20},{12,16},{16,12},{20,8},{24,4},{28,0},{1,29},{... | collective-permute-start | bytes 245768 | tf_op jit(solution)/shard_map/ppermute | solution.py:17
  13.1 9.2 %collective-permute-start = (bf16[256,384]{1,0:T(8,128)(2,1)S(1)}, bf16[256,384]{1,0:T(8,128)(2,1)S(1)}, u32[]{:S(2)}, u32[]{:S(2)}) collective-permute-start(bf16[256,384]{1,0:T(8,128)(2,1)S(1)} %shard_map.149), channel_id=1, source_target_pairs={{0,4},{4,0},{8,12},{12,8},{16,20},{20,16},{24,28},{28,24},{1,5},{5... | collective-permute-start | bytes 589832 | tf_op jit(solution)/shard_map/ppermute | solution.py:17
  22.3 7.4 %collective-permute-start.7 = (bf16[80,512]{1,0:T(8,128)(2,1)}, bf16[80,512]{1,0:T(8,128)(2,1)S(1)}, u32[]{:S(2)}, u32[]{:S(2)}) collective-permute-start(bf16[80,512]{1,0:T(8,128)(2,1)} %get-tuple-element.38), channel_id=1, source_target_pairs={{0,4},{4,0},{8,12},{12,8},{16,20},{20,16},{24,28},{28,24},{1,5},{5... | collective-permute-start | bytes 245768 | tf_op jit(solution)/shard_map/ppermute | solution.py:17
  24.2 6.2 %collective-permute-start.9 = (bf16[80,512]{1,0:T(8,128)(2,1)}, bf16[80,512]{1,0:T(8,128)(2,1)S(1)}, u32[]{:S(2)}, u32[]{:S(2)}) collective-permute-start(bf16[80,512]{1,0:T(8,128)(2,1)} %get-tuple-element.40), channel_id=1, source_target_pairs={{0,12},{4,8},{8,4},{12,0},{16,28},{20,24},{24,20},{28,16},{1,13},{... | collective-permute-start | bytes 245768 | tf_op jit(solution)/shard_map/ppermute | solution.py:17
  27.0 11.4 %collective-permute-start.1 = (bf16[512,256]{1,0:T(8,128)(2,1)S(1)}, bf16[512,256]{1,0:T(8,128)(2,1)S(1)}, u32[]{:S(2)}, u32[]{:S(2)}) collective-permute-start(bf16[512,256]{1,0:T(8,128)(2,1)S(1)} %get-tuple-element.32.own_ref), channel_id=1, source_target_pairs={{0,8},{4,12},{8,16},{12,20},{16,24},{20,28},{1,9},{5,13},{9,17},{1... | collective-permute-start | bytes 786440 | tf_op jit(solution)/shard_map/ppermute | solution.py:30
  31.5 8.2 %collective-permute-start.22 = (bf16[320,512]{1,0:T(8,128)(2,1)S(1)}, bf16[320,512]{1,0:T(8,128)(2,1)S(1)}, u32[]{:S(2)}, u32[]{:S(2)}) collective-permute-start(bf16[320,512]{1,0:T(8,128)(2,1)S(1)} %get-tuple-element.60), channel_id=1, source_target_pairs={{0,2},{1,3},{2,0},{3,1},{4,6},{5,7},{6,4},{7,5},{8,10},{9,11},{10,... | collective-permute-start | bytes 983048 | tf_op jit(solution)/shard_map/ppermute | solution.py:17
  33.1 22.0 %collective-permute-start.14 = (bf16[640,512]{1,0:T(8,128)(2,1)S(1)}, bf16[640,512]{1,0:T(8,128)(2,1)S(1)}, u32[]{:S(2)}, u32[]{:S(2)}) collective-permute-start(bf16[640,512]{1,0:T(8,128)(2,1)S(1)} %shard_map.154.own), channel_id=1, source_target_pairs={{0,1},{1,0},{2,3},{3,2},{4,5},{5,4},{6,7},{7,6},{8,9},{9,8},{10,11... | collective-permute-start | bytes 1966088 | tf_op jit(solution)/shard_map/ppermute | solution.py:17
  33.1 11.6 %collective-permute-start.2 = (bf16[512,256]{1,0:T(8,128)(2,1)S(1)}, bf16[512,256]{1,0:T(8,128)(2,1)S(1)}, u32[]{:S(2)}, u32[]{:S(2)}) collective-permute-start(bf16[512,256]{1,0:T(8,128)(2,1)S(1)} %get-tuple-element.32.own_ref), channel_id=1, source_target_pairs={{0,16},{4,20},{8,24},{12,28},{1,17},{5,21},{9,25},{13,29},{2,18},{... | collective-permute-start | bytes 786440 | tf_op jit(solution)/shard_map/ppermute | solution.py:30
  38.4 6.2 %collective-permute-start.3 = (bf16[512,256]{1,0:T(8,128)(2,1)S(1)}, bf16[512,256]{1,0:T(8,128)(2,1)S(1)}, u32[]{:S(2)}, u32[]{:S(2)}) collective-permute-start(bf16[512,256]{1,0:T(8,128)(2,1)S(1)} %collective-permute-done.1.rest_0_), channel_id=1, source_target_pairs={{8,24},{12,28},{9,25},{13,29},{10,26},{14,30},{11,27},{15,31}} | collective-permute-start | bytes 786440 | tf_op jit(solution)/shard_map/ppermute | solution.py:30
  39.2 14.8 %collective-permute-start.15 = (bf16[320,512]{1,0:T(8,128)(2,1)S(1)}, bf16[320,512]{1,0:T(8,128)(2,1)S(1)}, u32[]{:S(2)}, u32[]{:S(2)}) collective-permute-start(bf16[320,512]{1,0:T(8,128)(2,1)S(1)} %get-tuple-element.61), channel_id=1, source_target_pairs={{0,2},{1,3},{2,0},{3,1},{4,6},{5,7},{6,4},{7,5},{8,10},{9,11},{10,... | collective-permute-start | bytes 983048 | tf_op jit(solution)/shard_map/ppermute | solution.py:17
  39.7 15.4 %collective-permute-start.23 = (bf16[320,512]{1,0:T(8,128)(2,1)S(1)}, bf16[320,512]{1,0:T(8,128)(2,1)S(1)}, u32[]{:S(2)}, u32[]{:S(2)}) collective-permute-start(bf16[320,512]{1,0:T(8,128)(2,1)S(1)} %collective-permute-done.22.far), channel_id=1, source_target_pairs={{0,1},{1,0},{2,3},{3,2},{4,5},{5,4},{6,7},{7,6},{8,9},{9,8},{10,11... | collective-permute-start | bytes 983048 | tf_op jit(solution)/shard_map/ppermute | solution.py:17
  54.5 10.9 %collective-permute-start.5 = (bf16[128,2048]{1,0:T(8,128)(2,1)S(1)}, bf16[128,2048]{1,0:T(8,128)(2,1)S(1)}, u32[]{:S(2)}, u32[]{:S(2)}) collective-permute-start(bf16[128,2048]{1,0:T(8,128)(2,1)S(1)} %get-tuple-element.36), channel_id=1, source_target_pairs={{0,1},{1,0},{2,3},{3,2},{4,5},{5,4},{6,7},{7,6},{8,9},{9,8},{10,11... | collective-permute-start | bytes 1572872 | tf_op jit(solution)/shard_map/ppermute | solution.py:17
  59.9 6.2 %collective-permute-start.24 = (bf16[320,1024]{1,0:T(8,128)(2,1)S(1)}, bf16[320,1024]{1,0:T(8,128)(2,1)S(1)}, u32[]{:S(2)}, u32[]{:S(2)}) collective-permute-start(bf16[320,1024]{1,0:T(8,128)(2,1)S(1)} %get-tuple-element.55), channel_id=1, source_target_pairs={{0,1},{1,0},{2,3},{3,2},{4,5},{5,4},{6,7},{7,6},{8,9},{9,8},{10,11... | collective-permute-start | bytes 1966088 | tf_op jit(solution)/shard_map/ppermute | solution.py:17
  65.5 37.7 %collective-permute-start.6 = (bf16[64,2048]{1,0:T(8,128)(2,1)S(1)}, bf16[64,2048]{1,0:T(8,128)(2,1)S(1)}, u32[]{:S(2)}, u32[]{:S(2)}) collective-permute-start(bf16[64,2048]{1,0:T(8,128)(2,1)S(1)} %add_convert_fusion.2), channel_id=1, source_target_pairs={{0,2},{1,3},{2,0},{3,1},{4,6},{5,7},{6,4},{7,5},{8,10},{9,11},{10,... | collective-permute-start | bytes 786440 | tf_op jit(solution)/shard_map/ppermute | solution.py:17
  66.2 15.6 %collective-permute-start.25 = (bf16[320,512]{1,0:T(8,128)(2,1)S(1)}, bf16[320,512]{1,0:T(8,128)(2,1)S(1)}, u32[]{:S(2)}, u32[]{:S(2)}) collective-permute-start(bf16[320,512]{1,0:T(8,128)(2,1)S(1)} %add_convert_fusion), channel_id=1, source_target_pairs={{0,2},{1,3},{2,0},{3,1},{4,6},{5,7},{6,4},{7,5},{8,10},{9,11},{10,... | collective-permute-start | bytes 983048 | tf_op jit(solution)/shard_map/ppermute | solution.py:17
  67.9 32.4 %collective-permute-start.18 = (bf16[320,512]{1,0:T(8,128)(2,1)S(1)}, bf16[320,512]{1,0:T(8,128)(2,1)S(1)}, u32[]{:S(2)}, u32[]{:S(2)}) collective-permute-start(bf16[320,512]{1,0:T(8,128)(2,1)S(1)} %add_convert_fusion.1), channel_id=1, source_target_pairs={{0,2},{1,3},{2,0},{3,1},{4,6},{5,7},{6,4},{7,5},{8,10},{9,11},{10,... | collective-permute-start | bytes 983048 | tf_op jit(solution)/shard_map/ppermute | solution.py:17
  82.0 23.1 %collective-permute-start.26 = (bf16[80,512]{1,0:T(8,128)(2,1)S(1)}, bf16[80,512]{1,0:T(8,128)(2,1)S(1)}, u32[]{:S(2)}, u32[]{:S(2)}) collective-permute-start(bf16[80,512]{1,0:T(8,128)(2,1)S(1)} %get-tuple-element.56), channel_id=1, source_target_pairs={{0,16},{4,20},{8,24},{12,28},{16,0},{20,4},{24,8},{28,12},{1,17},{... | collective-permute-start | bytes 245768 | tf_op jit(solution)/shard_map/ppermute | solution.py:17
  85.5 19.6 %collective-permute-start.27 = (bf16[80,512]{1,0:T(8,128)(2,1)S(1)}, bf16[80,512]{1,0:T(8,128)(2,1)S(1)}, u32[]{:S(2)}, u32[]{:S(2)}) collective-permute-start(bf16[80,512]{1,0:T(8,128)(2,1)S(1)} %get-tuple-element.57), channel_id=1, source_target_pairs={{0,20},{4,16},{8,28},{12,24},{16,4},{20,0},{24,12},{28,8},{1,21},{... | collective-permute-start | bytes 245768 | tf_op jit(solution)/shard_map/ppermute | solution.py:17
  86.5 21.3 %collective-permute-start.28 = (bf16[80,512]{1,0:T(8,128)(2,1)S(1)}, bf16[80,512]{1,0:T(8,128)(2,1)S(1)}, u32[]{:S(2)}, u32[]{:S(2)}) collective-permute-start(bf16[80,512]{1,0:T(8,128)(2,1)S(1)} %get-tuple-element.58), channel_id=1, source_target_pairs={{0,24},{4,28},{8,16},{12,20},{16,8},{20,12},{24,0},{28,4},{1,25},{... | collective-permute-start | bytes 245768 | tf_op jit(solution)/shard_map/ppermute | solution.py:17
  100.3 8.1 %collective-permute-start.29 = (bf16[80,512]{1,0:T(8,128)(2,1)S(1)}, bf16[80,512]{1,0:T(8,128)(2,1)S(1)}, u32[]{:S(2)}, u32[]{:S(2)}) collective-permute-start(bf16[80,512]{1,0:T(8,128)(2,1)S(1)} %get-tuple-element.59), channel_id=1, source_target_pairs={{0,28},{4,24},{8,20},{12,16},{16,12},{20,8},{24,4},{28,0},{1,29},{... | collective-permute-start | bytes 245768 | tf_op jit(solution)/shard_map/ppermute | solution.py:17
  103.2 6.1 %collective-permute-start.19 = (bf16[80,512]{1,0:T(8,128)(2,1)S(1)}, bf16[80,512]{1,0:T(8,128)(2,1)S(1)}, u32[]{:S(2)}, u32[]{:S(2)}) collective-permute-start(bf16[80,512]{1,0:T(8,128)(2,1)S(1)} %get-tuple-element.51), channel_id=1, source_target_pairs={{0,4},{4,0},{8,12},{12,8},{16,20},{20,16},{24,28},{28,24},{1,5},{5... | collective-permute-start | bytes 245768 | tf_op jit(solution)/shard_map/ppermute | solution.py:17
  (11 other events, 162.4 us)
